TPU v7x, 32 devices: a whole 2x2x4 slice. The times are simulated.
32 devices in a mesh: grp: 2 (over y), fs: 4 (over z), tp: 4 (over x, core).
Axes of the slice: x: 2, y: 2, z: 4, core: 2. Of those that a mesh axis runs over, the one named last changes fastest.
Arguments:
- tokens: bfloat16 [32, 128, 2048], P(('grp', 'fs'), None, 'tp'), parts along dimension 0, may hold values from -100 to 100
- mix_gain: float32 [2048], replicated, may hold values from 0.1 to 1.9
- gate_outer: bfloat16 [2048, 1024], P('fs', 'tp'), may hold values from -0.125 to 0.125
- gate_inner: bfloat16 [2048, 1024], P('fs', 'tp'), may hold values from -0.125 to 0.125
- value_weight: bfloat16 [2048, 1024], P('fs', 'tp'), may hold values from -0.125 to 0.125
- conv_taps: float32 [3, 1024], replicated, may hold values from -3 to 3
- mix_out: bfloat16 [1024, 2048], P('tp', 'fs'), may hold values from -0.25 to 0.25
- ffn_gain: float32 [2048], replicated, may hold values from 0.1 to 1.9
- ffn_gate: bfloat16 [2048, 5632], P('fs', 'tp'), may hold values from -0.125 to 0.125
- ffn_up: bfloat16 [2048, 5632], P('fs', 'tp'), may hold values from -0.125 to 0.125
- ffn_down: bfloat16 [5632, 2048], P('tp', 'fs'), may hold values from -0.109375 to 0.109375
- out_gain: float32 [2048], replicated, may hold values from 0.1 to 1.9
Outputs:
- layer_out: bfloat16 [32, 128, 2048], P(('grp', 'fs'), None, 'tp'), parts along dimension 0
There are 2 independent parts, one for each index of `grp`. A program takes and returns all parts, laid end to end along the dimension named above; an argument that names none is the same for every part. Nothing has to cross between parts.
All inputs are finite; a program needn't handle non-finite values.
Results may differ from a plain program's by a relative error of at most 0.015.
Values may be sent and summed in bfloat16 or wider, within the bound.
No kernel may reach another device: no remote copies, remote signals or barrier semaphores. Data moves between devices by JAX's collectives and lax.ppermute only.
A program may use at most 64 MiB of HBM per device.

v0:
```python
import jax
import jax.numpy as jnp
from jax import lax
from jax.sharding import PartitionSpec as P


def rms_norm(values, gain):
    floats = values.astype(jnp.float32)
    scaled = floats * lax.rsqrt(jnp.mean(floats * floats, axis=-1, keepdims=True) + 1e-06)
    return (scaled * gain).astype(jnp.bfloat16)


def local(
    tokens,
    mix_gain,
    gate_outer,
    gate_inner,
    value_weight,
    conv_taps,
    mix_out,
    ffn_gain,
    ffn_gate,
    ffn_up,
    ffn_down,
    out_gain,
):
    seq_count, length, columns = tokens.shape
    row_count = seq_count * length
    width = columns * lax.axis_size("tp")
    whole = lax.all_gather(tokens, "tp", axis=2, tiled=True).reshape(row_count, width)
    normed = rms_norm(whole, mix_gain)
    channels = gate_outer.shape[1]
    pieces = (
        lax.all_gather(gate_outer, "fs", axis=0, tiled=True),
        lax.all_gather(gate_inner, "fs", axis=0, tiled=True),
        lax.all_gather(value_weight, "fs", axis=0, tiled=True),
    )
    sliced = normed
    outer = jnp.dot(sliced, pieces[0], preferred_element_type=jnp.float32)
    inner = jnp.dot(sliced, pieces[1], preferred_element_type=jnp.float32)
    values = jnp.dot(sliced, pieces[2], preferred_element_type=jnp.float32)
    outer = outer.astype(jnp.bfloat16)
    inner = inner.astype(jnp.bfloat16)
    values = values.astype(jnp.bfloat16)
    product = (inner.astype(jnp.float32) * values.astype(jnp.float32)).reshape(
        seq_count, length, channels
    )
    own_taps = lax.dynamic_slice_in_dim(conv_taps, lax.axis_index("tp") * channels, channels, 1)
    tap_count = conv_taps.shape[0]
    padded = jnp.pad(product, ((0, 0), (tap_count - 1, 0), (0, 0)))
    conv = jnp.zeros((seq_count, length, channels), jnp.float32)
    for offset in range(tap_count):
        conv = conv + own_taps[offset] * padded[:, offset : offset + length]
    gated = (outer.astype(jnp.float32) * conv.reshape(row_count, channels)).astype(jnp.bfloat16)
    mix_terms = jnp.dot(
        gated, lax.all_gather(mix_out, "fs", axis=1, tiled=True), preferred_element_type=jnp.float32
    )
    mix_full = lax.psum(mix_terms.astype(jnp.bfloat16), "tp").astype(jnp.float32)
    first_full = (whole.astype(jnp.float32) + mix_full).astype(jnp.bfloat16)
    first = lax.dynamic_slice_in_dim(first_full, lax.axis_index("tp") * columns, columns, 1)
    normed_ffn = rms_norm(first_full, ffn_gain)
    pieces = (
        lax.all_gather(ffn_gate, "fs", axis=0, tiled=True),
        lax.all_gather(ffn_up, "fs", axis=0, tiled=True),
    )
    sliced = normed_ffn
    gate = jnp.dot(sliced, pieces[0], preferred_element_type=jnp.float32)
    upward = jnp.dot(sliced, pieces[1], preferred_element_type=jnp.float32)
    hidden = (jax.nn.silu(gate) * upward).astype(jnp.bfloat16)
    down_terms = jnp.dot(
        hidden,
        lax.all_gather(ffn_down, "fs", axis=1, tiled=True),
        preferred_element_type=jnp.float32,
    )
    down_summed = lax.psum_scatter(
        down_terms.astype(jnp.bfloat16), "tp", scatter_dimension=1, tiled=True
    ).astype(jnp.float32)
    second = first.astype(jnp.float32) + down_summed
    squares = lax.psum(jnp.sum(second * second, axis=1), "tp")
    factor = lax.rsqrt(squares / width + 1e-06)
    own_gain = lax.dynamic_slice_in_dim(out_gain, lax.axis_index("tp") * columns, columns, 0)
    result = second * factor[:, None] * own_gain
    return result.astype(jnp.bfloat16).reshape(seq_count, length, columns)


def solution(mesh):
    in_specs = (
        P(("grp", "fs"), None, "tp"),
        P(),
        P("fs", "tp"),
        P("fs", "tp"),
        P("fs", "tp"),
        P(),
        P("tp", "fs"),
        P(),
        P("fs", "tp"),
        P("fs", "tp"),
        P("tp", "fs"),
        P(),
    )
    out_specs = P(("grp", "fs"), None, "tp")
    return jax.shard_map(local, mesh=mesh, in_specs=in_specs, out_specs=out_specs, check_vma=False)
```

profile of v0, /device:TPU:0, one launch (start us, length us, event | category | flops | bytes accessed | tf_op | source)
XLA Modules:
  0.0 587.0 jit_solution(15794149463791373341)
XLA Ops:
  6.5 0.7 all-gather.9.cloned.1.call-update
  7.3 0.7 all-gather.15.cloned.1.call-update
  8.1 0.7 all-gather.13.cloned.1.call-update
  8.8 0.5 all-gather.11.cloned.1.call-update
  9.4 0.5 all-gather.17.cloned.1.call-update
  10.0 0.9 constant_dynamic-slice_fusion
  10.8 23.4 %all-gather.9.cloned.1.call-done = bf16[4,128,2048]{2,1,0:T(8,128)(2,1)} async-done(((bf16[4,128,512]{2,1,0:T(8,128)(2,1)}), bf16[4,128,2048]{2,1,0:T(8,128)(2,1)}) %all-gather.9.cloned.1.call-update) | async-done | bytes 2097168 | tf_op jit(solution)/shard_map/all_gather | solution.py:30
  34.2 2.2 fusion.3
  36.5 0.5 fusion.5
  37.0 26.8 %all-gather.15.cloned.1.call-done = bf16[2048,256]{1,0:T(8,128)(2,1)} async-done(((bf16[512,256]{1,0:T(8,128)(2,1)}), bf16[2048,256]{1,0:T(8,128)(2,1)}) %all-gather.15.cloned.1.call-update) | async-done | bytes 1048592 | tf_op jit(solution)/shard_map/all_gather | solution.py:36
  63.8 1.9 fusion.13
  65.7 27.0 %all-gather.13.cloned.1.call-done = bf16[2048,256]{1,0:T(8,128)(2,1)} async-done(((bf16[512,256]{1,0:T(8,128)(2,1)}), bf16[2048,256]{1,0:T(8,128)(2,1)}) %all-gather.13.cloned.1.call-update) | async-done | bytes 1048592 | tf_op jit(solution)/shard_map/all_gather | solution.py:35
  92.8 1.9 fusion.12
  94.9 26.7 %all-gather.11.cloned.1.call-done = bf16[2048,256]{1,0:T(8,128)(2,1)} async-done(((bf16[512,256]{1,0:T(8,128)(2,1)}), bf16[2048,256]{1,0:T(8,128)(2,1)}) %all-gather.11.cloned.1.call-update) | async-done | bytes 1048592 | tf_op jit(solution)/shard_map/all_gather | solution.py:34
  121.6 28.8 %all-gather.17.cloned.1.call-done = bf16[256,2048]{1,0:T(8,128)(2,1)} async-done(((bf16[256,512]{1,0:T(8,128)(2,1)}), bf16[256,2048]{1,0:T(8,128)(2,1)}) %all-gather.17.cloned.1.call-update) | async-done | bytes 1048592 | tf_op jit(solution)/shard_map/all_gather | solution.py:56
  150.4 5.2 convolution_convert_fusion
  155.7 0.7 all-gather.19.cloned.1.call-update
  156.4 0.7 all-gather.21.cloned.1.call-update
  157.2 0.7 all-gather.23.cloned.1.call-update
  157.9 0.2 reduce-scatter.2.cloned.1.call-start
  158.1 48.4 %all-reduce.3.cloned.1.call-done = bf16[512,2048]{1,0:T(8,128)(2,1)} async-done(((bf16[512,2048]{1,0:T(8,128)(2,1)}), bf16[512,2048]{1,0:T(8,128)(2,1)}) %all-reduce.3.cloned.1.call-update) | async-done | bytes 2097168 | tf_op jit(solution)/shard_map/psum | solution.py:58
  206.5 3.9 fusion
  210.5 104.4 %all-gather.19.cloned.1.call-done = bf16[2048,1408]{1,0:T(8,128)(2,1)} async-done(((bf16[512,1408]{1,0:T(8,128)(2,1)}), bf16[2048,1408]{1,0:T(8,128)(2,1)}) %all-gather.19.cloned.1.call-update) | async-done | bytes 5767184 | tf_op jit(solution)/shard_map/all_gather | solution.py:63
  314.9 8.4 %fusion.16 = f32[512,1408]{1,0:T(8,128)} fusion(bf16[2048,1408]{1,0:T(8,128)(2,1)} %all-gather.19.cloned.1.call-done, bf16[512,2048]{1,0:T(8,128)(2,1)} %get-tuple-element.6, f32[2048]{0:T(1024)S(1)} %copy-done.4, f32[512]{0:T(512)S(1)} %add_rsqrt_fusion.1), kind=kOutput, calls=%fused_computation.28 | convolution fusion | flops 2956984320 | bytes 10758144 | tf_op jit(solution)/shard_map/dot_general | solution.py:67
  323.3 98.1 %all-gather.21.cloned.1.call-done = bf16[2048,1408]{1,0:T(8,128)(2,1)} async-done(((bf16[512,1408]{1,0:T(8,128)(2,1)}), bf16[2048,1408]{1,0:T(8,128)(2,1)}) %all-gather.21.cloned.1.call-update) | async-done | bytes 5767184 | tf_op jit(solution)/shard_map/all_gather | solution.py:64
  421.4 106.5 %all-gather.23.cloned.1.call-done = bf16[1408,2048]{1,0:T(8,128)(2,1)} async-done(((bf16[1408,512]{1,0:T(8,128)(2,1)}), bf16[1408,2048]{1,0:T(8,128)(2,1)}) %all-gather.23.cloned.1.call-update) | async-done | bytes 5767184 | tf_op jit(solution)/shard_map/all_gather | solution.py:72
  528.0 13.4 %convolution_convert_fusion.1 = bf16[512,2048]{1,0:T(8,128)(2,1)} fusion(bf16[1408,2048]{1,0:T(8,128)(2,1)} %all-gather.23.cloned.1.call-done, bf16[2048,1408]{1,0:T(8,128)(2,1)} %all-gather.21.cloned.1.call-done, f32[512,1408]{1,0:T(8,128)} %fusion.16, bf16[512,2048]{1,0:T(8,128)(2,1)S(1)} %copy-done.2, f32[2048]{0:T(1024)S(1)} %copy-done.4, ...), kind=kOutput, calls=%fused_computation.15 | convolution fusion | flops 5915148288 | bytes 18622464 | tf_op jit(solution)/shard_map/dot_general | solution.py:70
  541.4 0.8 dynamic_slice.11
  542.2 28.8 %reduce-scatter.2.cloned.1.call-done = bf16[512,512]{1,0:T(8,128)(2,1)} async-done(((bf16[512,2048]{1,0:T(8,128)(2,1)}), bf16[512,512]{1,0:T(8,128)(2,1)}) %reduce-scatter.2.cloned.1.call-update) | async-done | bytes 524304 | tf_op jit(solution)/shard_map/reduce_scatter | solution.py:75
  571.0 1.3 multiply_reduce_fusion
  572.3 5.8 psum.15
  578.1 2.0 multiply_convert_fusion
  (25 shorter events, 0.5 us)
Async XLA Ops:
  6.5 29.9 %copy-start.3 = (f32[2048]{0:T(1024)S(1)}, f32[2048]{0:T(1024)}, u32[]{:S(2)}) copy-start(f32[2048]{0:T(1024)} %param.13) | copy-start | bytes 24580
  6.5 27.7 %all-gather.9.cloned.1.call-start = ((), (), s32[]{:S(2)}) async-start(), calls=%async_computation.1 | async-start | bytes 2621440 | tf_op jit(solution)/shard_map/all_gather | solution.py:30
  7.3 56.5 %all-gather.15.cloned.1.call-start = ((), (), s32[]{:S(2)}) async-start(), calls=%async_computation.4 | async-start | bytes 1310720 | tf_op jit(solution)/shard_map/all_gather | solution.py:36
  8.0 84.8 %all-gather.13.cloned.1.call-start = ((), (), s32[]{:S(2)}) async-start(), calls=%async_computation.3 | async-start | bytes 1310720 | tf_op jit(solution)/shard_map/all_gather | solution.py:35
  8.7 112.8 %all-gather.11.cloned.1.call-start = ((), (), s32[]{:S(2)}) async-start(), calls=%async_computation.2 | async-start | bytes 1310720 | tf_op jit(solution)/shard_map/all_gather | solution.py:34
  9.3 141.1 %all-gather.17.cloned.1.call-start = ((), (), s32[]{:S(2)}) async-start(), calls=%async_computation.5 | async-start | bytes 1310720 | tf_op jit(solution)/shard_map/all_gather | solution.py:56
  9.9 196.6 %all-reduce.3.cloned.1.call-start = ((), (), s32[]{:S(2)}) async-start(), calls=%async_computation.6 | async-start | bytes 4194304 | tf_op jit(solution)/shard_map/psum | solution.py:58
  34.2 2.2 copy-start
  155.6 50.9 %copy-start.1 = (bf16[4,128,2048]{2,1,0:T(8,128)(2,1)S(1)}, bf16[4,128,2048]{2,1,0:T(8,128)(2,1)}, u32[]{:S(2)}) copy-start(bf16[4,128,2048]{2,1,0:T(8,128)(2,1)} %all-gather.9.cloned.1.call-done) | copy-start | bytes 6291460
  155.6 159.3 %all-gather.19.cloned.1.call-start = ((), (), s32[]{:S(2)}) async-start(), calls=%async_computation.7 | async-start | bytes 7208960 | tf_op jit(solution)/shard_map/all_gather | solution.py:63
  156.4 265.1 %all-gather.21.cloned.1.call-start = ((), (), s32[]{:S(2)}) async-start(), calls=%async_computation.8 | async-start | bytes 7208960 | tf_op jit(solution)/shard_map/all_gather | solution.py:64
  157.1 370.9 %all-gather.23.cloned.1.call-start = ((), (), s32[]{:S(2)}) async-start(), calls=%async_computation.9 | async-start | bytes 7208960 | tf_op jit(solution)/shard_map/all_gather | solution.py:72
  157.9 157.0 %copy-start.4 = (f32[2048]{0:T(1024)S(1)}, f32[2048]{0:T(1024)}, u32[]{:S(2)}) copy-start(f32[2048]{0:T(1024)} %param.19) | copy-start | bytes 24580
  157.9 413.2 %reduce-scatter.2.cloned.1.call-start = ((), (), s32[]{:S(2)}) async-start(), calls=%async_computation.10 | async-start | bytes 2621440 | tf_op jit(solution)/shard_map/reduce_scatter | solution.py:75
  314.9 213.1 %copy-start.2 = (bf16[512,2048]{1,0:T(8,128)(2,1)S(1)}, bf16[512,2048]{1,0:T(8,128)(2,1)}, u32[]{:S(2)}) copy-start(bf16[512,2048]{1,0:T(8,128)(2,1)} %get-tuple-element.6) | copy-start | bytes 6291460
Sparse Core Ops, SparseCore 0:
  8.9 25.2 all-gather.8
  35.8 27.9 all-gather.14
  65.4 27.3 all-gather.12
  94.2 27.3 all-gather.10
  123.0 27.3 all-gather.16
  155.7 50.7 all-reduce.2
  208.1 106.7 all-gather.18
  316.5 104.9 all-gather.20
  423.0 104.9 all-gather.22
  541.6 29.4 reduce-scatter.1
where the time goes:
time: 587 us
  waiting for transfers between devices  524 us (89%)
  matrix products  30.9 us (5%)
  between operations  13.6 us (2%)
  other arithmetic  10.2 us (2%)
    all_gather x1, waiting for transfers between devices, local(): lax.all_gather(ffn_down, 'fs', axis=1, tiled=True)  107 us
    all_gather x1, waiting for transfers between devices, local(): lax.all_gather(ffn_gate, 'fs', axis=0, tiled=True)  104 us
    all_gather x1, waiting for transfers between devices, local(): lax.all_gather(ffn_up, 'fs', axis=0, tiled=True)  98.1 us
    psum x1, waiting for transfers between devices, local(): lax.psum(mix_terms.astype(jnp.bfloat16), 'tp').astype(jnp.float32)  48.4 us
    reduce_scatter x1, waiting for transfers between devices, local(): lax.psum_scatter(down_terms.astype(jnp.bfloat16), 'tp', scatter_dimension...  28.8 us
    all_gather x1, waiting for transfers between devices, local(): lax.all_gather(mix_out, 'fs', axis=1, tiled=True)  28.8 us
    all_gather x1, waiting for transfers between devices, local(): lax.all_gather(gate_inner, 'fs', axis=0, tiled=True)  27 us
    all_gather x1, waiting for transfers between devices, local(): lax.all_gather(value_weight, 'fs', axis=0, tiled=True)  26.8 us
  transfers between devices with their start and end apart: 10, of which 10 were waited for; matrix products, arithmetic and copies ran while one was open for 4% of the time, Pallas kernels for 0%

commit v1 on v0

v1 whole, which is shorter than its diff:
```python
import functools

import jax
import jax.numpy as jnp
from jax import lax
from jax.experimental import pallas as pl
from jax.experimental.pallas import tpu as pltpu
from jax.sharding import PartitionSpec as P


BF16 = jnp.bfloat16
F32 = jnp.float32
VMEM_LIMIT = 56 * 1024 * 1024


def rms_norm(values, gain):
    floats = values.astype(F32)
    scaled = floats * lax.rsqrt(jnp.mean(floats * floats, axis=-1, keepdims=True) + 1e-06)
    return (scaled * gain).astype(BF16)


def plain_local(
    tokens, mix_gain, gate_outer, gate_inner, value_weight, conv_taps, mix_out,
    ffn_gain, ffn_gate, ffn_up, ffn_down, out_gain,
):
    seq_count, length, columns = tokens.shape
    row_count = seq_count * length
    width = columns * lax.axis_size("tp")
    whole = lax.all_gather(tokens, "tp", axis=2, tiled=True).reshape(row_count, width)
    normed = rms_norm(whole, mix_gain)
    channels = gate_outer.shape[1]

    def project(left, weight):
        full = lax.all_gather(weight, "fs", axis=0, tiled=True)
        return jnp.dot(left, full, preferred_element_type=F32)

    outer = project(normed, gate_outer).astype(BF16)
    inner = project(normed, gate_inner).astype(BF16)
    values = project(normed, value_weight).astype(BF16)
    product = (inner.astype(F32) * values.astype(F32)).reshape(seq_count, length, channels)
    own_taps = lax.dynamic_slice_in_dim(conv_taps, lax.axis_index("tp") * channels, channels, 1)
    tap_count = conv_taps.shape[0]
    padded = jnp.pad(product, ((0, 0), (tap_count - 1, 0), (0, 0)))
    conv = jnp.zeros((seq_count, length, channels), F32)
    for offset in range(tap_count):
        conv = conv + own_taps[offset] * padded[:, offset : offset + length]
    gated = (outer.astype(F32) * conv.reshape(row_count, channels)).astype(BF16)
    mix_terms = jnp.dot(
        gated, lax.all_gather(mix_out, "fs", axis=1, tiled=True), preferred_element_type=F32
    )
    mix_full = lax.psum(mix_terms.astype(BF16), "tp").astype(F32)
    first_full = (whole.astype(F32) + mix_full).astype(BF16)
    first = lax.dynamic_slice_in_dim(first_full, lax.axis_index("tp") * columns, columns, 1)
    normed_ffn = rms_norm(first_full, ffn_gain)
    gate = project(normed_ffn, ffn_gate)
    upward = project(normed_ffn, ffn_up)
    hidden = (jax.nn.silu(gate) * upward).astype(BF16)
    down_terms = jnp.dot(
        hidden, lax.all_gather(ffn_down, "fs", axis=1, tiled=True), preferred_element_type=F32
    )
    down_summed = lax.psum_scatter(
        down_terms.astype(BF16), "tp", scatter_dimension=1, tiled=True
    ).astype(F32)
    second = first.astype(F32) + down_summed
    squares = lax.psum(jnp.sum(second * second, axis=1), "tp")
    factor = lax.rsqrt(squares / width + 1e-06)
    own_gain = lax.dynamic_slice_in_dim(out_gain, lax.axis_index("tp") * columns, columns, 0)
    result = second * factor[:, None] * own_gain
    return result.astype(BF16).reshape(seq_count, length, columns)


def dot(left, right):
    return jnp.dot(left, right, preferred_element_type=F32)


def norm_kernel(info, gain, b0, b1, b2, b3, out, *, width):
    q = info[2]
    blocks = [b[h].astype(F32) for b in (b0, b1, b2, b3) for h in range(2)]
    squares = sum(jnp.sum(b * b, axis=-1, keepdims=True) for b in blocks)
    factor = lax.rsqrt(squares / width + 1e-06)
    for r in range(4):
        for h in range(2):
            own = gain[(q ^ r) * 2 + h]
            out[2 * r + h] = (blocks[2 * r + h] * factor * own).astype(BF16)


def norm_call(info, gain, blocks):
    _, rows, half = blocks[0].shape
    tile = min(rows, 128)
    width = 8 * half
    spec = pl.BlockSpec((2, tile, half), lambda i, s: (0, i, 0))
    return pl.pallas_call(
        functools.partial(norm_kernel, width=width),
        grid_spec=pltpu.PrefetchScalarGridSpec(
            num_scalar_prefetch=1,
            grid=(rows // tile,),
            in_specs=[pl.BlockSpec((8, 1, half), lambda i, s: (0, 0, 0))] + [spec] * 4,
            out_specs=pl.BlockSpec((8, tile, half), lambda i, s: (0, i, 0)),
        ),
        out_shape=jax.ShapeDtypeStruct((8, rows, half), BF16),
        cost_estimate=pl.CostEstimate(
            flops=4000000 * rows // 512, bytes_accessed=4 * rows * width, transcendentals=rows
        ),
        name="norm",
    )(info, gain.reshape(8, 1, half), *blocks)


def place(info, step, direction, count):
    z, q = info[0], info[2]
    shard = lax.rem(z + (count - step if direction > 0 else step), count)
    return shard ^ q


def contract(x, info, own, own_row, pieces, direction, count, row, columns):
    g = info[1]
    half = x.shape[2]
    total = None
    spot = place(info, 0, direction, count)
    for h in range(2):
        term = dot(x[2 * spot + h], own[own_row + h * half : own_row + (h + 1) * half, columns])
        total = term if total is None else total + term
    for step, swapped, piece in pieces:
        spot = place(info, step, direction, count)
        part = 1 - g if swapped else g
        total = total + dot(x[2 * spot + part], piece[row : row + half, :])
    return total


def mixer_kernel(*refs, count, length):
    info, taps, x, outer_own, inner_own, value_own, mix_own = refs[:7]
    steps = count - 1
    ahead, ahead_y = refs[7 : 7 + steps], refs[7 + steps : 7 + 2 * steps]
    back, back_y = refs[7 + 2 * steps : 7 + 3 * steps], refs[7 + 3 * steps : 7 + 4 * steps]
    out = refs[-1]
    half = x.shape[2]
    everything = slice(None)
    g = info[1]
    cw = [(k + 1, s, p) for s, group in ((False, ahead), (True, ahead_y)) for k, p in enumerate(group)]
    ccw = [(k + 1, s, p) for s, group in ((False, back), (True, back_y)) for k, p in enumerate(group)]
    inner = contract(x, info, inner_own, 0, cw, 1, count, 0, everything).astype(BF16)
    values = contract(x, info, value_own, 0, cw, 1, count, half, everything).astype(BF16)
    outer = contract(x, info, outer_own, 0, ccw, -1, count, 0, everything).astype(BF16)
    product = inner.astype(F32) * values.astype(F32)
    position = lax.broadcasted_iota(jnp.int32, product.shape, 0) % length
    tap_count = taps.shape[0]
    conv = jnp.zeros(product.shape, F32)
    for offset in range(tap_count):
        back_by = tap_count - 1 - offset
        if back_by:
            moved = pltpu.roll(product, back_by, axis=0)
            moved = jnp.where(position >= back_by, moved, 0.0)
        else:
            moved = product
        conv = conv + taps[offset][None, :] * moved
    gated = (outer.astype(F32) * conv).astype(BF16)

    def store(step, part, value):
        spot = place(info, step, -1, count)
        out[lax.rem(spot, 2), spot // 2, part] = value.astype(BF16)

    for h in range(2):
        store(0, h, dot(gated, mix_own[:, h * half : (h + 1) * half]))
    for step, swapped, piece in ccw:
        store(step, 1 - g if swapped else g, dot(gated, piece[half:, :]))


def full(shape):
    return pl.BlockSpec(shape, lambda *_: (0,) * len(shape))


def mixer_call(info, taps, x, owns, cw, cw_y, ccw, ccw_y, count, length):
    _, rows, half = x.shape
    tap_count = taps.shape[0]
    channels = owns[0].shape[1]
    operands = [x, *owns, *cw, *cw_y, *ccw, *ccw_y]
    return pl.pallas_call(
        functools.partial(mixer_kernel, count=count, length=length),
        grid_spec=pltpu.PrefetchScalarGridSpec(
            num_scalar_prefetch=1,
            grid=(1,),
            in_specs=[pl.BlockSpec((tap_count, channels), lambda i, s: (0, s[2]))]
            + [full(o.shape) for o in operands],
            out_specs=full((2, 2, 2, rows, half)),
        ),
        out_shape=jax.ShapeDtypeStruct((2, 2, 2, rows, half), BF16),
        cost_estimate=pl.CostEstimate(
            flops=8 * rows * 8 * half * channels, bytes_accessed=16000000, transcendentals=0
        ),
        compiler_params=pltpu.CompilerParams(vmem_limit_bytes=VMEM_LIMIT),
        name="mixer",
    )(info, taps, *operands)


def hidden_kernel(*refs, count, start, size):
    info, x, gate_own, up_own = refs[:4]
    steps = count - 1
    groups = [refs[4 + i * steps : 4 + (i + 1) * steps] for i in range(4)]
    out = refs[-1]
    columns = slice(start, start + size)
    cw = [(k + 1, i == 1, p) for i in (0, 1) for k, p in enumerate(groups[i])]
    ccw = [(k + 1, i == 3, p) for i in (2, 3) for k, p in enumerate(groups[i])]
    gate = contract(x, info, gate_own, 0, cw, 1, count, 0, columns)
    upward = contract(x, info, up_own, 0, ccw, -1, count, 0, columns)
    out[...] = (gate / (1.0 + jnp.exp(-gate)) * upward).astype(BF16)


def hidden_call(info, x, gate_own, up_own, cw, cw_y, ccw, ccw_y, count, start, size):
    _, rows, half = x.shape
    operands = [gate_own, up_own, *cw, *cw_y, *ccw, *ccw_y]
    tile = min(rows, 256)
    return pl.pallas_call(
        functools.partial(hidden_kernel, count=count, start=start, size=size),
        grid_spec=pltpu.PrefetchScalarGridSpec(
            num_scalar_prefetch=1,
            grid=(rows // tile,),
            in_specs=[pl.BlockSpec((8, tile, half), lambda i, s: (0, i, 0))]
            + [full(o.shape) for o in operands],
            out_specs=pl.BlockSpec((tile, size), lambda i, s: (i, 0)),
        ),
        out_shape=jax.ShapeDtypeStruct((rows, size), BF16),
        cost_estimate=pl.CostEstimate(
            flops=4 * rows * 8 * half * size,
            bytes_accessed=4 * 8 * half * size,
            transcendentals=rows * size,
        ),
        compiler_params=pltpu.CompilerParams(vmem_limit_bytes=VMEM_LIMIT),
        name="hidden",
    )(info, x, *operands)


def down_kernel(*refs, count, split):
    info, left, right, own = refs[:4]
    steps = count - 1
    groups = [refs[4 + i * steps : 4 + (i + 1) * steps] for i in range(4)]
    out = refs[-1]
    g = info[1]
    piece = out.shape[-1]

    def product(weight):
        return dot(left[...], weight[:split]) + dot(right[...], weight[split:])

    def store(spot, part, value):
        out[lax.rem(spot, 2), spot // 2, part] = value.astype(BF16)

    for h in range(2):
        value = product(own[:, 2 * h * piece : 2 * (h + 1) * piece])
        for i in range(2):
            store(place(info, 0, 1, count), 2 * h + i, value[:, i * piece : (i + 1) * piece])
    for k in range(steps):
        for direction, mine, other in ((1, groups[0][k], groups[1][k]), (-1, groups[2][k], groups[3][k])):
            value = product(jnp.concatenate([mine[...], other[...]], axis=1))
            spot = place(info, k + 1, direction, count)
            last = 0 if direction > 0 else 1
            store(spot, 2 * g + last, value[:, :piece])
            store(spot, 2 * (1 - g) + last, value[:, piece:])


def down_call(info, left, right, own, cw, cw_y, ccw, ccw_y, count):
    rows, split = left.shape
    piece = cw[0].shape[1]
    operands = [left, right, own, *cw, *cw_y, *ccw, *ccw_y]
    return pl.pallas_call(
        functools.partial(down_kernel, count=count, split=split),
        grid_spec=pltpu.PrefetchScalarGridSpec(
            num_scalar_prefetch=1,
            grid=(1,),
            in_specs=[full(o.shape) for o in operands],
            out_specs=full((2, 2, 4, rows, piece)),
        ),
        out_shape=jax.ShapeDtypeStruct((2, 2, 4, rows, piece), BF16),
        cost_estimate=pl.CostEstimate(
            flops=2 * rows * own.shape[0] * 16 * piece,
            bytes_accessed=2 * own.shape[0] * 16 * piece,
            transcendentals=0,
        ),
        compiler_params=pltpu.CompilerParams(vmem_limit_bytes=VMEM_LIMIT),
        name="down",
    )(info, *operands)


def ring_local(
    tokens, mix_gain, gate_outer, gate_inner, value_weight, conv_taps, mix_out,
    ffn_gain, ffn_gate, ffn_up, ffn_down, out_gain,
):
    count = lax.axis_size("fs")
    seq_count, length, columns = tokens.shape
    rows = seq_count * length
    half = columns // 2
    width = columns * lax.axis_size("tp")
    z, g, q = lax.axis_index("fs"), lax.axis_index("grp"), lax.axis_index("tp")
    info = jnp.stack([z, g, q]).astype(jnp.int32)

    ahead = [(i, (i + 1) % count) for i in range(count)]
    behind = [(d, s) for s, d in ahead]

    def ring(value, pairs):
        arrived, swapped = [], []
        for _ in range(1, count):
            value = lax.ppermute(value, "fs", pairs)
            arrived.append(value)
            swapped.append(lax.ppermute(value, "grp", [(0, 1), (1, 0)]))
        return arrived, swapped

    def mate(value):
        return lax.ppermute(value, "tp", [(i, i ^ 1) for i in range(4)])

    def across(value):
        return lax.ppermute(value, "tp", [(i, i ^ 2) for i in range(4)])

    def gather(own):
        other = across(own)
        return own, mate(own), other, mate(other)

    def rows_of(weight):
        return lax.dynamic_slice_in_dim(weight, g * half, half, 0)

    own_tokens = tokens.reshape(rows, 2, half).transpose(1, 0, 2)
    blocks = gather(own_tokens)

    mix_half = lax.dynamic_slice_in_dim(mix_out, g * half, half, 1)
    m_cw = ring(jnp.concatenate([rows_of(gate_inner), rows_of(value_weight)]), ahead)
    m_ccw = ring(jnp.concatenate([rows_of(gate_outer), mix_half]), behind)
    units = ffn_gate.shape[1]
    split = -(-units // 256) * 128
    gate_half, up_half = rows_of(ffn_gate), rows_of(ffn_up)
    g1 = ring(gate_half[:, :split], ahead)
    u1 = ring(up_half[:, :split], behind)
    g2 = ring(gate_half[:, split:], ahead)
    u2 = ring(up_half[:, split:], behind)
    down_half = lax.dynamic_slice_in_dim(ffn_down, g * half, half, 1)
    d_cw = ring(down_half[:, : half // 2], ahead)
    d_ccw = ring(down_half[:, half // 2 :], behind)

    def scatter(partial):
        met = partial[0].astype(F32) + mate(partial[1]).astype(F32)
        return met[0] + across(met[1].astype(BF16)).astype(F32)

    x = norm_call(info, mix_gain, blocks)
    partial = mixer_call(
        info, conv_taps, x, (gate_outer, gate_inner, value_weight, mix_out), *m_cw, *m_ccw, count, length
    )
    first = (own_tokens.astype(F32) + scatter(partial)).astype(BF16)
    x = norm_call(info, ffn_gain, gather(first))
    left = hidden_call(info, x, ffn_gate, ffn_up, *g1, *u1, count, 0, split)
    right = hidden_call(info, x, ffn_gate, ffn_up, *g2, *u2, count, split, units - split)
    partial = down_call(info, left, right, ffn_down, *d_cw, *d_ccw, count)
    summed = scatter(partial)
    second = first.transpose(1, 0, 2).reshape(rows, columns).astype(F32)
    second = second + summed.transpose(1, 0, 2).reshape(rows, columns)
    squares = lax.psum(jnp.sum(second * second, axis=1), "tp")
    factor = lax.rsqrt(squares / width + 1e-06)
    own_gain = lax.dynamic_slice_in_dim(out_gain, q * columns, columns, 0)
    result = second * factor[:, None] * own_gain
    return result.astype(BF16).reshape(seq_count, length, columns)


def fits_ring(mesh):
    shape = mesh.shape
    return shape["grp"] == 2 and shape["tp"] == 4 and shape["fs"] == 4


def solution(mesh):
    in_specs = (
        P(("grp", "fs"), None, "tp"),
        P(),
        P("fs", "tp"),
        P("fs", "tp"),
        P("fs", "tp"),
        P(),
        P("tp", "fs"),
        P(),
        P("fs", "tp"),
        P("fs", "tp"),
        P("tp", "fs"),
        P(),
    )
    out_specs = P(("grp", "fs"), None, "tp")
    body = ring_local if fits_ring(mesh) else plain_local

    return jax.shard_map(body, mesh=mesh, in_specs=in_specs, out_specs=out_specs, check_vma=False)
```

time: 587 us -> 329 us (0.56)
  waiting for transfers between devices: 524 us -> 173 us
  starting transfers between devices: 0.53 us -> 77.9 us
  Pallas kernels: 0 us -> 43.8 us
  matrix products: 30.9 us -> 0 us
  local copies, waits for them, and re-layouts: 1.66 us -> 22 us
  between operations: 13.6 us -> 0.39 us
    all_gather x8 -> x0, waiting for transfers between devices: 442 us -> none  [the longest x1 107 us: local(): lax.all_gather(ffn_down, 'fs', axis=1, tiled=True)]
    ppermute x0 -> x58, waiting for transfers between devices: none -> 173 us  [the longest x24 98 us: ring(): value = lax.ppermute(value, 'fs', pairs)]
    ppermute x0 -> x58, starting transfers between devices: none -> 77.9 us  [the longest x24 43 us: ring(): value = lax.ppermute(value, 'fs', pairs)]
    psum x1 -> x0, waiting for transfers between devices: 48.4 us -> none  [local(): lax.psum(mix_terms.astype(jnp.bfloat16), 'tp').astype(jnp.float32)]
    pallas_call x0 -> x6, Pallas kernels: none -> 43.8 us  [the longest x2 16.9 us: hidden_call(): pl.pallas_call(functools.partial(hidden_kernel, count=count, start=start,...]
    dot_general x5 -> x0, matrix products: 30.9 us -> none  [the longest x1 13.4 us: local(): jnp.dot(hidden, lax.all_gather(ffn_down, 'fs', axis=1, tiled=True), prefe...]
    reduce_scatter x1 -> x0, waiting for transfers between devices: 28.8 us -> none  [local(): lax.psum_scatter(down_terms.astype(jnp.bfloat16), 'tp', scatter_dimension...]
    convert_element_type x0 -> x6, local copies, waits for them, and re-layouts: none -> 8.62 us  [the longest x4 7.71 us: ring_local(): second = first.transpose(1, 0, 2).reshape(rows, columns).astype(F32)]
  transfers between devices with their start and end apart: 10 -> 58, of which waited for: 10 -> 31; matrix products, arithmetic and copies ran while one was open for 4% -> 5% of each run, Pallas kernels for 0% -> 8%
where the time goes in v1:
time: 329 us; the launch traced here: 328 us
  waiting for transfers between devices  173 us (53%)
  starting transfers between devices  77.9 us (24%)
  Pallas kernels  43.8 us (13%)
  local copies, waits for them, and re-layouts  22 us (7%)
  blocking collectives  5.91 us (2%)
  other arithmetic  5.13 us (2%)
    ppermute x24, waiting for transfers between devices, ring(): value = lax.ppermute(value, 'fs', pairs)  98 us
    ppermute x24, waiting for transfers between devices, ring(): swapped.append(lax.ppermute(value, 'grp', [(0, 1), (1, 0)]))  67.2 us
    ppermute x24, starting transfers between devices, ring(): value = lax.ppermute(value, 'fs', pairs)  43 us
    ppermute x24, starting transfers between devices, ring(): swapped.append(lax.ppermute(value, 'grp', [(0, 1), (1, 0)]))  29.5 us
    pallas_call x2, Pallas kernels, hidden_call(): pl.pallas_call(functools.partial(hidden_kernel, count=count, start=start,...  16.9 us
    pallas_call x2, Pallas kernels, norm_call(): pl.pallas_call(functools.partial(norm_kernel, width=width), grid_spec=plt...  10.2 us
    pallas_call x1, Pallas kernels, down_call(): pl.pallas_call(functools.partial(down_kernel, count=count, split=split),...  8.58 us
    pallas_call x1, Pallas kernels, mixer_call(): pl.pallas_call(functools.partial(mixer_kernel, count=count, length=length...  8.2 us
  transfers between devices with their start and end apart: 58, of which 31 were waited for; matrix products, arithmetic and copies ran while one was open for 5% of the time, Pallas kernels for 8%

profile of v1, /device:TPU:0, one launch (start us, length us, event | category | flops | bytes accessed | tf_op | source)
XLA Modules:
  0.0 328.3 jit_solution(3801928901055699822)
XLA Ops:
  4.5 3.7 %collective-permute-start.9 = (bf16[512,256]{1,0:T(8,128)(2,1)S(1)}, bf16[512,256]{1,0:T(8,128)(2,1)S(1)}, u32[]{:S(2)}, u32[]{:S(2)}) collective-permute-start(bf16[512,256]{1,0:T(8,128)(2,1)S(1)} %pad_maximum_fusion.1), channel_id=1, source_target_pairs={{4,0},{8,4},{12,8},{0,12},{5,1},{9,5},{13,9},{1,13},{6,2},{10,6},{... | collective-permute-start | bytes 786440 | tf_op jit(solution)/shard_map/ppermute | solution.py:299
  8.3 6.5 %collective-permute-done.9.refs_13_ = bf16[512,256]{1,0:T(8,128)(2,1)S(1)} collective-permute-done((bf16[512,256]{1,0:T(8,128)(2,1)S(1)}, bf16[512,256]{1,0:T(8,128)(2,1)S(1)}, u32[]{:S(2)}, u32[]{:S(2)}) %collective-permute-start.9) | collective-permute-done | bytes 262176 | tf_op jit(solution)/shard_map/ppermute | solution.py:299
  14.8 4.3 %collective-permute-start.10 = (bf16[512,256]{1,0:T(8,128)(2,1)S(1)}, bf16[512,256]{1,0:T(8,128)(2,1)S(1)}, u32[]{:S(2)}, u32[]{:S(2)}) collective-permute-start(bf16[512,256]{1,0:T(8,128)(2,1)S(1)} %collective-permute-done.9.refs_13_), channel_id=1, source_target_pairs={{4,0},{8,4},{12,8},{0,12},{5,1},{9,5},{13,9},{1,13},{6,2},{10,6},{... | collective-permute-start | bytes 786440 | tf_op jit(solution)/shard_map/ppermute | solution.py:299
  26.1 4.3 %collective-permute-start.11 = (bf16[512,256]{1,0:T(8,128)(2,1)S(1)}, bf16[512,256]{1,0:T(8,128)(2,1)}, u32[]{:S(2)}, u32[]{:S(2)}) collective-permute-start(bf16[512,256]{1,0:T(8,128)(2,1)S(1)} %collective-permute-done.10.refs_14_), channel_id=1, source_target_pairs={{4,0},{8,4},{12,8},{0,12},{5,1},{9,5},{13,9},{1,13},{6,2},{10,6},{... | collective-permute-start | bytes 786440 | tf_op jit(solution)/shard_map/ppermute | solution.py:299
  45.3 5.1 %norm.2.refs_2_ = bf16[8,512,256]{2,1,0:T(8,128)(2,1)} custom-call(s32[3]{0:T(128)} %pad_add_fusion.info.refs_0_, f32[8,1,256]{2,1,0:T(1,128)} %bitcast.57, bf16[2,512,256]{2,1,0:T(8,128)(2,1)} %bitcast.56, bf16[2,512,256]{2,1,0:T(8,128)(2,1)} %copy-done.10, bf16[2,512,256]{2,1,0:T(8,128)(2,1)} %copy-done.8, bf16[2,512,256]{2,1,0:T(8,128)(2,1)} %copy-done.11), custom_call_target="tpu_custom_call" | custom-call | flops 4000000 | bytes 4194304 | tf_op jit(solution)/shard_map/norm/pallas_call | solution.py:92
  50.5 4.3 %collective-permute-done.7.refs_11_ = bf16[512,256]{1,0:T(8,128)(2,1)} collective-permute-done((bf16[512,256]{1,0:T(8,128)(2,1)}, bf16[512,256]{1,0:T(8,128)(2,1)}, u32[]{:S(2)}, u32[]{:S(2)}) %collective-permute-start.7) | collective-permute-done | bytes 262176 | tf_op jit(solution)/shard_map/ppermute | solution.py:301
  54.8 4.5 %collective-permute-done.14.refs_18_ = bf16[512,256]{1,0:T(8,128)(2,1)} collective-permute-done((bf16[512,256]{1,0:T(8,128)(2,1)}, bf16[512,256]{1,0:T(8,128)(2,1)}, u32[]{:S(2)}, u32[]{:S(2)}) %collective-permute-start.14) | collective-permute-done | bytes 262176 | tf_op jit(solution)/shard_map/ppermute | solution.py:301
  62.2 8.2 %mixer.1 = bf16[2,2,2,512,256]{4,3,2,1,0:T(8,128)(2,1)} custom-call(s32[3]{0:T(128)} %pad_add_fusion.info.refs_0_, f32[3,1024]{1,0:T(4,128)} %refs_1_.1, bf16[8,512,256]{2,1,0:T(8,128)(2,1)} %norm.2.refs_2_, bf16[512,256]{1,0:T(8,128)(2,1)} %refs_3_.4, bf16[512,256]{1,0:T(8,128)(2,1)} %refs_4_.1, bf16[512,256]{1,0:T(8,128)(2,1)} %refs_5_.1, ...), custom_call_target="tpu_custom_call" | custom-call | flops 2147483648 | bytes 16000000 | tf_op jit(solution)/shard_map/mixer/pallas_call | solution.py:176
  89.2 27.6 %collective-permute-done.38.refs_10_ = bf16[256,640]{1,0:T(8,128)(2,1)S(1)} collective-permute-done((bf16[256,640]{1,0:T(8,128)(2,1)S(1)}, bf16[256,640]{1,0:T(8,128)(2,1)S(1)}, u32[]{:S(2)}, u32[]{:S(2)}) %collective-permute-start.38) | collective-permute-done | bytes 327712 | tf_op jit(solution)/shard_map/ppermute | solution.py:299
  118.9 3.3 collective-permute-start.39
  126.2 6.5 %collective-permute-done.33.refs_5_ = bf16[256,640]{1,0:T(8,128)(2,1)S(1)} collective-permute-done((bf16[256,640]{1,0:T(8,128)(2,1)}, bf16[256,640]{1,0:T(8,128)(2,1)S(1)}, u32[]{:S(2)}, u32[]{:S(2)}) %collective-permute-start.33) | collective-permute-done | bytes 327712 | tf_op jit(solution)/shard_map/ppermute | solution.py:299
  132.7 6.8 %collective-permute-done.39.refs_11_ = bf16[256,640]{1,0:T(8,128)(2,1)S(1)} collective-permute-done((bf16[256,640]{1,0:T(8,128)(2,1)S(1)}, bf16[256,640]{1,0:T(8,128)(2,1)S(1)}, u32[]{:S(2)}, u32[]{:S(2)}) %collective-permute-start.39) | collective-permute-done | bytes 327712 | tf_op jit(solution)/shard_map/ppermute | solution.py:299
  140.1 3.3 collective-permute-start.51
  148.5 14.7 %collective-permute-done.51.refs_11_ = bf16[1408,128]{1,0:T(8,128)(2,1)S(1)} collective-permute-done((bf16[1408,128]{1,0:T(8,128)(2,1)S(1)}, bf16[1408,128]{1,0:T(8,128)(2,1)S(1)}, u32[]{:S(2)}, u32[]{:S(2)}) %collective-permute-start.51) | collective-permute-done | bytes 360480 | tf_op jit(solution)/shard_map/ppermute | solution.py:299
  165.9 3.3 collective-permute-start.40
  177.0 6.9 %collective-permute-done.29.refs_13_ = bf16[256,768]{1,0:T(8,128)(2,1)S(1)} collective-permute-done((bf16[256,768]{1,0:T(8,128)(2,1)S(1)}, bf16[256,768]{1,0:T(8,128)(2,1)S(1)}, u32[]{:S(2)}, u32[]{:S(2)}) %collective-permute-start.29) | collective-permute-done | bytes 393248 | tf_op jit(solution)/shard_map/ppermute | solution.py:301
  184.4 3.3 collective-permute-start.52
  191.6 5.3 %collective-permute-done.42.refs_14_ = bf16[256,640]{1,0:T(8,128)(2,1)S(1)} collective-permute-done((bf16[256,640]{1,0:T(8,128)(2,1)S(1)}, bf16[256,640]{1,0:T(8,128)(2,1)S(1)}, u32[]{:S(2)}, u32[]{:S(2)}) %collective-permute-start.42) | collective-permute-done | bytes 327712 | tf_op jit(solution)/shard_map/ppermute | solution.py:301
  197.4 3.3 collective-permute-start.28
  200.7 3.2 collective-permute-done.52.refs_12_
  205.4 6.9 %collective-permute-done.22.refs_6_ = bf16[256,768]{1,0:T(8,128)(2,1)} collective-permute-done((bf16[256,768]{1,0:T(8,128)(2,1)S(1)}, bf16[256,768]{1,0:T(8,128)(2,1)}, u32[]{:S(2)}, u32[]{:S(2)}) %collective-permute-start.22) | collective-permute-done | bytes 393248 | tf_op jit(solution)/shard_map/ppermute | solution.py:299
  213.8 4.2 %collective-permute-done.28.refs_12_ = bf16[256,768]{1,0:T(8,128)(2,1)} collective-permute-done((bf16[256,768]{1,0:T(8,128)(2,1)}, bf16[256,768]{1,0:T(8,128)(2,1)}, u32[]{:S(2)}, u32[]{:S(2)}) %collective-permute-start.28) | collective-permute-done | bytes 393248 | tf_op jit(solution)/shard_map/ppermute | solution.py:299
  222.4 5.1 %norm.3.refs_1_ = bf16[8,512,256]{2,1,0:T(8,128)(2,1)} custom-call(s32[3]{0:T(128)} %pad_add_fusion.info.refs_0_, f32[8,1,256]{2,1,0:T(1,128)} %bitcast.58, bf16[2,512,256]{2,1,0:T(8,128)(2,1)} %copy-done.1, bf16[2,512,256]{2,1,0:T(8,128)(2,1)} %copy-done.12, bf16[2,512,256]{2,1,0:T(8,128)(2,1)} %copy-done.9, bf16[2,512,256]{2,1,0:T(8,128)(2,1)} %copy-done.13), custom_call_target="tpu_custom_call" | custom-call | flops 4000000 | bytes 4194304 | tf_op jit(solution)/shard_map/norm/pallas_call | solution.py:92
  228.9 16.9 %collective-permute-done.37.refs_9_ = bf16[256,640]{1,0:T(8,128)(2,1)} collective-permute-done((bf16[256,640]{1,0:T(8,128)(2,1)}, bf16[256,640]{1,0:T(8,128)(2,1)}, u32[]{:S(2)}, u32[]{:S(2)}) %collective-permute-start.37) | collective-permute-done | bytes 327712 | tf_op jit(solution)/shard_map/ppermute | solution.py:301
  247.3 5.5 %collective-permute-done.43.refs_15_ = bf16[256,640]{1,0:T(8,128)(2,1)} collective-permute-done((bf16[256,640]{1,0:T(8,128)(2,1)}, bf16[256,640]{1,0:T(8,128)(2,1)}, u32[]{:S(2)}, u32[]{:S(2)}) %collective-permute-start.43) | collective-permute-done | bytes 327712 | tf_op jit(solution)/shard_map/ppermute | solution.py:301
  256.4 8.3 %hidden.3.refs_2_ = bf16[512,640]{1,0:T(8,128)(2,1)} custom-call(s32[3]{0:T(128)} %pad_add_fusion.info.refs_0_, bf16[8,512,256]{2,1,0:T(8,128)(2,1)} %norm.3.refs_1_, bf16[512,1408]{1,0:T(8,128)(2,1)} %refs_2_.3, bf16[512,1408]{1,0:T(8,128)(2,1)} %refs_3_.6, bf16[256,640]{1,0:T(8,128)(2,1)} %collective-permute-done.32.refs_4_, bf16[256,640]{1,0:T(8,128)(2,1)} %copy-done.34, ...), custom_call_target="tpu_custom_call" | custom-call | flops 2684354560 | bytes 5242880 | tf_op jit(solution)/shard_map/hidden/pallas_call | solution.py:211
  264.7 8.5 %hidden.2.refs_1_ = bf16[512,768]{1,0:T(8,128)(2,1)} custom-call(s32[3]{0:T(128)} %pad_add_fusion.info.refs_0_, bf16[8,512,256]{2,1,0:T(8,128)(2,1)} %norm.3.refs_1_, bf16[512,1408]{1,0:T(8,128)(2,1)} %refs_2_.3, bf16[512,1408]{1,0:T(8,128)(2,1)} %refs_3_.6, bf16[256,768]{1,0:T(8,128)(2,1)} %collective-permute-done.20.refs_4_, bf16[256,768]{1,0:T(8,128)(2,1)} %copy-done.19, ...), custom_call_target="tpu_custom_call" | custom-call | flops 3221225472 | bytes 6291456 | tf_op jit(solution)/shard_map/hidden/pallas_call | solution.py:211
  275.9 7.7 %collective-permute-done.49.refs_9_ = bf16[1408,128]{1,0:T(8,128)(2,1)S(1)} collective-permute-done((bf16[1408,128]{1,0:T(8,128)(2,1)}, bf16[1408,128]{1,0:T(8,128)(2,1)S(1)}, u32[]{:S(2)}, u32[]{:S(2)}) %collective-permute-start.49) | collective-permute-done | bytes 360480 | tf_op jit(solution)/shard_map/ppermute | solution.py:301
  283.6 6.2 %collective-permute-done.55.refs_15_ = bf16[1408,128]{1,0:T(8,128)(2,1)S(1)} collective-permute-done((bf16[1408,128]{1,0:T(8,128)(2,1)}, bf16[1408,128]{1,0:T(8,128)(2,1)S(1)}, u32[]{:S(2)}, u32[]{:S(2)}) %collective-permute-start.55) | collective-permute-done | bytes 360480 | tf_op jit(solution)/shard_map/ppermute | solution.py:301
  290.6 8.6 %down.1 = bf16[2,2,4,512,128]{4,3,2,1,0:T(8,128)(2,1)} custom-call(s32[3]{0:T(128)} %pad_add_fusion.info.refs_0_, bf16[512,768]{1,0:T(8,128)(2,1)} %hidden.2.refs_1_, bf16[512,640]{1,0:T(8,128)(2,1)} %hidden.3.refs_2_, bf16[1408,512]{1,0:T(8,128)(2,1)} %refs_3_.7, bf16[1408,128]{1,0:T(8,128)(2,1)} %copy-done.23, bf16[1408,128]{1,0:T(8,128)(2,1)} %copy-done.25, ...), custom_call_target="tpu_custom_call" | custom-call | flops 2952790016 | bytes 5767168 | tf_op jit(solution)/shard_map/down/pallas_call | solution.py:262
  313.4 5.3 %collective-permute-done.57 = bf16[4,512,128]{2,1,0:T(8,128)(2,1)} collective-permute-done((bf16[4,512,128]{2,1,0:T(8,128)(2,1)}, bf16[4,512,128]{2,1,0:T(8,128)(2,1)}, u32[]{:S(2)}, u32[]{:S(2)}) %collective-permute-start.57) | collective-permute-done | bytes 524320 | tf_op jit(solution)/shard_map/ppermute | solution.py:308
  321.4 5.9 %psum.7 = f32[512]{0:T(512)S(1)} all-reduce(f32[512]{0:T(512)S(1)} %get-tuple-element.5), channel_id=1, replica_groups=mesh['grp'=2,'fs'=4,'tp'=4] {'tp'}, use_global_device_ids=true, to_apply=%region_1.0 | all-reduce | flops 512 | bytes 4096 | tf_op jit(solution)/shard_map/psum | solution.py:350
  (198 shorter events, 110.6 us)
Async XLA Ops:
  1.4 21.6 %collective-permute-start.1 = (bf16[2,512,256]{2,1,0:T(8,128)(2,1)S(1)}, bf16[2,512,256]{2,1,0:T(8,128)(2,1)S(1)}, u32[]{:S(2)}, u32[]{:S(2)}) collective-permute-start(bf16[2,512,256]{2,1,0:T(8,128)(2,1)S(1)} %bitcast.54), channel_id=1, source_target_pairs={{0,2},{1,3},{2,0},{3,1},{4,6},{5,7},{6,4},{7,5},{8,10},{9,11},{10,... | collective-permute-start | bytes 1572872 | tf_op jit(solution)/shard_map/ppermute | solution.py:308
  8.2 27.6 %collective-permute-start = (bf16[2,512,256]{2,1,0:T(8,128)(2,1)S(1)}, bf16[2,512,256]{2,1,0:T(8,128)(2,1)S(1)}, u32[]{:S(2)}, u32[]{:S(2)}) collective-permute-start(bf16[2,512,256]{2,1,0:T(8,128)(2,1)S(1)} %bitcast.55), channel_id=1, source_target_pairs={{0,1},{1,0},{2,3},{3,2},{4,5},{5,4},{6,7},{7,6},{8,9},{9,8},{10,11... | collective-permute-start | bytes 1572872 | tf_op jit(solution)/shard_map/ppermute | solution.py:305
  22.9 21.2 %collective-permute-start.2 = (bf16[2,512,256]{2,1,0:T(8,128)(2,1)S(1)}, bf16[2,512,256]{2,1,0:T(8,128)(2,1)S(1)}, u32[]{:S(2)}, u32[]{:S(2)}) collective-permute-start(bf16[2,512,256]{2,1,0:T(8,128)(2,1)S(1)} %collective-permute-done.1.b2), channel_id=1, source_target_pairs={{0,1},{1,0},{2,3},{3,2},{4,5},{5,4},{6,7},{7,6},{8,9},{9,8},{10,11... | collective-permute-start | bytes 1572872 | tf_op jit(solution)/shard_map/ppermute | solution.py:305
  76.4 45.8 %collective-permute-start.20 = (bf16[256,768]{1,0:T(8,128)(2,1)S(1)}, bf16[256,768]{1,0:T(8,128)(2,1)}, u32[]{:S(2)}, u32[]{:S(2)}) collective-permute-start(bf16[256,768]{1,0:T(8,128)(2,1)S(1)} %constant_dynamic-slice_fusion.1), channel_id=1, source_target_pairs={{0,4},{4,8},{8,12},{12,0},{1,5},{5,9},{9,13},{13,1},{2,6},{6,10},{... | collective-permute-start | bytes 1179656 | tf_op jit(solution)/shard_map/ppermute | solution.py:299
  78.4 38.9 %collective-permute-start.44 = (bf16[1408,128]{1,0:T(8,128)(2,1)S(1)}, bf16[1408,128]{1,0:T(8,128)(2,1)S(1)}, u32[]{:S(2)}, u32[]{:S(2)}) collective-permute-start(bf16[1408,128]{1,0:T(8,128)(2,1)S(1)} %get-tuple-element.10), channel_id=1, source_target_pairs={{0,4},{4,8},{8,12},{12,0},{1,5},{5,9},{9,13},{13,1},{2,6},{6,10},{... | collective-permute-start | bytes 1081352 | tf_op jit(solution)/shard_map/ppermute | solution.py:299
  79.5 39.4 %collective-permute-start.50 = (bf16[1408,128]{1,0:T(8,128)(2,1)S(1)}, bf16[1408,128]{1,0:T(8,128)(2,1)S(1)}, u32[]{:S(2)}, u32[]{:S(2)}) collective-permute-start(bf16[1408,128]{1,0:T(8,128)(2,1)S(1)} %get-tuple-element.9), channel_id=1, source_target_pairs={{4,0},{8,4},{12,8},{0,12},{5,1},{9,5},{13,9},{1,13},{6,2},{10,6},{... | collective-permute-start | bytes 1081352 | tf_op jit(solution)/shard_map/ppermute | solution.py:299
  86.5 30.3 %collective-permute-start.38 = (bf16[256,640]{1,0:T(8,128)(2,1)S(1)}, bf16[256,640]{1,0:T(8,128)(2,1)S(1)}, u32[]{:S(2)}, u32[]{:S(2)}) collective-permute-start(bf16[256,640]{1,0:T(8,128)(2,1)S(1)} %dynamic-slice.3), channel_id=1, source_target_pairs={{4,0},{8,4},{12,8},{0,12},{5,1},{9,5},{13,9},{1,13},{6,2},{10,6},{... | collective-permute-start | bytes 983048 | tf_op jit(solution)/shard_map/ppermute | solution.py:299
  86.8 38.9 %collective-permute-start.26 = (bf16[256,768]{1,0:T(8,128)(2,1)S(1)}, bf16[256,768]{1,0:T(8,128)(2,1)S(1)}, u32[]{:S(2)}, u32[]{:S(2)}) collective-permute-start(bf16[256,768]{1,0:T(8,128)(2,1)S(1)} %constant_dynamic-slice_fusion), channel_id=1, source_target_pairs={{4,0},{8,4},{12,8},{0,12},{5,1},{9,5},{13,9},{1,13},{6,2},{10,6},{... | collective-permute-start | bytes 1179656 | tf_op jit(solution)/shard_map/ppermute | solution.py:299
  117.4 22.7 %collective-permute-start.35 = (bf16[256,640]{1,0:T(8,128)(2,1)}, bf16[256,640]{1,0:T(8,128)(2,1)S(1)}, u32[]{:S(2)}, u32[]{:S(2)}) collective-permute-start(bf16[256,640]{1,0:T(8,128)(2,1)} %collective-permute-done.32.refs_4_), channel_id=1, source_target_pairs={{0,16},{16,0},{1,17},{17,1},{2,18},{18,2},{3,19},{19,3},{4,20},{20... | collective-permute-start | bytes 983048 | tf_op jit(solution)/shard_map/ppermute | solution.py:301
  118.9 20.7 %collective-permute-start.39 = (bf16[256,640]{1,0:T(8,128)(2,1)S(1)}, bf16[256,640]{1,0:T(8,128)(2,1)S(1)}, u32[]{:S(2)}, u32[]{:S(2)}) collective-permute-start(bf16[256,640]{1,0:T(8,128)(2,1)S(1)} %collective-permute-done.38.refs_10_), channel_id=1, source_target_pairs={{4,0},{8,4},{12,8},{0,12},{5,1},{9,5},{13,9},{1,13},{6,2},{10,6},{... | collective-permute-start | bytes 983048 | tf_op jit(solution)/shard_map/ppermute | solution.py:299
  122.2 21.2 %collective-permute-start.41 = (bf16[256,640]{1,0:T(8,128)(2,1)S(1)}, bf16[256,640]{1,0:T(8,128)(2,1)S(1)}, u32[]{:S(2)}, u32[]{:S(2)}) collective-permute-start(bf16[256,640]{1,0:T(8,128)(2,1)S(1)} %collective-permute-done.38.refs_10_), channel_id=1, source_target_pairs={{0,16},{16,0},{1,17},{17,1},{2,18},{18,2},{3,19},{19,3},{4,20},{20... | collective-permute-start | bytes 983048 | tf_op jit(solution)/shard_map/ppermute | solution.py:301
  125.7 40.1 %collective-permute-start.16 = (bf16[2,512,256]{2,1,0:T(8,128)(2,1)S(1)}, bf16[2,512,256]{2,1,0:T(8,128)(2,1)S(1)}, u32[]{:S(2)}, u32[]{:S(2)}) collective-permute-start(bf16[2,512,256]{2,1,0:T(8,128)(2,1)S(1)} %fusion.5), channel_id=1, source_target_pairs={{0,2},{1,3},{2,0},{3,1},{4,6},{5,7},{6,4},{7,5},{8,10},{9,11},{10,... | collective-permute-start | bytes 1572872 | tf_op jit(solution)/shard_map/ppermute | solution.py:308
  139.6 25.7 %collective-permute-start.21 = (bf16[256,768]{1,0:T(8,128)(2,1)}, bf16[256,768]{1,0:T(8,128)(2,1)S(1)}, u32[]{:S(2)}, u32[]{:S(2)}) collective-permute-start(bf16[256,768]{1,0:T(8,128)(2,1)} %collective-permute-done.20.refs_4_), channel_id=1, source_target_pairs={{0,4},{4,8},{8,12},{12,0},{1,5},{5,9},{9,13},{13,1},{2,6},{6,10},{... | collective-permute-start | bytes 1179656 | tf_op jit(solution)/shard_map/ppermute | solution.py:299
  140.1 23.1 %collective-permute-start.51 = (bf16[1408,128]{1,0:T(8,128)(2,1)S(1)}, bf16[1408,128]{1,0:T(8,128)(2,1)S(1)}, u32[]{:S(2)}, u32[]{:S(2)}) collective-permute-start(bf16[1408,128]{1,0:T(8,128)(2,1)S(1)} %collective-permute-done.50.refs_10_), channel_id=1, source_target_pairs={{4,0},{8,4},{12,8},{0,12},{5,1},{9,5},{13,9},{1,13},{6,2},{10,6},{... | collective-permute-start | bytes 1081352 | tf_op jit(solution)/shard_map/ppermute | solution.py:299
  143.4 21.4 %collective-permute-start.47 = (bf16[1408,128]{1,0:T(8,128)(2,1)S(1)}, bf16[1408,128]{1,0:T(8,128)(2,1)}, u32[]{:S(2)}, u32[]{:S(2)}) collective-permute-start(bf16[1408,128]{1,0:T(8,128)(2,1)S(1)} %collective-permute-done.44.refs_4_), channel_id=1, source_target_pairs={{0,16},{16,0},{1,17},{17,1},{2,18},{18,2},{3,19},{19,3},{4,20},{20... | collective-permute-start | bytes 1081352 | tf_op jit(solution)/shard_map/ppermute | solution.py:301
  147.6 24.7 %collective-permute-start.27 = (bf16[256,768]{1,0:T(8,128)(2,1)S(1)}, bf16[256,768]{1,0:T(8,128)(2,1)}, u32[]{:S(2)}, u32[]{:S(2)}) collective-permute-start(bf16[256,768]{1,0:T(8,128)(2,1)S(1)} %collective-permute-done.26.refs_10_), channel_id=1, source_target_pairs={{4,0},{8,4},{12,8},{0,12},{5,1},{9,5},{13,9},{1,13},{6,2},{10,6},{... | collective-permute-start | bytes 1179656 | tf_op jit(solution)/shard_map/ppermute | solution.py:299
  164.8 19.1 %collective-permute-start.29 = (bf16[256,768]{1,0:T(8,128)(2,1)S(1)}, bf16[256,768]{1,0:T(8,128)(2,1)S(1)}, u32[]{:S(2)}, u32[]{:S(2)}) collective-permute-start(bf16[256,768]{1,0:T(8,128)(2,1)S(1)} %collective-permute-done.26.refs_10_), channel_id=1, source_target_pairs={{0,16},{16,0},{1,17},{17,1},{2,18},{18,2},{3,19},{19,3},{4,20},{20... | collective-permute-start | bytes 1179656 | tf_op jit(solution)/shard_map/ppermute | solution.py:301
  165.3 19.1 %collective-permute-start.34 = (bf16[256,640]{1,0:T(8,128)(2,1)S(1)}, bf16[256,640]{1,0:T(8,128)(2,1)}, u32[]{:S(2)}, u32[]{:S(2)}) collective-permute-start(bf16[256,640]{1,0:T(8,128)(2,1)S(1)} %collective-permute-done.33.refs_5_), channel_id=1, source_target_pairs={{0,4},{4,8},{8,12},{12,0},{1,5},{5,9},{9,13},{13,1},{2,6},{6,10},{... | collective-permute-start | bytes 983048 | tf_op jit(solution)/shard_map/ppermute | solution.py:299
  165.9 21.9 %collective-permute-start.40 = (bf16[256,640]{1,0:T(8,128)(2,1)S(1)}, bf16[256,640]{1,0:T(8,128)(2,1)}, u32[]{:S(2)}, u32[]{:S(2)}) collective-permute-start(bf16[256,640]{1,0:T(8,128)(2,1)S(1)} %collective-permute-done.39.refs_11_), channel_id=1, source_target_pairs={{4,0},{8,4},{12,8},{0,12},{5,1},{9,5},{13,9},{1,13},{6,2},{10,6},{... | collective-permute-start | bytes 983048 | tf_op jit(solution)/shard_map/ppermute | solution.py:299
  184.4 19.4 %collective-permute-start.52 = (bf16[1408,128]{1,0:T(8,128)(2,1)S(1)}, bf16[1408,128]{1,0:T(8,128)(2,1)}, u32[]{:S(2)}, u32[]{:S(2)}) collective-permute-start(bf16[1408,128]{1,0:T(8,128)(2,1)S(1)} %collective-permute-done.51.refs_11_), channel_id=1, source_target_pairs={{4,0},{8,4},{12,8},{0,12},{5,1},{9,5},{13,9},{1,13},{6,2},{10,6},{... | collective-permute-start | bytes 1081352 | tf_op jit(solution)/shard_map/ppermute | solution.py:299
  191.0 29.1 %collective-permute-start.17 = (bf16[2,512,256]{2,1,0:T(8,128)(2,1)S(1)}, bf16[2,512,256]{2,1,0:T(8,128)(2,1)S(1)}, u32[]{:S(2)}, u32[]{:S(2)}) collective-permute-start(bf16[2,512,256]{2,1,0:T(8,128)(2,1)S(1)} %get-tuple-element.8.b0), channel_id=1, source_target_pairs={{0,1},{1,0},{2,3},{3,2},{4,5},{5,4},{6,7},{7,6},{8,9},{9,8},{10,11... | collective-permute-start | bytes 1572872 | tf_op jit(solution)/shard_map/ppermute | solution.py:305
  191.0 30.6 %collective-permute-start.19 = (bf16[2,512,256]{2,1,0:T(8,128)(2,1)S(1)}, bf16[2,512,256]{2,1,0:T(8,128)(2,1)S(1)}, u32[]{:S(2)}, u32[]{:S(2)}) collective-permute-start(bf16[2,512,256]{2,1,0:T(8,128)(2,1)S(1)} %collective-permute-done.18.b2), channel_id=1, source_target_pairs={{0,1},{1,0},{2,3},{3,2},{4,5},{5,4},{6,7},{7,6},{8,9},{9,8},{10,11... | collective-permute-start | bytes 1572872 | tf_op jit(solution)/shard_map/ppermute | solution.py:305
  197.4 20.6 %collective-permute-start.28 = (bf16[256,768]{1,0:T(8,128)(2,1)}, bf16[256,768]{1,0:T(8,128)(2,1)}, u32[]{:S(2)}, u32[]{:S(2)}) collective-permute-start(bf16[256,768]{1,0:T(8,128)(2,1)} %collective-permute-done.27.refs_11_), channel_id=1, source_target_pairs={{4,0},{8,4},{12,8},{0,12},{5,1},{9,5},{13,9},{1,13},{6,2},{10,6},{... | collective-permute-start | bytes 1179656 | tf_op jit(solution)/shard_map/ppermute | solution.py:299
  218.0 36.3 %collective-permute-start.25 = (bf16[256,768]{1,0:T(8,128)(2,1)}, bf16[256,768]{1,0:T(8,128)(2,1)}, u32[]{:S(2)}, u32[]{:S(2)}) collective-permute-start(bf16[256,768]{1,0:T(8,128)(2,1)} %collective-permute-done.22.refs_6_), channel_id=1, source_target_pairs={{0,16},{16,0},{1,17},{17,1},{2,18},{18,2},{3,19},{19,3},{4,20},{20... | collective-permute-start | bytes 1179656 | tf_op jit(solution)/shard_map/ppermute | solution.py:301
  219.6 35.3 %collective-permute-start.31 = (bf16[256,768]{1,0:T(8,128)(2,1)}, bf16[256,768]{1,0:T(8,128)(2,1)}, u32[]{:S(2)}, u32[]{:S(2)}) collective-permute-start(bf16[256,768]{1,0:T(8,128)(2,1)} %collective-permute-done.28.refs_12_), channel_id=1, source_target_pairs={{0,16},{16,0},{1,17},{17,1},{2,18},{18,2},{3,19},{19,3},{4,20},{20... | collective-permute-start | bytes 1179656 | tf_op jit(solution)/shard_map/ppermute | solution.py:301
  220.1 25.7 %collective-permute-start.37 = (bf16[256,640]{1,0:T(8,128)(2,1)}, bf16[256,640]{1,0:T(8,128)(2,1)}, u32[]{:S(2)}, u32[]{:S(2)}) collective-permute-start(bf16[256,640]{1,0:T(8,128)(2,1)} %collective-permute-done.34.refs_6_), channel_id=1, source_target_pairs={{0,16},{16,0},{1,17},{17,1},{2,18},{18,2},{3,19},{19,3},{4,20},{20... | collective-permute-start | bytes 983048 | tf_op jit(solution)/shard_map/ppermute | solution.py:301
  221.6 31.2 %collective-permute-start.43 = (bf16[256,640]{1,0:T(8,128)(2,1)}, bf16[256,640]{1,0:T(8,128)(2,1)}, u32[]{:S(2)}, u32[]{:S(2)}) collective-permute-start(bf16[256,640]{1,0:T(8,128)(2,1)} %collective-permute-done.40.refs_12_), channel_id=1, source_target_pairs={{0,16},{16,0},{1,17},{17,1},{2,18},{18,2},{3,19},{19,3},{4,20},{20... | collective-permute-start | bytes 983048 | tf_op jit(solution)/shard_map/ppermute | solution.py:301
  227.5 45.7 %collective-permute-start.53 = (bf16[1408,128]{1,0:T(8,128)(2,1)}, bf16[1408,128]{1,0:T(8,128)(2,1)S(1)}, u32[]{:S(2)}, u32[]{:S(2)}) collective-permute-start(bf16[1408,128]{1,0:T(8,128)(2,1)} %copy-done.24), channel_id=1, source_target_pairs={{0,16},{16,0},{1,17},{17,1},{2,18},{18,2},{3,19},{19,3},{4,20},{20... | collective-permute-start | bytes 1081352 | tf_op jit(solution)/shard_map/ppermute | solution.py:301
  245.8 27.5 %collective-permute-start.48 = (bf16[1408,128]{1,0:T(8,128)(2,1)}, bf16[1408,128]{1,0:T(8,128)(2,1)S(1)}, u32[]{:S(2)}, u32[]{:S(2)}) collective-permute-start(bf16[1408,128]{1,0:T(8,128)(2,1)} %copy-done.25), channel_id=1, source_target_pairs={{0,16},{16,0},{1,17},{17,1},{2,18},{18,2},{3,19},{19,3},{4,20},{20... | collective-permute-start | bytes 1081352 | tf_op jit(solution)/shard_map/ppermute | solution.py:301
  252.8 23.1 %collective-permute-start.54 = (bf16[1408,128]{1,0:T(8,128)(2,1)}, bf16[1408,128]{1,0:T(8,128)(2,1)S(1)}, u32[]{:S(2)}, u32[]{:S(2)}) collective-permute-start(bf16[1408,128]{1,0:T(8,128)(2,1)} %copy-done.26), channel_id=1, source_target_pairs={{0,16},{16,0},{1,17},{17,1},{2,18},{18,2},{3,19},{19,3},{4,20},{20... | collective-permute-start | bytes 1081352 | tf_op jit(solution)/shard_map/ppermute | solution.py:301
  254.3 29.3 %collective-permute-start.49 = (bf16[1408,128]{1,0:T(8,128)(2,1)}, bf16[1408,128]{1,0:T(8,128)(2,1)S(1)}, u32[]{:S(2)}, u32[]{:S(2)}) collective-permute-start(bf16[1408,128]{1,0:T(8,128)(2,1)} %copy-done.27), channel_id=1, source_target_pairs={{0,16},{16,0},{1,17},{17,1},{2,18},{18,2},{3,19},{19,3},{4,20},{20... | collective-permute-start | bytes 1081352 | tf_op jit(solution)/shard_map/ppermute | solution.py:301
  254.9 34.9 %collective-permute-start.55 = (bf16[1408,128]{1,0:T(8,128)(2,1)}, bf16[1408,128]{1,0:T(8,128)(2,1)S(1)}, u32[]{:S(2)}, u32[]{:S(2)}) collective-permute-start(bf16[1408,128]{1,0:T(8,128)(2,1)} %collective-permute-done.52.refs_12_), channel_id=1, source_target_pairs={{0,16},{16,0},{1,17},{17,1},{2,18},{18,2},{3,19},{19,3},{4,20},{20... | collective-permute-start | bytes 1081352 | tf_op jit(solution)/shard_map/ppermute | solution.py:301
  (65 other events, 1555.7 us)

commit v2 on v1

v2 whole, which is shorter than its diff:
```python
import functools

import jax
import jax.numpy as jnp
from jax import lax
from jax.experimental import pallas as pl
from jax.experimental.pallas import tpu as pltpu
from jax.sharding import PartitionSpec as P


BF16 = jnp.bfloat16
F32 = jnp.float32
VMEM_LIMIT = 56 * 1024 * 1024


def rms_norm(values, gain):
    floats = values.astype(F32)
    scaled = floats * lax.rsqrt(jnp.mean(floats * floats, axis=-1, keepdims=True) + 1e-06)
    return (scaled * gain).astype(BF16)


def plain_local(
    tokens, mix_gain, gate_outer, gate_inner, value_weight, conv_taps, mix_out,
    ffn_gain, ffn_gate, ffn_up, ffn_down, out_gain,
):
    seq_count, length, columns = tokens.shape
    row_count = seq_count * length
    width = columns * lax.axis_size("tp")
    whole = lax.all_gather(tokens, "tp", axis=2, tiled=True).reshape(row_count, width)
    normed = rms_norm(whole, mix_gain)
    channels = gate_outer.shape[1]

    def project(left, weight):
        full = lax.all_gather(weight, "fs", axis=0, tiled=True)
        return jnp.dot(left, full, preferred_element_type=F32)

    outer = project(normed, gate_outer).astype(BF16)
    inner = project(normed, gate_inner).astype(BF16)
    values = project(normed, value_weight).astype(BF16)
    product = (inner.astype(F32) * values.astype(F32)).reshape(seq_count, length, channels)
    own_taps = lax.dynamic_slice_in_dim(conv_taps, lax.axis_index("tp") * channels, channels, 1)
    tap_count = conv_taps.shape[0]
    padded = jnp.pad(product, ((0, 0), (tap_count - 1, 0), (0, 0)))
    conv = jnp.zeros((seq_count, length, channels), F32)
    for offset in range(tap_count):
        conv = conv + own_taps[offset] * padded[:, offset : offset + length]
    gated = (outer.astype(F32) * conv.reshape(row_count, channels)).astype(BF16)
    mix_terms = jnp.dot(
        gated, lax.all_gather(mix_out, "fs", axis=1, tiled=True), preferred_element_type=F32
    )
    mix_full = lax.psum(mix_terms.astype(BF16), "tp").astype(F32)
    first_full = (whole.astype(F32) + mix_full).astype(BF16)
    first = lax.dynamic_slice_in_dim(first_full, lax.axis_index("tp") * columns, columns, 1)
    normed_ffn = rms_norm(first_full, ffn_gain)
    gate = project(normed_ffn, ffn_gate)
    upward = project(normed_ffn, ffn_up)
    hidden = (jax.nn.silu(gate) * upward).astype(BF16)
    down_terms = jnp.dot(
        hidden, lax.all_gather(ffn_down, "fs", axis=1, tiled=True), preferred_element_type=F32
    )
    down_summed = lax.psum_scatter(
        down_terms.astype(BF16), "tp", scatter_dimension=1, tiled=True
    ).astype(F32)
    second = first.astype(F32) + down_summed
    squares = lax.psum(jnp.sum(second * second, axis=1), "tp")
    factor = lax.rsqrt(squares / width + 1e-06)
    own_gain = lax.dynamic_slice_in_dim(out_gain, lax.axis_index("tp") * columns, columns, 0)
    result = second * factor[:, None] * own_gain
    return result.astype(BF16).reshape(seq_count, length, columns)


def dot(left, right):
    return jnp.dot(left, right, preferred_element_type=F32)


def norm_kernel(info, gain, b0, b1, b2, b3, out, *, width):
    q = info[2]
    blocks = [(b, h) for b in (b0, b1, b2, b3) for h in range(2)]
    squares = None
    for b, h in blocks:
        value = b[h].astype(F32)
        squares = value * value if squares is None else squares + value * value
    factor = lax.rsqrt(jnp.sum(squares, axis=-1, keepdims=True) / width + 1e-06)
    for i, (b, h) in enumerate(blocks):
        own = gain[(q ^ (i // 2)) * 2 + h]
        out[i] = (b[h].astype(F32) * factor * own).astype(BF16)


def call(kernel, info, operands, outs, flops):
    in_vmem = pl.BlockSpec(memory_space=pltpu.VMEM)
    moved = 2 * sum(o.size for o in operands)
    return pl.pallas_call(
        kernel,
        in_specs=[pl.BlockSpec(memory_space=pltpu.SMEM)] + [in_vmem] * len(operands),
        out_specs=[in_vmem] * len(outs),
        out_shape=[jax.ShapeDtypeStruct(shape, BF16) for shape in outs],
        cost_estimate=pl.CostEstimate(flops=flops, bytes_accessed=moved, transcendentals=0),
        compiler_params=pltpu.CompilerParams(vmem_limit_bytes=VMEM_LIMIT),
    )(info, *operands)


def norm_call(info, gain, blocks):
    _, rows, half = blocks[0].shape
    width = 8 * half
    kernel = functools.partial(norm_kernel, width=width)
    operands = [gain.reshape(8, 1, half), *blocks]
    return call(kernel, info, operands, [(8, rows, half)], 4000000)[0]


def place(info, step, direction, count):
    z, q = info[0], info[2]
    shard = lax.rem(z + (count - step if direction > 0 else step), count)
    return shard ^ q


def gathered(x, info, pieces, direction, count):
    g = info[1]
    spot = place(info, 0, direction, count)
    parts = [x[2 * spot], x[2 * spot + 1]]
    for step, swapped, _ in pieces:
        spot = place(info, step, direction, count)
        parts.append(x[2 * spot + (1 - g if swapped else g)])
    return jnp.concatenate(parts, axis=1)


def stacked(own, pieces, row, half, columns):
    rows = [own[:, columns]] + [piece[row : row + half, :] for _, _, piece in pieces]
    return jnp.concatenate(rows, axis=0)


def sort_out(keep, give, spot, part, value):
    value = value.astype(BF16)

    @pl.when(lax.rem(spot, 2) == 0)
    def _():
        keep[spot // 2, part] = value

    @pl.when(lax.rem(spot, 2) == 1)
    def _():
        give[spot // 2, part] = value


def mixer_kernel(*refs, count, length):
    info, taps, x, outer_own, inner_own, value_own, mix_own = refs[:7]
    steps = count - 1
    ahead, ahead_y = refs[7 : 7 + steps], refs[7 + steps : 7 + 2 * steps]
    back, back_y = refs[7 + 2 * steps : 7 + 3 * steps], refs[7 + 3 * steps : 7 + 4 * steps]
    keep, give = refs[-2:]
    half = x.shape[2]
    everything = slice(None)
    g = info[1]
    cw = [(k + 1, s, p) for s, group in ((False, ahead), (True, ahead_y)) for k, p in enumerate(group)]
    ccw = [(k + 1, s, p) for s, group in ((False, back), (True, back_y)) for k, p in enumerate(group)]
    left = gathered(x, info, cw, 1, count)
    inner = dot(left, stacked(inner_own, cw, 0, half, everything)).astype(BF16)
    values = dot(left, stacked(value_own, cw, half, half, everything)).astype(BF16)
    left = gathered(x, info, ccw, -1, count)
    outer = dot(left, stacked(outer_own, ccw, 0, half, everything)).astype(BF16)
    product = inner.astype(F32) * values.astype(F32)
    position = lax.broadcasted_iota(jnp.int32, product.shape, 0) % length
    tap_count = taps.shape[0]
    conv = jnp.zeros(product.shape, F32)
    channels = product.shape[1]
    own_taps = taps[:, pl.ds(pl.multiple_of(info[2] * channels, 128), channels)]
    for offset in range(tap_count):
        back_by = tap_count - 1 - offset
        if back_by:
            moved = pltpu.roll(product, back_by, axis=0)
            moved = jnp.where(position >= back_by, moved, 0.0)
        else:
            moved = product
        conv = conv + own_taps[offset][None, :] * moved
    gated = (outer.astype(F32) * conv).astype(BF16)

    own = dot(gated, mix_own[...])
    for h in range(2):
        sort_out(keep, give, place(info, 0, -1, count), h, own[:, h * half : (h + 1) * half])
    for step, swapped, piece in ccw:
        spot = place(info, step, -1, count)
        sort_out(keep, give, spot, 1 - g if swapped else g, dot(gated, piece[half:, :]))


def mixer_call(info, taps, x, owns, cw, cw_y, ccw, ccw_y, count, length):
    _, rows, half = x.shape
    kernel = functools.partial(mixer_kernel, count=count, length=length)
    operands = [taps, x, *owns, *cw, *cw_y, *ccw, *ccw_y]
    flops = 8 * rows * 8 * half * owns[0].shape[1]
    return call(kernel, info, operands, [(2, 2, rows, half)] * 2, flops)


def hidden_kernel(*refs, count, start, size):
    info, x, gate_own, up_own = refs[:4]
    steps = count - 1
    groups = [refs[4 + i * steps : 4 + (i + 1) * steps] for i in range(4)]
    out = refs[-1]
    columns = slice(start, start + size)
    cw = [(k + 1, i == 1, p) for i in (0, 1) for k, p in enumerate(groups[i])]
    ccw = [(k + 1, i == 3, p) for i in (2, 3) for k, p in enumerate(groups[i])]
    half = x.shape[2]
    gate = dot(gathered(x, info, cw, 1, count), stacked(gate_own, cw, 0, half, columns))
    upward = dot(gathered(x, info, ccw, -1, count), stacked(up_own, ccw, 0, half, columns))
    out[...] = (gate / (1.0 + jnp.exp(-gate)) * upward).astype(BF16)


def hidden_call(info, x, gate_own, up_own, cw, cw_y, ccw, ccw_y, count, start, size):
    _, rows, half = x.shape
    kernel = functools.partial(hidden_kernel, count=count, start=start, size=size)
    operands = [x, gate_own, up_own, *cw, *cw_y, *ccw, *ccw_y]
    return call(kernel, info, operands, [(rows, size)], 4 * rows * 8 * half * size)[0]


def down_early_kernel(*refs, count, split):
    info, left, right, own = refs[:4]
    steps = count - 2
    groups = [refs[4 + i * steps : 4 + (i + 1) * steps] for i in range(4)]
    keep, give = refs[-2:]
    g = info[1]
    rows, piece = keep.shape[-2:]

    def product(weight):
        return dot(left[...], weight[:split]) + dot(right[...], weight[split:])

    def store(step, direction, part, value):
        sort_out(keep, give, place(info, step, direction, count), part, value)

    value = product(own[...])
    for i in range(4):
        store(0, 1, i, value[:, i * piece : (i + 1) * piece])
    for direction, last, mine, other in ((1, 0, groups[0], groups[1]), (-1, 1, groups[2], groups[3])):
        value = product(jnp.concatenate([p[...] for k in range(steps) for p in (mine[k], other[k])], axis=1))
        for k in range(steps):
            at = 2 * k * piece
            store(k + 1, direction, 2 * g + last, value[:, at : at + piece])
            store(k + 1, direction, 2 * (1 - g) + last, value[:, at + piece : at + 2 * piece])
        for i in range(2):
            store(count - 1, direction, 2 * i + last, jnp.zeros((rows, piece), F32))


def down_late_kernel(info, left, right, cw, cw_y, ccw, ccw_y, out, *, count, split):
    g = info[1]
    piece = out.shape[-1]
    for direction, mine, other in ((1, cw, cw_y), (-1, ccw, ccw_y)):
        weight = jnp.concatenate([mine[...], other[...]], axis=1)
        value = dot(left[...], weight[:split]) + dot(right[...], weight[split:])
        spot = place(info, count - 1, direction, count) // 2
        out[spot, g] = value[:, :piece].astype(BF16)
        out[spot, 1 - g] = value[:, piece:].astype(BF16)


def ring_local(
    tokens, mix_gain, gate_outer, gate_inner, value_weight, conv_taps, mix_out,
    ffn_gain, ffn_gate, ffn_up, ffn_down, out_gain,
):
    count = lax.axis_size("fs")
    seq_count, length, columns = tokens.shape
    rows = seq_count * length
    half = columns // 2
    width = columns * lax.axis_size("tp")
    z, g, q = lax.axis_index("fs"), lax.axis_index("grp"), lax.axis_index("tp")
    info = jnp.stack([z, g, q]).astype(jnp.int32)

    ahead = [(i, (i + 1) % count) for i in range(count)]
    behind = [(d, s) for s, d in ahead]

    def ring(value, pairs):
        arrived, swapped = [], []
        for _ in range(1, count):
            value = lax.ppermute(value, "fs", pairs)
            arrived.append(value)
            swapped.append(lax.ppermute(value, "grp", [(0, 1), (1, 0)]))
        return arrived, swapped

    def mate(value):
        return lax.ppermute(value, "tp", [(i, i ^ 1) for i in range(4)])

    def across(value):
        return lax.ppermute(value, "tp", [(i, i ^ 2) for i in range(4)])

    def gather(own):
        other = across(own)
        return own, mate(own), other, mate(other)

    def rows_of(weight):
        return lax.dynamic_slice_in_dim(weight, g * half, half, 0)

    own_tokens = tokens.reshape(rows, 2, half).transpose(1, 0, 2)
    blocks = gather(own_tokens)

    mix_half = lax.dynamic_slice_in_dim(mix_out, g * half, half, 1)
    m_cw = ring(jnp.concatenate([rows_of(gate_inner), rows_of(value_weight)]), ahead)
    m_ccw = ring(jnp.concatenate([rows_of(gate_outer), mix_half]), behind)
    units = ffn_gate.shape[1]
    split = -(-units // 256) * 128
    gate_half, up_half = rows_of(ffn_gate), rows_of(ffn_up)
    g1 = ring(gate_half[:, :split], ahead)
    u1 = ring(up_half[:, :split], behind)
    g2 = ring(gate_half[:, split:], ahead)
    u2 = ring(up_half[:, split:], behind)
    down_half = lax.dynamic_slice_in_dim(ffn_down, g * half, half, 1)
    d_cw = ring(down_half[:, : half // 2], ahead)
    d_ccw = ring(down_half[:, half // 2 :], behind)

    def scatter(partial):
        met = partial[0].astype(F32) + mate(partial[1]).astype(F32)
        return met[0] + across(met[1].astype(BF16)).astype(F32)

    x = norm_call(info, mix_gain, blocks)
    owns = (gate_outer, gate_inner, value_weight, mix_out)
    partial = mixer_call(info, conv_taps, x, owns, *m_cw, *m_ccw, count, length)
    first = (own_tokens.astype(F32) + scatter(partial)).astype(BF16)
    blocks = gather(first)
    x = norm_call(info, ffn_gain, blocks)
    left = hidden_call(info, x, ffn_gate, ffn_up, *g1, *u1, count, 0, split)
    right = hidden_call(info, x, ffn_gate, ffn_up, *g2, *u2, count, split, units - split)
    flops = 2 * rows * units * width
    early = [left, right, ffn_down, *[p for ring_part in (*d_cw, *d_ccw) for p in ring_part[:-1]]]
    late = [left, right, *[ring_part[-1] for ring_part in (*d_cw, *d_ccw)]]
    split_by = {"count": count, "split": split}
    piece = (rows, half // 2)
    kernel = functools.partial(down_early_kernel, **split_by)
    partial = call(kernel, info, early, [(2, 4, *piece)] * 2, flops * 3 // 4)
    second = first.reshape(2, rows, 2, half // 2).transpose(0, 2, 1, 3).reshape(4, rows, half // 2)
    second = second.astype(F32) + scatter(partial)
    kernel = functools.partial(down_late_kernel, **split_by)
    rest = call(kernel, info, late, [(2, 2, *piece)], flops // 4)[0]

    takers = [[(s + 1) % 2 == i % 2 for i in range(4)] for s in range(count)]
    to_mate = [(4 * s + i, 4 * s + (i ^ 1)) for s in range(count) for i in range(4) if not takers[s][i]]
    to_other = [(4 * s + i, 4 * s + (i ^ 2)) for s in range(count) for i in range(4) if takers[s][i]]
    met = rest.astype(F32) + lax.ppermute(rest, ("fs", "tp"), to_mate).astype(F32)
    met = met[0] + lax.ppermute(met[1].astype(BF16), ("fs", "tp"), to_other).astype(F32)
    takes = lax.rem(z + 1 + q, 2) == 0
    parity = jnp.where(q == lax.rem(z + 1, count), 0, 1)
    mask = takes & (jnp.arange(2) == parity)
    late_part = jnp.where(mask[None, :, None, None], met[:, None], 0.0).reshape(second.shape)
    second = second + late_part
    squares = lax.psum(jnp.sum(second * second, axis=(0, 2)), "tp")
    factor = lax.rsqrt(squares / width + 1e-06)
    own_gain = lax.dynamic_slice_in_dim(out_gain, q * columns, columns, 0).reshape(4, 1, half // 2)
    result = (second * factor[None, :, None] * own_gain).astype(BF16)
    return result.transpose(1, 0, 2).reshape(seq_count, length, columns)


def fits_ring(mesh):
    shape = mesh.shape
    return shape["grp"] == 2 and shape["tp"] == 4 and shape["fs"] == 4


def solution(mesh):
    in_specs = (
        P(("grp", "fs"), None, "tp"),
        P(),
        P("fs", "tp"),
        P("fs", "tp"),
        P("fs", "tp"),
        P(),
        P("tp", "fs"),
        P(),
        P("fs", "tp"),
        P("fs", "tp"),
        P("tp", "fs"),
        P(),
    )
    out_specs = P(("grp", "fs"), None, "tp")
    ring = fits_ring(mesh)
    body = ring_local if ring else plain_local

    return jax.shard_map(body, mesh=mesh, in_specs=in_specs, out_specs=out_specs, check_vma=False)
```

time: 329 us -> 328 us (level)
  waiting for transfers between devices: 173 us -> 192 us
  starting transfers between devices: 77.9 us -> 67.7 us
  local copies, waits for them, and re-layouts: 22 us -> 11.9 us
    ppermute x24, waiting for transfers between devices: 98 us -> 129 us  [ring(): value = lax.ppermute(value, 'fs', pairs)]
    ppermute x24, waiting for transfers between devices: 67.2 us -> 47.5 us  [ring(): swapped.append(lax.ppermute(value, 'grp', [(0, 1), (1, 0)]))]
    ppermute x24, starting transfers between devices: 43 us -> 27.5 us  [ring(): value = lax.ppermute(value, 'fs', pairs)]
    ppermute x4, waiting for transfers between devices: 5.28 us -> 13.8 us  [across(): return lax.ppermute(value, 'tp', [(i, i ^ 2) for i in range(4)])]
    convert_element_type x4 -> x1, local copies, waits for them, and re-layouts: 7.71 us -> 0.04 us  [ring_local(): met[1].astype(BF16)]
    squeeze x2 -> x0, local copies, waits for them, and re-layouts: 3.75 us -> none  [scatter(): met = partial[0].astype(F32) + mate(partial[1]).astype(F32)]
    pallas_call x6 -> x7, Pallas kernels: 43.8 us -> 43.2 us  [call(): pl.pallas_call(kernel, in_specs=[pl.BlockSpec(memory_space=pltpu.SMEM)] +...]
  transfers between devices with their start and end apart: 58 -> 60, of which waited for: 31 -> 35; matrix products, arithmetic and copies ran while one was open for 5% -> 3% of each run, Pallas kernels for 8% -> 11%
where the time goes in v2:
time: 328 us; the launch traced here: 327 us
  waiting for transfers between devices  192 us (59%)
  starting transfers between devices  67.7 us (21%)
  Pallas kernels  43.2 us (13%)
  local copies, waits for them, and re-layouts  11.9 us (4%)
  blocking collectives  6.49 us (2%)
  other arithmetic  5.82 us (2%)
    ppermute x24, waiting for transfers between devices, ring(): value = lax.ppermute(value, 'fs', pairs)  129 us
    ppermute x24, waiting for transfers between devices, ring(): swapped.append(lax.ppermute(value, 'grp', [(0, 1), (1, 0)]))  47.5 us
    pallas_call x7, Pallas kernels, call(): pl.pallas_call(kernel, in_specs=[pl.BlockSpec(memory_space=pltpu.SMEM)] +...  43.2 us
    ppermute x24, starting transfers between devices, ring(): swapped.append(lax.ppermute(value, 'grp', [(0, 1), (1, 0)]))  32.2 us
    ppermute x24, starting transfers between devices, ring(): value = lax.ppermute(value, 'fs', pairs)  27.5 us
    ppermute x4, waiting for transfers between devices, across(): return lax.ppermute(value, 'tp', [(i, i ^ 2) for i in range(4)])  13.8 us
  transfers between devices with their start and end apart: 60, of which 35 were waited for; matrix products, arithmetic and copies ran while one was open for 3% of the time, Pallas kernels for 11%

profile of v2, /device:TPU:0, one launch (start us, length us, event | category | flops | bytes accessed | tf_op | source)
XLA Modules:
  0.0 327.2 jit_solution(6249980288874534220)
XLA Ops:
  8.5 7.1 %collective-permute-done.3.refs_7_ = bf16[512,256]{1,0:T(8,128)(2,1)S(1)} collective-permute-done((bf16[512,256]{1,0:T(8,128)(2,1)S(1)}, bf16[512,256]{1,0:T(8,128)(2,1)S(1)}, u32[]{:S(2)}, u32[]{:S(2)}) %collective-permute-start.3) | collective-permute-done | bytes 262176 | tf_op jit(solution)/shard_map/ppermute | solution.py:268
  15.6 4.6 %collective-permute-done.9.refs_13_ = bf16[512,256]{1,0:T(8,128)(2,1)S(1)} collective-permute-done((bf16[512,256]{1,0:T(8,128)(2,1)S(1)}, bf16[512,256]{1,0:T(8,128)(2,1)S(1)}, u32[]{:S(2)}, u32[]{:S(2)}) %collective-permute-start.9) | collective-permute-done | bytes 262176 | tf_op jit(solution)/shard_map/ppermute | solution.py:268
  27.7 5.6 %collective-permute-done.10.refs_14_ = bf16[512,256]{1,0:T(8,128)(2,1)} collective-permute-done((bf16[512,256]{1,0:T(8,128)(2,1)S(1)}, bf16[512,256]{1,0:T(8,128)(2,1)}, u32[]{:S(2)}, u32[]{:S(2)}) %collective-permute-start.10) | collective-permute-done | bytes 262176 | tf_op jit(solution)/shard_map/ppermute | solution.py:268
  49.9 4.7 %collective-permute-done.13.refs_17_ = bf16[512,256]{1,0:T(8,128)(2,1)} collective-permute-done((bf16[512,256]{1,0:T(8,128)(2,1)}, bf16[512,256]{1,0:T(8,128)(2,1)}, u32[]{:S(2)}, u32[]{:S(2)}) %collective-permute-start.13) | collective-permute-done | bytes 262176 | tf_op jit(solution)/shard_map/ppermute | solution.py:270
  54.7 5.6 %collective-permute-done.8.refs_12_ = bf16[512,256]{1,0:T(8,128)(2,1)} collective-permute-done((bf16[512,256]{1,0:T(8,128)(2,1)}, bf16[512,256]{1,0:T(8,128)(2,1)}, u32[]{:S(2)}, u32[]{:S(2)}) %collective-permute-start.8) | collective-permute-done | bytes 262176 | tf_op jit(solution)/shard_map/ppermute | solution.py:270
  63.7 8.7 %shard_map.119 = (bf16[2,2,512,256]{3,2,1,0:T(8,128)(2,1)}, bf16[2,2,512,256]{3,2,1,0:T(8,128)(2,1)}) custom-call(s32[3]{0:T(128)} %pad_add_fusion.info.refs_0_, f32[3,1024]{1,0:T(4,128)} %refs_1_.1, bf16[8,512,256]{2,1,0:T(8,128)(2,1)} %shard_map.118.refs_2_, bf16[512,256]{1,0:T(8,128)(2,1)} %refs_3_.4, bf16[512,256]{1,0:T(8,128)(2,1)} %refs_4_.1, ...), custom_call_target="tpu_custom_call" | custom-call | flops 2147483648 | bytes 6297600 | tf_op jit(solution)/shard_map/pallas_call | solution.py:92
  86.2 7.1 %collective-permute-done.38.refs_10_ = bf16[256,640]{1,0:T(8,128)(2,1)} collective-permute-done((bf16[256,640]{1,0:T(8,128)(2,1)S(1)}, bf16[256,640]{1,0:T(8,128)(2,1)}, u32[]{:S(2)}, u32[]{:S(2)}) %collective-permute-start.38) | collective-permute-done | bytes 327712 | tf_op jit(solution)/shard_map/ppermute | solution.py:268
  94.8 6.0 %collective-permute-done.44.refs_4_ = bf16[1408,128]{1,0:T(8,128)(2,1)S(1)} collective-permute-done((bf16[1408,128]{1,0:T(8,128)(2,1)S(1)}, bf16[1408,128]{1,0:T(8,128)(2,1)S(1)}, u32[]{:S(2)}, u32[]{:S(2)}) %collective-permute-start.44) | collective-permute-done | bytes 360480 | tf_op jit(solution)/shard_map/ppermute | solution.py:268
  100.8 7.7 %collective-permute-done.48.refs_8_ = bf16[1408,128]{1,0:T(8,128)(2,1)S(1)} collective-permute-done((bf16[1408,128]{1,0:T(8,128)(2,1)S(1)}, bf16[1408,128]{1,0:T(8,128)(2,1)S(1)}, u32[]{:S(2)}, u32[]{:S(2)}) %collective-permute-start.48) | collective-permute-done | bytes 360480 | tf_op jit(solution)/shard_map/ppermute | solution.py:268
  112.1 5.0 %collective-permute-done.20.refs_4_ = bf16[256,768]{1,0:T(8,128)(2,1)S(1)} collective-permute-done((bf16[256,768]{1,0:T(8,128)(2,1)S(1)}, bf16[256,768]{1,0:T(8,128)(2,1)S(1)}, u32[]{:S(2)}, u32[]{:S(2)}) %collective-permute-start.20) | collective-permute-done | bytes 393248 | tf_op jit(solution)/shard_map/ppermute | solution.py:268
  118.6 6.8 %collective-permute-done.26.refs_10_ = bf16[256,768]{1,0:T(8,128)(2,1)S(1)} collective-permute-done((bf16[256,768]{1,0:T(8,128)(2,1)S(1)}, bf16[256,768]{1,0:T(8,128)(2,1)S(1)}, u32[]{:S(2)}, u32[]{:S(2)}) %collective-permute-start.26) | collective-permute-done | bytes 393248 | tf_op jit(solution)/shard_map/ppermute | solution.py:268
  125.9 6.6 %collective-permute-done.33.refs_5_ = bf16[256,640]{1,0:T(8,128)(2,1)S(1)} collective-permute-done((bf16[256,640]{1,0:T(8,128)(2,1)}, bf16[256,640]{1,0:T(8,128)(2,1)S(1)}, u32[]{:S(2)}, u32[]{:S(2)}) %collective-permute-start.33) | collective-permute-done | bytes 327712 | tf_op jit(solution)/shard_map/ppermute | solution.py:268
  134.3 5.1 %collective-permute-done.39.refs_11_ = bf16[256,640]{1,0:T(8,128)(2,1)S(1)} collective-permute-done((bf16[256,640]{1,0:T(8,128)(2,1)}, bf16[256,640]{1,0:T(8,128)(2,1)S(1)}, u32[]{:S(2)}, u32[]{:S(2)}) %collective-permute-start.39) | collective-permute-done | bytes 327712 | tf_op jit(solution)/shard_map/ppermute | solution.py:268
  140.6 6.7 %collective-permute-done.45.refs_5_ = bf16[1408,128]{1,0:T(8,128)(2,1)S(1)} collective-permute-done((bf16[1408,128]{1,0:T(8,128)(2,1)S(1)}, bf16[1408,128]{1,0:T(8,128)(2,1)S(1)}, u32[]{:S(2)}, u32[]{:S(2)}) %collective-permute-start.45) | collective-permute-done | bytes 360480 | tf_op jit(solution)/shard_map/ppermute | solution.py:268
  148.9 5.7 %collective-permute-done.49.refs_9_ = bf16[1408,128]{1,0:T(8,128)(2,1)S(1)} collective-permute-done((bf16[1408,128]{1,0:T(8,128)(2,1)S(1)}, bf16[1408,128]{1,0:T(8,128)(2,1)S(1)}, u32[]{:S(2)}, u32[]{:S(2)}) %collective-permute-start.49) | collective-permute-done | bytes 360480 | tf_op jit(solution)/shard_map/ppermute | solution.py:268
  158.3 5.2 %collective-permute-done.21.refs_5_ = bf16[256,768]{1,0:T(8,128)(2,1)S(1)} collective-permute-done((bf16[256,768]{1,0:T(8,128)(2,1)S(1)}, bf16[256,768]{1,0:T(8,128)(2,1)S(1)}, u32[]{:S(2)}, u32[]{:S(2)}) %collective-permute-start.21) | collective-permute-done | bytes 393248 | tf_op jit(solution)/shard_map/ppermute | solution.py:268
  165.2 6.6 %collective-permute-done.27.refs_11_ = bf16[256,768]{1,0:T(8,128)(2,1)S(1)} collective-permute-done((bf16[256,768]{1,0:T(8,128)(2,1)S(1)}, bf16[256,768]{1,0:T(8,128)(2,1)S(1)}, u32[]{:S(2)}, u32[]{:S(2)}) %collective-permute-start.27) | collective-permute-done | bytes 393248 | tf_op jit(solution)/shard_map/ppermute | solution.py:268
  181.6 4.6 %collective-permute-done.40.refs_12_ = bf16[256,640]{1,0:T(8,128)(2,1)} collective-permute-done((bf16[256,640]{1,0:T(8,128)(2,1)S(1)}, bf16[256,640]{1,0:T(8,128)(2,1)}, u32[]{:S(2)}, u32[]{:S(2)}) %collective-permute-start.40) | collective-permute-done | bytes 327712 | tf_op jit(solution)/shard_map/ppermute | solution.py:268
  188.4 5.4 %collective-permute-done.54.cw = bf16[1408,128]{1,0:T(8,128)(2,1)S(1)} collective-permute-done((bf16[1408,128]{1,0:T(8,128)(2,1)S(1)}, bf16[1408,128]{1,0:T(8,128)(2,1)S(1)}, u32[]{:S(2)}, u32[]{:S(2)}) %collective-permute-start.54) | collective-permute-done | bytes 360480 | tf_op jit(solution)/shard_map/ppermute | solution.py:268
  195.4 6.1 %collective-permute-done.56.ccw = bf16[1408,128]{1,0:T(8,128)(2,1)S(1)} collective-permute-done((bf16[1408,128]{1,0:T(8,128)(2,1)S(1)}, bf16[1408,128]{1,0:T(8,128)(2,1)S(1)}, u32[]{:S(2)}, u32[]{:S(2)}) %collective-permute-start.56) | collective-permute-done | bytes 360480 | tf_op jit(solution)/shard_map/ppermute | solution.py:268
  202.1 7.9 %collective-permute-done.22.refs_6_ = bf16[256,768]{1,0:T(8,128)(2,1)S(1)} collective-permute-done((bf16[256,768]{1,0:T(8,128)(2,1)S(1)}, bf16[256,768]{1,0:T(8,128)(2,1)S(1)}, u32[]{:S(2)}, u32[]{:S(2)}) %collective-permute-start.22) | collective-permute-done | bytes 393248 | tf_op jit(solution)/shard_map/ppermute | solution.py:268
  212.0 5.8 %collective-permute-done.28.refs_12_ = bf16[256,768]{1,0:T(8,128)(2,1)S(1)} collective-permute-done((bf16[256,768]{1,0:T(8,128)(2,1)S(1)}, bf16[256,768]{1,0:T(8,128)(2,1)S(1)}, u32[]{:S(2)}, u32[]{:S(2)}) %collective-permute-start.28) | collective-permute-done | bytes 393248 | tf_op jit(solution)/shard_map/ppermute | solution.py:268
  226.2 4.2 %collective-permute-done.25.refs_9_ = bf16[256,768]{1,0:T(8,128)(2,1)S(1)} collective-permute-done((bf16[256,768]{1,0:T(8,128)(2,1)S(1)}, bf16[256,768]{1,0:T(8,128)(2,1)S(1)}, u32[]{:S(2)}, u32[]{:S(2)}) %collective-permute-start.25) | collective-permute-done | bytes 393248 | tf_op jit(solution)/shard_map/ppermute | solution.py:270
  232.0 6.8 %collective-permute-done.31.refs_15_ = bf16[256,768]{1,0:T(8,128)(2,1)S(1)} collective-permute-done((bf16[256,768]{1,0:T(8,128)(2,1)S(1)}, bf16[256,768]{1,0:T(8,128)(2,1)S(1)}, u32[]{:S(2)}, u32[]{:S(2)}) %collective-permute-start.31) | collective-permute-done | bytes 393248 | tf_op jit(solution)/shard_map/ppermute | solution.py:270
  240.5 8.2 %shard_map.121.refs_1_.left = bf16[512,768]{1,0:T(8,128)(2,1)} custom-call(s32[3]{0:T(128)} %pad_add_fusion.info.refs_0_, bf16[8,512,256]{2,1,0:T(8,128)(2,1)} %shard_map.120.refs_1_, bf16[512,1408]{1,0:T(8,128)(2,1)} %refs_2_.3, bf16[512,1408]{1,0:T(8,128)(2,1)} %refs_3_.6, bf16[256,768]{1,0:T(8,128)(2,1)} %copy-done.22, bf16[256,768]{1,0:T(8,128)(2,1)} %copy-done.24, ...), custom_call_target="tpu_custom_call" | custom-call | flops 3221225472 | bytes 9699328 | tf_op jit(solution)/shard_map/pallas_call | solution.py:92
  254.6 7.8 %shard_map.122.refs_2_.right = bf16[512,640]{1,0:T(8,128)(2,1)} custom-call(s32[3]{0:T(128)} %pad_add_fusion.info.refs_0_, bf16[8,512,256]{2,1,0:T(8,128)(2,1)} %shard_map.120.refs_1_, bf16[512,1408]{1,0:T(8,128)(2,1)} %refs_2_.3, bf16[512,1408]{1,0:T(8,128)(2,1)} %refs_3_.6, bf16[256,640]{1,0:T(8,128)(2,1)} %collective-permute-done.32.refs_4_, ...), custom_call_target="tpu_custom_call" | custom-call | flops 2684354560 | bytes 8912896 | tf_op jit(solution)/shard_map/pallas_call | solution.py:92
  262.4 5.9 %collective-permute-done.47.refs_7_ = bf16[1408,128]{1,0:T(8,128)(2,1)S(1)} collective-permute-done((bf16[1408,128]{1,0:T(8,128)(2,1)}, bf16[1408,128]{1,0:T(8,128)(2,1)S(1)}, u32[]{:S(2)}, u32[]{:S(2)}) %collective-permute-start.47) | collective-permute-done | bytes 360480 | tf_op jit(solution)/shard_map/ppermute | solution.py:270
  268.3 7.7 %collective-permute-done.51.refs_11_ = bf16[1408,128]{1,0:T(8,128)(2,1)S(1)} collective-permute-done((bf16[1408,128]{1,0:T(8,128)(2,1)}, bf16[1408,128]{1,0:T(8,128)(2,1)S(1)}, u32[]{:S(2)}, u32[]{:S(2)}) %collective-permute-start.51) | collective-permute-done | bytes 360480 | tf_op jit(solution)/shard_map/ppermute | solution.py:270
  276.8 7.4 %shard_map.123 = (bf16[2,4,512,128]{3,2,1,0:T(8,128)(2,1)}, bf16[2,4,512,128]{3,2,1,0:T(8,128)(2,1)}) custom-call(s32[3]{0:T(128)} %pad_add_fusion.info.refs_0_, bf16[512,768]{1,0:T(8,128)(2,1)} %shard_map.121.refs_1_.left, bf16[512,640]{1,0:T(8,128)(2,1)} %shard_map.122.refs_2_.right, bf16[1408,512]{1,0:T(8,128)(2,1)} %refs_3_.7, ...), custom_call_target="tpu_custom_call" | custom-call | flops 2214592512 | bytes 5767168 | tf_op jit(solution)/shard_map/pallas_call | solution.py:92
  284.2 5.5 %collective-permute-done.57.ccw_y = bf16[1408,128]{1,0:T(8,128)(2,1)S(1)} collective-permute-done((bf16[1408,128]{1,0:T(8,128)(2,1)S(1)}, bf16[1408,128]{1,0:T(8,128)(2,1)S(1)}, u32[]{:S(2)}, u32[]{:S(2)}) %collective-permute-start.57) | collective-permute-done | bytes 360480 | tf_op jit(solution)/shard_map/ppermute | solution.py:270
  302.8 13.8 %collective-permute-done.53 = bf16[4,512,128]{2,1,0:T(8,128)(2,1)S(1)} collective-permute-done((bf16[4,512,128]{2,1,0:T(8,128)(2,1)S(1)}, bf16[4,512,128]{2,1,0:T(8,128)(2,1)S(1)}, u32[]{:S(2)}, u32[]{:S(2)}) %collective-permute-start.53) | collective-permute-done | bytes 524320 | tf_op jit(solution)/shard_map/ppermute | solution.py:277
  317.8 6.5 %psum.7 = f32[512]{0:T(512)S(1)} all-reduce(f32[512]{0:T(512)S(1)} %multiply_reduce_fusion), channel_id=1, replica_groups=mesh['grp'=2,'fs'=4,'tp'=4] {'tp'}, use_global_device_ids=true, to_apply=%region_1.2 | all-reduce | flops 512 | bytes 4096 | tf_op jit(solution)/shard_map/psum | solution.py:337
  (231 shorter events, 118.1 us)
Async XLA Ops:
  1.4 21.4 %collective-permute-start.1 = (bf16[2,512,256]{2,1,0:T(8,128)(2,1)S(1)}, bf16[2,512,256]{2,1,0:T(8,128)(2,1)S(1)}, u32[]{:S(2)}, u32[]{:S(2)}) collective-permute-start(bf16[2,512,256]{2,1,0:T(8,128)(2,1)S(1)} %bitcast.56), channel_id=1, source_target_pairs={{0,2},{1,3},{2,0},{3,1},{4,6},{5,7},{6,4},{7,5},{8,10},{9,11},{10,... | collective-permute-start | bytes 1572872 | tf_op jit(solution)/shard_map/ppermute | solution.py:277
  8.5 25.7 %collective-permute-start = (bf16[2,512,256]{2,1,0:T(8,128)(2,1)S(1)}, bf16[2,512,256]{2,1,0:T(8,128)(2,1)S(1)}, u32[]{:S(2)}, u32[]{:S(2)}) collective-permute-start(bf16[2,512,256]{2,1,0:T(8,128)(2,1)S(1)} %bitcast.57), channel_id=1, source_target_pairs={{0,1},{1,0},{2,3},{3,2},{4,5},{5,4},{6,7},{7,6},{8,9},{9,8},{10,11... | collective-permute-start | bytes 1572872 | tf_op jit(solution)/shard_map/ppermute | solution.py:274
  22.8 22.4 %collective-permute-start.2 = (bf16[2,512,256]{2,1,0:T(8,128)(2,1)S(1)}, bf16[2,512,256]{2,1,0:T(8,128)(2,1)S(1)}, u32[]{:S(2)}, u32[]{:S(2)}) collective-permute-start(bf16[2,512,256]{2,1,0:T(8,128)(2,1)S(1)} %collective-permute-done.1.b2), channel_id=1, source_target_pairs={{0,1},{1,0},{2,3},{3,2},{4,5},{5,4},{6,7},{7,6},{8,9},{9,8},{10,11... | collective-permute-start | bytes 1572872 | tf_op jit(solution)/shard_map/ppermute | solution.py:274
  72.5 37.7 %collective-permute-start.15 = (bf16[2,2,512,256]{3,2,1,0:T(8,128)(2,1)}, bf16[2,2,512,256]{3,2,1,0:T(8,128)(2,1)S(1)}, u32[]{:S(2)}, u32[]{:S(2)}) collective-permute-start(bf16[2,2,512,256]{3,2,1,0:T(8,128)(2,1)} %get-tuple-element.10), channel_id=1, source_target_pairs={{0,1},{1,0},{2,3},{3,2},{4,5},{5,4},{6,7},{7,6},{8,9},{9,8},{10,11... | collective-permute-start | bytes 3145736 | tf_op jit(solution)/shard_map/ppermute | solution.py:274
  79.7 21.2 %collective-permute-start.44 = (bf16[1408,128]{1,0:T(8,128)(2,1)S(1)}, bf16[1408,128]{1,0:T(8,128)(2,1)S(1)}, u32[]{:S(2)}, u32[]{:S(2)}) collective-permute-start(bf16[1408,128]{1,0:T(8,128)(2,1)S(1)} %get-tuple-element.14), channel_id=1, source_target_pairs={{0,4},{4,8},{8,12},{12,0},{1,5},{5,9},{9,13},{13,1},{2,6},{6,10},{... | collective-permute-start | bytes 1081352 | tf_op jit(solution)/shard_map/ppermute | solution.py:268
  79.7 28.9 %collective-permute-start.48 = (bf16[1408,128]{1,0:T(8,128)(2,1)S(1)}, bf16[1408,128]{1,0:T(8,128)(2,1)S(1)}, u32[]{:S(2)}, u32[]{:S(2)}) collective-permute-start(bf16[1408,128]{1,0:T(8,128)(2,1)S(1)} %get-tuple-element.13), channel_id=1, source_target_pairs={{4,0},{8,4},{12,8},{0,12},{5,1},{9,5},{13,9},{1,13},{6,2},{10,6},{... | collective-permute-start | bytes 1081352 | tf_op jit(solution)/shard_map/ppermute | solution.py:268
  86.2 30.9 %collective-permute-start.20 = (bf16[256,768]{1,0:T(8,128)(2,1)S(1)}, bf16[256,768]{1,0:T(8,128)(2,1)S(1)}, u32[]{:S(2)}, u32[]{:S(2)}) collective-permute-start(bf16[256,768]{1,0:T(8,128)(2,1)S(1)} %constant_dynamic-slice_fusion.1), channel_id=1, source_target_pairs={{0,4},{4,8},{8,12},{12,0},{1,5},{5,9},{9,13},{13,1},{2,6},{6,10},{... | collective-permute-start | bytes 1179656 | tf_op jit(solution)/shard_map/ppermute | solution.py:268
  93.2 32.2 %collective-permute-start.26 = (bf16[256,768]{1,0:T(8,128)(2,1)S(1)}, bf16[256,768]{1,0:T(8,128)(2,1)S(1)}, u32[]{:S(2)}, u32[]{:S(2)}) collective-permute-start(bf16[256,768]{1,0:T(8,128)(2,1)S(1)} %constant_dynamic-slice_fusion), channel_id=1, source_target_pairs={{4,0},{8,4},{12,8},{0,12},{5,1},{9,5},{13,9},{1,13},{6,2},{10,6},{... | collective-permute-start | bytes 1179656 | tf_op jit(solution)/shard_map/ppermute | solution.py:268
  100.8 31.7 %collective-permute-start.33 = (bf16[256,640]{1,0:T(8,128)(2,1)}, bf16[256,640]{1,0:T(8,128)(2,1)S(1)}, u32[]{:S(2)}, u32[]{:S(2)}) collective-permute-start(bf16[256,640]{1,0:T(8,128)(2,1)} %collective-permute-done.32.refs_4_), channel_id=1, source_target_pairs={{0,4},{4,8},{8,12},{12,0},{1,5},{5,9},{9,13},{13,1},{2,6},{6,10},{... | collective-permute-start | bytes 983048 | tf_op jit(solution)/shard_map/ppermute | solution.py:268
  108.6 25.5 %collective-permute-start.35 = (bf16[256,640]{1,0:T(8,128)(2,1)}, bf16[256,640]{1,0:T(8,128)(2,1)S(1)}, u32[]{:S(2)}, u32[]{:S(2)}) collective-permute-start(bf16[256,640]{1,0:T(8,128)(2,1)} %collective-permute-done.32.refs_4_), channel_id=1, source_target_pairs={{0,16},{16,0},{1,17},{17,1},{2,18},{18,2},{3,19},{19,3},{4,20},{20... | collective-permute-start | bytes 983048 | tf_op jit(solution)/shard_map/ppermute | solution.py:270
  110.1 29.3 %collective-permute-start.39 = (bf16[256,640]{1,0:T(8,128)(2,1)}, bf16[256,640]{1,0:T(8,128)(2,1)S(1)}, u32[]{:S(2)}, u32[]{:S(2)}) collective-permute-start(bf16[256,640]{1,0:T(8,128)(2,1)} %collective-permute-done.38.refs_10_), channel_id=1, source_target_pairs={{4,0},{8,4},{12,8},{0,12},{5,1},{9,5},{13,9},{1,13},{6,2},{10,6},{... | collective-permute-start | bytes 983048 | tf_op jit(solution)/shard_map/ppermute | solution.py:268
  117.0 23.1 %collective-permute-start.41 = (bf16[256,640]{1,0:T(8,128)(2,1)}, bf16[256,640]{1,0:T(8,128)(2,1)}, u32[]{:S(2)}, u32[]{:S(2)}) collective-permute-start(bf16[256,640]{1,0:T(8,128)(2,1)} %collective-permute-done.38.refs_10_), channel_id=1, source_target_pairs={{0,16},{16,0},{1,17},{17,1},{2,18},{18,2},{3,19},{19,3},{4,20},{20... | collective-permute-start | bytes 983048 | tf_op jit(solution)/shard_map/ppermute | solution.py:270
  125.4 21.9 %collective-permute-start.45 = (bf16[1408,128]{1,0:T(8,128)(2,1)S(1)}, bf16[1408,128]{1,0:T(8,128)(2,1)S(1)}, u32[]{:S(2)}, u32[]{:S(2)}) collective-permute-start(bf16[1408,128]{1,0:T(8,128)(2,1)S(1)} %collective-permute-done.44.refs_4_), channel_id=1, source_target_pairs={{0,4},{4,8},{8,12},{12,0},{1,5},{5,9},{9,13},{13,1},{2,6},{6,10},{... | collective-permute-start | bytes 1081352 | tf_op jit(solution)/shard_map/ppermute | solution.py:268
  132.5 24.2 %collective-permute-start.46 = (bf16[1408,128]{1,0:T(8,128)(2,1)S(1)}, bf16[1408,128]{1,0:T(8,128)(2,1)S(1)}, u32[]{:S(2)}, u32[]{:S(2)}) collective-permute-start(bf16[1408,128]{1,0:T(8,128)(2,1)S(1)} %collective-permute-done.44.refs_4_), channel_id=1, source_target_pairs={{0,16},{16,0},{1,17},{17,1},{2,18},{18,2},{3,19},{19,3},{4,20},{20... | collective-permute-start | bytes 1081352 | tf_op jit(solution)/shard_map/ppermute | solution.py:270
  134.1 20.5 %collective-permute-start.49 = (bf16[1408,128]{1,0:T(8,128)(2,1)S(1)}, bf16[1408,128]{1,0:T(8,128)(2,1)S(1)}, u32[]{:S(2)}, u32[]{:S(2)}) collective-permute-start(bf16[1408,128]{1,0:T(8,128)(2,1)S(1)} %collective-permute-done.48.refs_8_), channel_id=1, source_target_pairs={{4,0},{8,4},{12,8},{0,12},{5,1},{9,5},{13,9},{1,13},{6,2},{10,6},{... | collective-permute-start | bytes 1081352 | tf_op jit(solution)/shard_map/ppermute | solution.py:268
  139.4 35.8 %collective-permute-start.16 = (bf16[2,512,256]{2,1,0:T(8,128)(2,1)S(1)}, bf16[2,512,256]{2,1,0:T(8,128)(2,1)S(1)}, u32[]{:S(2)}, u32[]{:S(2)}) collective-permute-start(bf16[2,512,256]{2,1,0:T(8,128)(2,1)S(1)} %fusion.7), channel_id=1, source_target_pairs={{0,2},{1,3},{2,0},{3,1},{4,6},{5,7},{6,4},{7,5},{8,10},{9,11},{10,... | collective-permute-start | bytes 1572872 | tf_op jit(solution)/shard_map/ppermute | solution.py:277
  140.1 23.4 %collective-permute-start.21 = (bf16[256,768]{1,0:T(8,128)(2,1)S(1)}, bf16[256,768]{1,0:T(8,128)(2,1)S(1)}, u32[]{:S(2)}, u32[]{:S(2)}) collective-permute-start(bf16[256,768]{1,0:T(8,128)(2,1)S(1)} %collective-permute-done.20.refs_4_), channel_id=1, source_target_pairs={{0,4},{4,8},{8,12},{12,0},{1,5},{5,9},{9,13},{13,1},{2,6},{6,10},{... | collective-permute-start | bytes 1179656 | tf_op jit(solution)/shard_map/ppermute | solution.py:268
  175.2 18.6 %collective-permute-start.54 = (bf16[1408,128]{1,0:T(8,128)(2,1)S(1)}, bf16[1408,128]{1,0:T(8,128)(2,1)S(1)}, u32[]{:S(2)}, u32[]{:S(2)}) collective-permute-start(bf16[1408,128]{1,0:T(8,128)(2,1)S(1)} %collective-permute-done.45.refs_5_), channel_id=1, source_target_pairs={{0,4},{4,8},{8,12},{12,0},{1,5},{5,9},{9,13},{13,1},{2,6},{6,10},{... | collective-permute-start | bytes 1081352 | tf_op jit(solution)/shard_map/ppermute | solution.py:268
  179.1 22.4 %collective-permute-start.18 = (bf16[2,512,256]{2,1,0:T(8,128)(2,1)S(1)}, bf16[2,512,256]{2,1,0:T(8,128)(2,1)S(1)}, u32[]{:S(2)}, u32[]{:S(2)}) collective-permute-start(bf16[2,512,256]{2,1,0:T(8,128)(2,1)S(1)} %fusion.5.b0), channel_id=1, source_target_pairs={{0,2},{1,3},{2,0},{3,1},{4,6},{5,7},{6,4},{7,5},{8,10},{9,11},{10,... | collective-permute-start | bytes 1572872 | tf_op jit(solution)/shard_map/ppermute | solution.py:277
  179.9 21.7 %collective-permute-start.56 = (bf16[1408,128]{1,0:T(8,128)(2,1)S(1)}, bf16[1408,128]{1,0:T(8,128)(2,1)S(1)}, u32[]{:S(2)}, u32[]{:S(2)}) collective-permute-start(bf16[1408,128]{1,0:T(8,128)(2,1)S(1)} %collective-permute-done.49.refs_9_), channel_id=1, source_target_pairs={{4,0},{8,4},{12,8},{0,12},{5,1},{9,5},{13,9},{1,13},{6,2},{10,6},{... | collective-permute-start | bytes 1081352 | tf_op jit(solution)/shard_map/ppermute | solution.py:268
  186.2 23.8 %collective-permute-start.22 = (bf16[256,768]{1,0:T(8,128)(2,1)S(1)}, bf16[256,768]{1,0:T(8,128)(2,1)S(1)}, u32[]{:S(2)}, u32[]{:S(2)}) collective-permute-start(bf16[256,768]{1,0:T(8,128)(2,1)S(1)} %collective-permute-done.21.refs_5_), channel_id=1, source_target_pairs={{0,4},{4,8},{8,12},{12,0},{1,5},{5,9},{9,13},{13,1},{2,6},{6,10},{... | collective-permute-start | bytes 1179656 | tf_op jit(solution)/shard_map/ppermute | solution.py:268
  186.8 24.8 %collective-permute-start.24 = (bf16[256,768]{1,0:T(8,128)(2,1)S(1)}, bf16[256,768]{1,0:T(8,128)(2,1)S(1)}, u32[]{:S(2)}, u32[]{:S(2)}) collective-permute-start(bf16[256,768]{1,0:T(8,128)(2,1)S(1)} %collective-permute-done.21.refs_5_), channel_id=1, source_target_pairs={{0,16},{16,0},{1,17},{17,1},{2,18},{18,2},{3,19},{19,3},{4,20},{20... | collective-permute-start | bytes 1179656 | tf_op jit(solution)/shard_map/ppermute | solution.py:270
  193.8 24.0 %collective-permute-start.28 = (bf16[256,768]{1,0:T(8,128)(2,1)S(1)}, bf16[256,768]{1,0:T(8,128)(2,1)S(1)}, u32[]{:S(2)}, u32[]{:S(2)}) collective-permute-start(bf16[256,768]{1,0:T(8,128)(2,1)S(1)} %collective-permute-done.27.refs_11_), channel_id=1, source_target_pairs={{4,0},{8,4},{12,8},{0,12},{5,1},{9,5},{13,9},{1,13},{6,2},{10,6},{... | collective-permute-start | bytes 1179656 | tf_op jit(solution)/shard_map/ppermute | solution.py:268
  211.6 18.8 %collective-permute-start.25 = (bf16[256,768]{1,0:T(8,128)(2,1)S(1)}, bf16[256,768]{1,0:T(8,128)(2,1)S(1)}, u32[]{:S(2)}, u32[]{:S(2)}) collective-permute-start(bf16[256,768]{1,0:T(8,128)(2,1)S(1)} %collective-permute-done.22.refs_6_), channel_id=1, source_target_pairs={{0,16},{16,0},{1,17},{17,1},{2,18},{18,2},{3,19},{19,3},{4,20},{20... | collective-permute-start | bytes 1179656 | tf_op jit(solution)/shard_map/ppermute | solution.py:270
  217.8 21.0 %collective-permute-start.31 = (bf16[256,768]{1,0:T(8,128)(2,1)S(1)}, bf16[256,768]{1,0:T(8,128)(2,1)S(1)}, u32[]{:S(2)}, u32[]{:S(2)}) collective-permute-start(bf16[256,768]{1,0:T(8,128)(2,1)S(1)} %collective-permute-done.28.refs_12_), channel_id=1, source_target_pairs={{0,16},{16,0},{1,17},{17,1},{2,18},{18,2},{3,19},{19,3},{4,20},{20... | collective-permute-start | bytes 1179656 | tf_op jit(solution)/shard_map/ppermute | solution.py:270
  219.4 29.2 %collective-permute-start.37 = (bf16[256,640]{1,0:T(8,128)(2,1)}, bf16[256,640]{1,0:T(8,128)(2,1)}, u32[]{:S(2)}, u32[]{:S(2)}) collective-permute-start(bf16[256,640]{1,0:T(8,128)(2,1)} %collective-permute-done.34.refs_6_), channel_id=1, source_target_pairs={{0,16},{16,0},{1,17},{17,1},{2,18},{18,2},{3,19},{19,3},{4,20},{20... | collective-permute-start | bytes 983048 | tf_op jit(solution)/shard_map/ppermute | solution.py:270
  219.8 33.1 %collective-permute-start.43 = (bf16[256,640]{1,0:T(8,128)(2,1)}, bf16[256,640]{1,0:T(8,128)(2,1)}, u32[]{:S(2)}, u32[]{:S(2)}) collective-permute-start(bf16[256,640]{1,0:T(8,128)(2,1)} %collective-permute-done.40.refs_12_), channel_id=1, source_target_pairs={{0,16},{16,0},{1,17},{17,1},{2,18},{18,2},{3,19},{19,3},{4,20},{20... | collective-permute-start | bytes 983048 | tf_op jit(solution)/shard_map/ppermute | solution.py:270
  225.4 37.0 %collective-permute-start.50 = (bf16[1408,128]{1,0:T(8,128)(2,1)S(1)}, bf16[1408,128]{1,0:T(8,128)(2,1)S(1)}, u32[]{:S(2)}, u32[]{:S(2)}) collective-permute-start(bf16[1408,128]{1,0:T(8,128)(2,1)S(1)} %copy-done.36), channel_id=1, source_target_pairs={{0,16},{16,0},{1,17},{17,1},{2,18},{18,2},{3,19},{19,3},{4,20},{20... | collective-permute-start | bytes 1081352 | tf_op jit(solution)/shard_map/ppermute | solution.py:270
  230.4 37.9 %collective-permute-start.47 = (bf16[1408,128]{1,0:T(8,128)(2,1)}, bf16[1408,128]{1,0:T(8,128)(2,1)S(1)}, u32[]{:S(2)}, u32[]{:S(2)}) collective-permute-start(bf16[1408,128]{1,0:T(8,128)(2,1)} %copy-done.37), channel_id=1, source_target_pairs={{0,16},{16,0},{1,17},{17,1},{2,18},{18,2},{3,19},{19,3},{4,20},{20... | collective-permute-start | bytes 1081352 | tf_op jit(solution)/shard_map/ppermute | solution.py:270
  238.8 37.2 %collective-permute-start.51 = (bf16[1408,128]{1,0:T(8,128)(2,1)}, bf16[1408,128]{1,0:T(8,128)(2,1)S(1)}, u32[]{:S(2)}, u32[]{:S(2)}) collective-permute-start(bf16[1408,128]{1,0:T(8,128)(2,1)} %copy-done.39), channel_id=1, source_target_pairs={{0,16},{16,0},{1,17},{17,1},{2,18},{18,2},{3,19},{19,3},{4,20},{20... | collective-permute-start | bytes 1081352 | tf_op jit(solution)/shard_map/ppermute | solution.py:270
  248.6 35.5 %collective-permute-start.55 = (bf16[1408,128]{1,0:T(8,128)(2,1)S(1)}, bf16[1408,128]{1,0:T(8,128)(2,1)S(1)}, u32[]{:S(2)}, u32[]{:S(2)}) collective-permute-start(bf16[1408,128]{1,0:T(8,128)(2,1)S(1)} %collective-permute-done.54.cw), channel_id=1, source_target_pairs={{0,16},{16,0},{1,17},{17,1},{2,18},{18,2},{3,19},{19,3},{4,20},{20... | collective-permute-start | bytes 1081352 | tf_op jit(solution)/shard_map/ppermute | solution.py:270
  253.0 36.7 %collective-permute-start.57 = (bf16[1408,128]{1,0:T(8,128)(2,1)S(1)}, bf16[1408,128]{1,0:T(8,128)(2,1)S(1)}, u32[]{:S(2)}, u32[]{:S(2)}) collective-permute-start(bf16[1408,128]{1,0:T(8,128)(2,1)S(1)} %collective-permute-done.56.ccw), channel_id=1, source_target_pairs={{0,16},{16,0},{1,17},{17,1},{2,18},{18,2},{3,19},{19,3},{4,20},{20... | collective-permute-start | bytes 1081352 | tf_op jit(solution)/shard_map/ppermute | solution.py:270
  (80 other events, 2160.0 us)

commit v3 on v2

--- a/solution.py
+++ b/solution.py
@@ -10,7 +10,7 @@
 
 BF16 = jnp.bfloat16
 F32 = jnp.float32
-VMEM_LIMIT = 56 * 1024 * 1024
+VMEM_LIMIT = 20 * 1024 * 1024
 
 
 def rms_norm(values, gain):
@@ -236,15 +236,27 @@
             store(count - 1, direction, 2 * i + last, jnp.zeros((rows, piece), F32))
 
 
-def down_late_kernel(info, left, right, cw, cw_y, ccw, ccw_y, out, *, count, split):
+def down_late_kernel(info, left, right, cw, cw_y, ccw, ccw_y, near, far, *, count, split):
     g = info[1]
-    piece = out.shape[-1]
-    for direction, mine, other in ((1, cw, cw_y), (-1, ccw, ccw_y)):
-        weight = jnp.concatenate([mine[...], other[...]], axis=1)
-        value = dot(left[...], weight[:split]) + dot(right[...], weight[split:])
+    piece = near.shape[-1]
+    weight = jnp.concatenate([p[...] for p in (cw, cw_y, ccw, ccw_y)], axis=1)
+    value = (dot(left[...], weight[:split]) + dot(right[...], weight[split:])).astype(BF16)
+    for i, direction in enumerate((1, -1)):
         spot = place(info, count - 1, direction, count) // 2
-        out[spot, g] = value[:, :piece].astype(BF16)
-        out[spot, 1 - g] = value[:, piece:].astype(BF16)
+        for at, target in enumerate((near, far)):
+
+            @pl.when(spot == at)
+            def _():
+                target[g] = value[:, 2 * i * piece : (2 * i + 1) * piece]
+                target[1 - g] = value[:, (2 * i + 1) * piece : (2 * i + 2) * piece]
+
+
+def close_kernel(squares, second, gain, out, *, width):
+    rows, piece = second.shape[1:]
+    factor = lax.rsqrt(squares[...] / width + 1e-06)
+    factor = jnp.broadcast_to(factor, (piece, rows)).T
+    for p in range(second.shape[0]):
+        out[:, p * piece : (p + 1) * piece] = (second[p] * factor * gain[p]).astype(BF16)
 
 
 def ring_local(
@@ -322,23 +334,35 @@
     second = first.reshape(2, rows, 2, half // 2).transpose(0, 2, 1, 3).reshape(4, rows, half // 2)
     second = second.astype(F32) + scatter(partial)
     kernel = functools.partial(down_late_kernel, **split_by)
-    rest = call(kernel, info, late, [(2, 2, *piece)], flops // 4)[0]
-
-    takers = [[(s + 1) % 2 == i % 2 for i in range(4)] for s in range(count)]
-    to_mate = [(4 * s + i, 4 * s + (i ^ 1)) for s in range(count) for i in range(4) if not takers[s][i]]
-    to_other = [(4 * s + i, 4 * s + (i ^ 2)) for s in range(count) for i in range(4) if takers[s][i]]
-    met = rest.astype(F32) + lax.ppermute(rest, ("fs", "tp"), to_mate).astype(F32)
-    met = met[0] + lax.ppermute(met[1].astype(BF16), ("fs", "tp"), to_other).astype(F32)
+    near, far = call(kernel, info, late, [(2, *piece)] * 2, flops // 4)
+
+    both = [(s, i) for s in range(count) for i in range(4)]
+    takers = [(s, i) for s, i in both if (s + 1) % 2 == i % 2]
+    others = [(s, i) for s, i in both if (s + 1) % 2 != i % 2]
+
+    def late_send(value, senders, flip):
+        pairs = [(4 * s + i, 4 * s + (i ^ flip)) for s, i in senders]
+        return lax.ppermute(value, ("fs", "tp"), pairs).astype(F32)
+
+    met = late_send(far, takers, 2) + late_send(far, others, 3)
+    met = met + late_send(near, others, 1) + near.astype(F32)
     takes = lax.rem(z + 1 + q, 2) == 0
     parity = jnp.where(q == lax.rem(z + 1, count), 0, 1)
     mask = takes & (jnp.arange(2) == parity)
     late_part = jnp.where(mask[None, :, None, None], met[:, None], 0.0).reshape(second.shape)
     second = second + late_part
     squares = lax.psum(jnp.sum(second * second, axis=(0, 2)), "tp")
-    factor = lax.rsqrt(squares / width + 1e-06)
     own_gain = lax.dynamic_slice_in_dim(out_gain, q * columns, columns, 0).reshape(4, 1, half // 2)
-    result = (second * factor[None, :, None] * own_gain).astype(BF16)
-    return result.transpose(1, 0, 2).reshape(seq_count, length, columns)
+    in_vmem = pl.BlockSpec(memory_space=pltpu.VMEM)
+    result = pl.pallas_call(
+        functools.partial(close_kernel, width=width),
+        in_specs=[in_vmem] * 3,
+        out_specs=in_vmem,
+        out_shape=jax.ShapeDtypeStruct((rows, columns), BF16),
+        compiler_params=pltpu.CompilerParams(vmem_limit_bytes=VMEM_LIMIT),
+        name="close",
+    )(squares.reshape(1, rows), second, own_gain)
+    return result.reshape(seq_count, length, columns)
 
 
 def fits_ring(mesh):

time: 328 us -> 333 us (1.015)
  Pallas kernels: 43.2 us -> 26.8 us
  waiting for transfers between devices: 192 us -> 208 us
  starting transfers between devices: 67.7 us -> 75.4 us
    ppermute x24, waiting for transfers between devices: 47.5 us -> 75.6 us  [ring(): swapped.append(lax.ppermute(value, 'grp', [(0, 1), (1, 0)]))]
    pallas_call x7, Pallas kernels: 43.2 us -> 25.8 us  [call(): pl.pallas_call(kernel, in_specs=[pl.BlockSpec(memory_space=pltpu.SMEM)] +...]
    ppermute x24, waiting for transfers between devices: 129 us -> 119 us  [ring(): value = lax.ppermute(value, 'fs', pairs)]
  transfers between devices with their start and end apart: 60 -> 61, of which waited for: 35 -> 39; matrix products, arithmetic and copies ran while one was open for 3% -> 4% of each run, Pallas kernels for 11% -> 4%
where the time goes in v3:
time: 333 us
  waiting for transfers between devices  208 us (62%)
  starting transfers between devices  75.4 us (23%)
  Pallas kernels  26.8 us (8%)
  local copies, waits for them, and re-layouts  11.9 us (4%)
  blocking collectives  6.69 us (2%)
  other arithmetic  3.81 us (1%)
    ppermute x24, waiting for transfers between devices, ring(): value = lax.ppermute(value, 'fs', pairs)  119 us
    ppermute x24, waiting for transfers between devices, ring(): swapped.append(lax.ppermute(value, 'grp', [(0, 1), (1, 0)]))  75.6 us
    ppermute x24, starting transfers between devices, ring(): swapped.append(lax.ppermute(value, 'grp', [(0, 1), (1, 0)]))  35.4 us
    ppermute x24, starting transfers between devices, ring(): value = lax.ppermute(value, 'fs', pairs)  30.4 us
    pallas_call x7, Pallas kernels, call(): pl.pallas_call(kernel, in_specs=[pl.BlockSpec(memory_space=pltpu.SMEM)] +...  25.8 us
    ppermute x4, waiting for transfers between devices, across(): return lax.ppermute(value, 'tp', [(i, i ^ 2) for i in range(4)])  12.3 us
    psum x1, blocking collectives, ring_local(): squares = lax.psum(jnp.sum(second * second, axis=(0, 2)), 'tp')  6.69 us
  transfers between devices with their start and end apart: 61, of which 39 were waited for; matrix products, arithmetic and copies ran while one was open for 4% of the time, Pallas kernels for 4%

profile of v3, /device:TPU:0, one launch (start us, length us, event | category | flops | bytes accessed | tf_op | source)
XLA Modules:
  0.0 332.9 jit_solution(5688509079754446095)
XLA Ops:
  9.1 7.1 %collective-permute-done.3.refs_7_ = bf16[512,256]{1,0:T(8,128)(2,1)S(1)} collective-permute-done((bf16[512,256]{1,0:T(8,128)(2,1)S(1)}, bf16[512,256]{1,0:T(8,128)(2,1)S(1)}, u32[]{:S(2)}, u32[]{:S(2)}) %collective-permute-start.3) | collective-permute-done | bytes 262176 | tf_op jit(solution)/shard_map/ppermute | solution.py:280
  16.2 4.7 %collective-permute-done.9.refs_13_ = bf16[512,256]{1,0:T(8,128)(2,1)} collective-permute-done((bf16[512,256]{1,0:T(8,128)(2,1)S(1)}, bf16[512,256]{1,0:T(8,128)(2,1)}, u32[]{:S(2)}, u32[]{:S(2)}) %collective-permute-start.9) | collective-permute-done | bytes 262176 | tf_op jit(solution)/shard_map/ppermute | solution.py:280
  28.4 4.5 %collective-permute-done.10.refs_14_ = bf16[512,256]{1,0:T(8,128)(2,1)} collective-permute-done((bf16[512,256]{1,0:T(8,128)(2,1)}, bf16[512,256]{1,0:T(8,128)(2,1)}, u32[]{:S(2)}, u32[]{:S(2)}) %collective-permute-start.10) | collective-permute-done | bytes 262176 | tf_op jit(solution)/shard_map/ppermute | solution.py:280
  49.9 5.6 %collective-permute-done.13.refs_17_ = bf16[512,256]{1,0:T(8,128)(2,1)} collective-permute-done((bf16[512,256]{1,0:T(8,128)(2,1)}, bf16[512,256]{1,0:T(8,128)(2,1)}, u32[]{:S(2)}, u32[]{:S(2)}) %collective-permute-start.13) | collective-permute-done | bytes 262176 | tf_op jit(solution)/shard_map/ppermute | solution.py:282
  55.6 5.6 %collective-permute-done.8.refs_12_ = bf16[512,256]{1,0:T(8,128)(2,1)} collective-permute-done((bf16[512,256]{1,0:T(8,128)(2,1)}, bf16[512,256]{1,0:T(8,128)(2,1)}, u32[]{:S(2)}, u32[]{:S(2)}) %collective-permute-start.8) | collective-permute-done | bytes 262176 | tf_op jit(solution)/shard_map/ppermute | solution.py:282
  64.0 7.2 %shard_map.119 = (bf16[2,2,512,256]{3,2,1,0:T(8,128)(2,1)S(1)}, bf16[2,2,512,256]{3,2,1,0:T(8,128)(2,1)}) custom-call(s32[3]{0:T(128)S(1)} %pad_add_fusion.info.refs_0_, f32[3,1024]{1,0:T(4,128)S(1)} %copy-done.18, bf16[8,512,256]{2,1,0:T(8,128)(2,1)S(1)} %shard_map.118.refs_2_, bf16[512,256]{1,0:T(8,128)(2,1)S(1)} %copy-done.4, ...), custom_call_target="tpu_custom_call" | custom-call | flops 2147483648 | bytes 6297600 | tf_op jit(solution)/shard_map/pallas_call | solution.py:92
  82.2 3.8 %collective-permute-start.38 = (bf16[256,640]{1,0:T(8,128)(2,1)}, bf16[256,640]{1,0:T(8,128)(2,1)}, u32[]{:S(2)}, u32[]{:S(2)}) collective-permute-start(bf16[256,640]{1,0:T(8,128)(2,1)} %dynamic-slice.3), channel_id=1, source_target_pairs={{4,0},{8,4},{12,8},{0,12},{5,1},{9,5},{13,9},{1,13},{6,2},{10,6},{... | collective-permute-start | bytes 983048 | tf_op jit(solution)/shard_map/ppermute | solution.py:280
  87.7 15.0 %collective-permute-done.32.refs_4_ = bf16[256,640]{1,0:T(8,128)(2,1)} collective-permute-done((bf16[256,640]{1,0:T(8,128)(2,1)}, bf16[256,640]{1,0:T(8,128)(2,1)}, u32[]{:S(2)}, u32[]{:S(2)}) %collective-permute-start.32) | collective-permute-done | bytes 327712 | tf_op jit(solution)/shard_map/ppermute | solution.py:280
  102.7 7.0 %collective-permute-done.38.refs_10_ = bf16[256,640]{1,0:T(8,128)(2,1)} collective-permute-done((bf16[256,640]{1,0:T(8,128)(2,1)}, bf16[256,640]{1,0:T(8,128)(2,1)}, u32[]{:S(2)}, u32[]{:S(2)}) %collective-permute-start.38) | collective-permute-done | bytes 327712 | tf_op jit(solution)/shard_map/ppermute | solution.py:280
  110.3 7.1 %collective-permute-done.44.refs_4_ = bf16[1408,128]{1,0:T(8,128)(2,1)S(1)} collective-permute-done((bf16[1408,128]{1,0:T(8,128)(2,1)S(1)}, bf16[1408,128]{1,0:T(8,128)(2,1)S(1)}, u32[]{:S(2)}, u32[]{:S(2)}) %collective-permute-start.44) | collective-permute-done | bytes 360480 | tf_op jit(solution)/shard_map/ppermute | solution.py:280
  117.9 6.9 %collective-permute-done.48.refs_8_ = bf16[1408,128]{1,0:T(8,128)(2,1)S(1)} collective-permute-done((bf16[1408,128]{1,0:T(8,128)(2,1)S(1)}, bf16[1408,128]{1,0:T(8,128)(2,1)S(1)}, u32[]{:S(2)}, u32[]{:S(2)}) %collective-permute-start.48) | collective-permute-done | bytes 360480 | tf_op jit(solution)/shard_map/ppermute | solution.py:280
  128.6 3.5 %collective-permute-done.33.refs_5_ = bf16[256,640]{1,0:T(8,128)(2,1)S(1)} collective-permute-done((bf16[256,640]{1,0:T(8,128)(2,1)}, bf16[256,640]{1,0:T(8,128)(2,1)S(1)}, u32[]{:S(2)}, u32[]{:S(2)}) %collective-permute-start.33) | collective-permute-done | bytes 327712 | tf_op jit(solution)/shard_map/ppermute | solution.py:280
  143.4 3.6 %collective-permute-done.45.refs_5_ = bf16[1408,128]{1,0:T(8,128)(2,1)S(1)} collective-permute-done((bf16[1408,128]{1,0:T(8,128)(2,1)S(1)}, bf16[1408,128]{1,0:T(8,128)(2,1)S(1)}, u32[]{:S(2)}, u32[]{:S(2)}) %collective-permute-start.45) | collective-permute-done | bytes 360480 | tf_op jit(solution)/shard_map/ppermute | solution.py:280
  149.0 13.6 %collective-permute-done.49.refs_9_ = bf16[1408,128]{1,0:T(8,128)(2,1)S(1)} collective-permute-done((bf16[1408,128]{1,0:T(8,128)(2,1)S(1)}, bf16[1408,128]{1,0:T(8,128)(2,1)S(1)}, u32[]{:S(2)}, u32[]{:S(2)}) %collective-permute-start.49) | collective-permute-done | bytes 360480 | tf_op jit(solution)/shard_map/ppermute | solution.py:280
  165.4 6.0 %collective-permute-done.27.refs_11_ = bf16[256,768]{1,0:T(8,128)(2,1)S(1)} collective-permute-done((bf16[256,768]{1,0:T(8,128)(2,1)S(1)}, bf16[256,768]{1,0:T(8,128)(2,1)S(1)}, u32[]{:S(2)}, u32[]{:S(2)}) %collective-permute-start.27) | collective-permute-done | bytes 393248 | tf_op jit(solution)/shard_map/ppermute | solution.py:280
  175.0 3.6 %collective-permute-done.34.refs_6_ = bf16[256,640]{1,0:T(8,128)(2,1)S(1)} collective-permute-done((bf16[256,640]{1,0:T(8,128)(2,1)S(1)}, bf16[256,640]{1,0:T(8,128)(2,1)S(1)}, u32[]{:S(2)}, u32[]{:S(2)}) %collective-permute-start.34) | collective-permute-done | bytes 327712 | tf_op jit(solution)/shard_map/ppermute | solution.py:280
  178.8 6.7 %collective-permute-done.40.refs_12_ = bf16[256,640]{1,0:T(8,128)(2,1)S(1)} collective-permute-done((bf16[256,640]{1,0:T(8,128)(2,1)S(1)}, bf16[256,640]{1,0:T(8,128)(2,1)S(1)}, u32[]{:S(2)}, u32[]{:S(2)}) %collective-permute-start.40) | collective-permute-done | bytes 327712 | tf_op jit(solution)/shard_map/ppermute | solution.py:280
  189.1 5.0 %collective-permute-done.22.refs_6_ = bf16[256,768]{1,0:T(8,128)(2,1)S(1)} collective-permute-done((bf16[256,768]{1,0:T(8,128)(2,1)S(1)}, bf16[256,768]{1,0:T(8,128)(2,1)S(1)}, u32[]{:S(2)}, u32[]{:S(2)}) %collective-permute-start.22) | collective-permute-done | bytes 393248 | tf_op jit(solution)/shard_map/ppermute | solution.py:280
  207.9 13.7 %collective-permute-done.37.refs_9_ = bf16[256,640]{1,0:T(8,128)(2,1)S(1)} collective-permute-done((bf16[256,640]{1,0:T(8,128)(2,1)S(1)}, bf16[256,640]{1,0:T(8,128)(2,1)S(1)}, u32[]{:S(2)}, u32[]{:S(2)}) %collective-permute-start.37) | collective-permute-done | bytes 327712 | tf_op jit(solution)/shard_map/ppermute | solution.py:282
  223.3 5.3 %collective-permute-done.43.refs_15_ = bf16[256,640]{1,0:T(8,128)(2,1)S(1)} collective-permute-done((bf16[256,640]{1,0:T(8,128)(2,1)S(1)}, bf16[256,640]{1,0:T(8,128)(2,1)S(1)}, u32[]{:S(2)}, u32[]{:S(2)}) %collective-permute-start.43) | collective-permute-done | bytes 327712 | tf_op jit(solution)/shard_map/ppermute | solution.py:282
  230.6 4.5 %shard_map.122.refs_2_.right = bf16[512,640]{1,0:T(8,128)(2,1)S(1)} custom-call(s32[3]{0:T(128)S(1)} %pad_add_fusion.info.refs_0_, bf16[8,512,256]{2,1,0:T(8,128)(2,1)S(1)} %shard_map.120.refs_1_, bf16[512,1408]{1,0:T(8,128)(2,1)S(1)} %copy-done.2, bf16[512,1408]{1,0:T(8,128)(2,1)S(1)} %copy-done.3, bf16[256,640]{1,0:T(8,128)(2,1)} %collective-permute-done.32.refs_4_, ...), custom_call_target="tpu_custom_call" | custom-call | flops 2684354560 | bytes 8912896 | tf_op jit(solution)/shard_map/pallas_call | solution.py:92
  237.0 4.0 %shard_map.121.refs_1_.left = bf16[512,768]{1,0:T(8,128)(2,1)S(1)} custom-call(s32[3]{0:T(128)S(1)} %pad_add_fusion.info.refs_0_, bf16[8,512,256]{2,1,0:T(8,128)(2,1)S(1)} %shard_map.120.refs_1_, bf16[512,1408]{1,0:T(8,128)(2,1)S(1)} %copy-done.2, bf16[512,1408]{1,0:T(8,128)(2,1)S(1)} %copy-done.3, bf16[256,768]{1,0:T(8,128)(2,1)S(1)} %copy-done.11, ...), custom_call_target="tpu_custom_call" | custom-call | flops 3221225472 | bytes 9699328 | tf_op jit(solution)/shard_map/pallas_call | solution.py:92
  241.0 3.8 %collective-permute-done.46.refs_6_ = bf16[1408,128]{1,0:T(8,128)(2,1)S(1)} collective-permute-done((bf16[1408,128]{1,0:T(8,128)(2,1)S(1)}, bf16[1408,128]{1,0:T(8,128)(2,1)S(1)}, u32[]{:S(2)}, u32[]{:S(2)}) %collective-permute-start.46) | collective-permute-done | bytes 360480 | tf_op jit(solution)/shard_map/ppermute | solution.py:282
  244.7 7.7 %collective-permute-done.50.refs_10_ = bf16[1408,128]{1,0:T(8,128)(2,1)S(1)} collective-permute-done((bf16[1408,128]{1,0:T(8,128)(2,1)S(1)}, bf16[1408,128]{1,0:T(8,128)(2,1)S(1)}, u32[]{:S(2)}, u32[]{:S(2)}) %collective-permute-start.50) | collective-permute-done | bytes 360480 | tf_op jit(solution)/shard_map/ppermute | solution.py:282
  252.5 7.7 %collective-permute-done.47.refs_7_ = bf16[1408,128]{1,0:T(8,128)(2,1)S(1)} collective-permute-done((bf16[1408,128]{1,0:T(8,128)(2,1)S(1)}, bf16[1408,128]{1,0:T(8,128)(2,1)S(1)}, u32[]{:S(2)}, u32[]{:S(2)}) %collective-permute-start.47) | collective-permute-done | bytes 360480 | tf_op jit(solution)/shard_map/ppermute | solution.py:282
  260.2 6.5 %collective-permute-done.51.refs_11_ = bf16[1408,128]{1,0:T(8,128)(2,1)S(1)} collective-permute-done((bf16[1408,128]{1,0:T(8,128)(2,1)S(1)}, bf16[1408,128]{1,0:T(8,128)(2,1)S(1)}, u32[]{:S(2)}, u32[]{:S(2)}) %collective-permute-start.51) | collective-permute-done | bytes 360480 | tf_op jit(solution)/shard_map/ppermute | solution.py:282
  266.7 5.0 %shard_map.123 = (bf16[2,4,512,128]{3,2,1,0:T(8,128)(2,1)S(1)}, bf16[2,4,512,128]{3,2,1,0:T(8,128)(2,1)}) custom-call(s32[3]{0:T(128)S(1)} %pad_add_fusion.info.refs_0_, bf16[512,768]{1,0:T(8,128)(2,1)S(1)} %shard_map.121.refs_1_.left, bf16[512,640]{1,0:T(8,128)(2,1)S(1)} %shard_map.122.refs_2_.right, bf16[1408,512]{1,0:T(8,128)(2,1)S(1)} %copy-done.1, ...), custom_call_target="tpu_custom_call" | custom-call | flops 2214592512 | bytes 5767168 | tf_op jit(solution)/shard_map/pallas_call | solution.py:92
  275.5 9.3 %collective-permute-done.54.cw = bf16[1408,128]{1,0:T(8,128)(2,1)S(1)} collective-permute-done((bf16[1408,128]{1,0:T(8,128)(2,1)S(1)}, bf16[1408,128]{1,0:T(8,128)(2,1)S(1)}, u32[]{:S(2)}, u32[]{:S(2)}) %collective-permute-start.54) | collective-permute-done | bytes 360480 | tf_op jit(solution)/shard_map/ppermute | solution.py:280
  286.6 4.1 %collective-permute-done.56.ccw = bf16[1408,128]{1,0:T(8,128)(2,1)} collective-permute-done((bf16[1408,128]{1,0:T(8,128)(2,1)S(1)}, bf16[1408,128]{1,0:T(8,128)(2,1)}, u32[]{:S(2)}, u32[]{:S(2)}) %collective-permute-start.56) | collective-permute-done | bytes 360480 | tf_op jit(solution)/shard_map/ppermute | solution.py:280
  296.0 6.2 %collective-permute-done.57.ccw_y = bf16[1408,128]{1,0:T(8,128)(2,1)} collective-permute-done((bf16[1408,128]{1,0:T(8,128)(2,1)}, bf16[1408,128]{1,0:T(8,128)(2,1)}, u32[]{:S(2)}, u32[]{:S(2)}) %collective-permute-start.57) | collective-permute-done | bytes 360480 | tf_op jit(solution)/shard_map/ppermute | solution.py:282
  312.5 12.3 %collective-permute-done.53 = bf16[4,512,128]{2,1,0:T(8,128)(2,1)S(1)} collective-permute-done((bf16[4,512,128]{2,1,0:T(8,128)(2,1)S(1)}, bf16[4,512,128]{2,1,0:T(8,128)(2,1)S(1)}, u32[]{:S(2)}, u32[]{:S(2)}) %collective-permute-start.53) | collective-permute-done | bytes 524320 | tf_op jit(solution)/shard_map/ppermute | solution.py:289
  325.2 6.7 %psum.7.squares = f32[1,512]{1,0:T(1,128)S(1)} all-reduce(f32[1,512]{1,0:T(1,128)S(1)} %bitcast.48), channel_id=1, replica_groups=mesh['grp'=2,'fs'=4,'tp'=4] {'tp'}, use_global_device_ids=true, to_apply=%region_1.2 | all-reduce | flops 512 | bytes 4096 | tf_op jit(solution)/shard_map/psum | solution.py:354
  (166 shorter events, 119.1 us)
Async XLA Ops:
  2.1 21.4 %collective-permute-start.1 = (bf16[2,512,256]{2,1,0:T(8,128)(2,1)S(1)}, bf16[2,512,256]{2,1,0:T(8,128)(2,1)S(1)}, u32[]{:S(2)}, u32[]{:S(2)}) collective-permute-start(bf16[2,512,256]{2,1,0:T(8,128)(2,1)S(1)} %bitcast.41), channel_id=1, source_target_pairs={{0,2},{1,3},{2,0},{3,1},{4,6},{5,7},{6,4},{7,5},{8,10},{9,11},{10,... | collective-permute-start | bytes 1572872 | tf_op jit(solution)/shard_map/ppermute | solution.py:289
  9.1 25.7 %collective-permute-start = (bf16[2,512,256]{2,1,0:T(8,128)(2,1)S(1)}, bf16[2,512,256]{2,1,0:T(8,128)(2,1)S(1)}, u32[]{:S(2)}, u32[]{:S(2)}) collective-permute-start(bf16[2,512,256]{2,1,0:T(8,128)(2,1)S(1)} %bitcast.42), channel_id=1, source_target_pairs={{0,1},{1,0},{2,3},{3,2},{4,5},{5,4},{6,7},{7,6},{8,9},{9,8},{10,11... | collective-permute-start | bytes 1572872 | tf_op jit(solution)/shard_map/ppermute | solution.py:286
  23.5 22.1 %collective-permute-start.2 = (bf16[2,512,256]{2,1,0:T(8,128)(2,1)S(1)}, bf16[2,512,256]{2,1,0:T(8,128)(2,1)S(1)}, u32[]{:S(2)}, u32[]{:S(2)}) collective-permute-start(bf16[2,512,256]{2,1,0:T(8,128)(2,1)S(1)} %collective-permute-done.1.b2), channel_id=1, source_target_pairs={{0,1},{1,0},{2,3},{3,2},{4,5},{5,4},{6,7},{7,6},{8,9},{9,8},{10,11... | collective-permute-start | bytes 1572872 | tf_op jit(solution)/shard_map/ppermute | solution.py:286
  39.8 15.8 %collective-permute-start.13 = (bf16[512,256]{1,0:T(8,128)(2,1)}, bf16[512,256]{1,0:T(8,128)(2,1)}, u32[]{:S(2)}, u32[]{:S(2)}) collective-permute-start(bf16[512,256]{1,0:T(8,128)(2,1)} %collective-permute-done.10.refs_14_), channel_id=1, source_target_pairs={{0,16},{16,0},{1,17},{17,1},{2,18},{18,2},{3,19},{19,3},{4,20},{20... | collective-permute-start | bytes 786440 | tf_op jit(solution)/shard_map/ppermute | solution.py:282
  43.1 18.0 %collective-permute-start.8 = (bf16[512,256]{1,0:T(8,128)(2,1)}, bf16[512,256]{1,0:T(8,128)(2,1)}, u32[]{:S(2)}, u32[]{:S(2)}) collective-permute-start(bf16[512,256]{1,0:T(8,128)(2,1)} %collective-permute-done.5.refs_9_), channel_id=1, source_target_pairs={{0,16},{16,0},{1,17},{17,1},{2,18},{18,2},{3,19},{19,3},{4,20},{20... | collective-permute-start | bytes 786440 | tf_op jit(solution)/shard_map/ppermute | solution.py:282
  45.6 18.4 %collective-permute-start.14 = (bf16[512,256]{1,0:T(8,128)(2,1)}, bf16[512,256]{1,0:T(8,128)(2,1)}, u32[]{:S(2)}, u32[]{:S(2)}) collective-permute-start(bf16[512,256]{1,0:T(8,128)(2,1)} %collective-permute-done.11.refs_15_), channel_id=1, source_target_pairs={{0,16},{16,0},{1,17},{17,1},{2,18},{18,2},{3,19},{19,3},{4,20},{20... | collective-permute-start | bytes 786440 | tf_op jit(solution)/shard_map/ppermute | solution.py:282
  73.1 53.5 %collective-permute-start.20 = (bf16[256,768]{1,0:T(8,128)(2,1)}, bf16[256,768]{1,0:T(8,128)(2,1)S(1)}, u32[]{:S(2)}, u32[]{:S(2)}) collective-permute-start(bf16[256,768]{1,0:T(8,128)(2,1)} %constant_dynamic-slice_fusion.1), channel_id=1, source_target_pairs={{0,4},{4,8},{8,12},{12,0},{1,5},{5,9},{9,13},{13,1},{2,6},{6,10},{... | collective-permute-start | bytes 1179656 | tf_op jit(solution)/shard_map/ppermute | solution.py:280
  76.6 52.0 %collective-permute-start.26 = (bf16[256,768]{1,0:T(8,128)(2,1)}, bf16[256,768]{1,0:T(8,128)(2,1)S(1)}, u32[]{:S(2)}, u32[]{:S(2)}) collective-permute-start(bf16[256,768]{1,0:T(8,128)(2,1)} %constant_dynamic-slice_fusion), channel_id=1, source_target_pairs={{4,0},{8,4},{12,8},{0,12},{5,1},{9,5},{13,9},{1,13},{6,2},{10,6},{... | collective-permute-start | bytes 1179656 | tf_op jit(solution)/shard_map/ppermute | solution.py:280
  80.4 22.3 %collective-permute-start.32 = (bf16[256,640]{1,0:T(8,128)(2,1)}, bf16[256,640]{1,0:T(8,128)(2,1)}, u32[]{:S(2)}, u32[]{:S(2)}) collective-permute-start(bf16[256,640]{1,0:T(8,128)(2,1)} %dynamic-slice.2), channel_id=1, source_target_pairs={{0,4},{4,8},{8,12},{12,0},{1,5},{5,9},{9,13},{13,1},{2,6},{6,10},{... | collective-permute-start | bytes 983048 | tf_op jit(solution)/shard_map/ppermute | solution.py:280
  82.2 27.6 %collective-permute-start.38 = (bf16[256,640]{1,0:T(8,128)(2,1)}, bf16[256,640]{1,0:T(8,128)(2,1)}, u32[]{:S(2)}, u32[]{:S(2)}) collective-permute-start(bf16[256,640]{1,0:T(8,128)(2,1)} %dynamic-slice.3), channel_id=1, source_target_pairs={{4,0},{8,4},{12,8},{0,12},{5,1},{9,5},{13,9},{1,13},{6,2},{10,6},{... | collective-permute-start | bytes 983048 | tf_op jit(solution)/shard_map/ppermute | solution.py:280
  86.1 31.3 %collective-permute-start.44 = (bf16[1408,128]{1,0:T(8,128)(2,1)S(1)}, bf16[1408,128]{1,0:T(8,128)(2,1)S(1)}, u32[]{:S(2)}, u32[]{:S(2)}) collective-permute-start(bf16[1408,128]{1,0:T(8,128)(2,1)S(1)} %get-tuple-element.20), channel_id=1, source_target_pairs={{0,4},{4,8},{8,12},{12,0},{1,5},{5,9},{9,13},{13,1},{2,6},{6,10},{... | collective-permute-start | bytes 1081352 | tf_op jit(solution)/shard_map/ppermute | solution.py:280
  102.7 22.1 %collective-permute-start.48 = (bf16[1408,128]{1,0:T(8,128)(2,1)S(1)}, bf16[1408,128]{1,0:T(8,128)(2,1)S(1)}, u32[]{:S(2)}, u32[]{:S(2)}) collective-permute-start(bf16[1408,128]{1,0:T(8,128)(2,1)S(1)} %get-tuple-element.19), channel_id=1, source_target_pairs={{4,0},{8,4},{12,8},{0,12},{5,1},{9,5},{13,9},{1,13},{6,2},{10,6},{... | collective-permute-start | bytes 1081352 | tf_op jit(solution)/shard_map/ppermute | solution.py:280
  109.7 22.5 %collective-permute-start.33 = (bf16[256,640]{1,0:T(8,128)(2,1)}, bf16[256,640]{1,0:T(8,128)(2,1)S(1)}, u32[]{:S(2)}, u32[]{:S(2)}) collective-permute-start(bf16[256,640]{1,0:T(8,128)(2,1)} %collective-permute-done.32.refs_4_), channel_id=1, source_target_pairs={{0,4},{4,8},{8,12},{12,0},{1,5},{5,9},{9,13},{13,1},{2,6},{6,10},{... | collective-permute-start | bytes 983048 | tf_op jit(solution)/shard_map/ppermute | solution.py:280
  117.4 29.8 %collective-permute-start.16 = (bf16[2,512,256]{2,1,0:T(8,128)(2,1)S(1)}, bf16[2,512,256]{2,1,0:T(8,128)(2,1)S(1)}, u32[]{:S(2)}, u32[]{:S(2)}) collective-permute-start(bf16[2,512,256]{2,1,0:T(8,128)(2,1)S(1)} %fusion.6), channel_id=1, source_target_pairs={{0,2},{1,3},{2,0},{3,1},{4,6},{5,7},{6,4},{7,5},{8,10},{9,11},{10,... | collective-permute-start | bytes 1572872 | tf_op jit(solution)/shard_map/ppermute | solution.py:289
  128.6 18.4 %collective-permute-start.45 = (bf16[1408,128]{1,0:T(8,128)(2,1)S(1)}, bf16[1408,128]{1,0:T(8,128)(2,1)S(1)}, u32[]{:S(2)}, u32[]{:S(2)}) collective-permute-start(bf16[1408,128]{1,0:T(8,128)(2,1)S(1)} %collective-permute-done.44.refs_4_), channel_id=1, source_target_pairs={{0,4},{4,8},{8,12},{12,0},{1,5},{5,9},{9,13},{13,1},{2,6},{6,10},{... | collective-permute-start | bytes 1081352 | tf_op jit(solution)/shard_map/ppermute | solution.py:280
  135.3 27.8 %collective-permute-start.21 = (bf16[256,768]{1,0:T(8,128)(2,1)S(1)}, bf16[256,768]{1,0:T(8,128)(2,1)S(1)}, u32[]{:S(2)}, u32[]{:S(2)}) collective-permute-start(bf16[256,768]{1,0:T(8,128)(2,1)S(1)} %collective-permute-done.20.refs_4_), channel_id=1, source_target_pairs={{0,4},{4,8},{8,12},{12,0},{1,5},{5,9},{9,13},{13,1},{2,6},{6,10},{... | collective-permute-start | bytes 1179656 | tf_op jit(solution)/shard_map/ppermute | solution.py:280
  139.2 23.4 %collective-permute-start.49 = (bf16[1408,128]{1,0:T(8,128)(2,1)S(1)}, bf16[1408,128]{1,0:T(8,128)(2,1)S(1)}, u32[]{:S(2)}, u32[]{:S(2)}) collective-permute-start(bf16[1408,128]{1,0:T(8,128)(2,1)S(1)} %collective-permute-done.48.refs_8_), channel_id=1, source_target_pairs={{4,0},{8,4},{12,8},{0,12},{5,1},{9,5},{13,9},{1,13},{6,2},{10,6},{... | collective-permute-start | bytes 1081352 | tf_op jit(solution)/shard_map/ppermute | solution.py:280
  141.7 22.0 %collective-permute-start.23 = (bf16[256,768]{1,0:T(8,128)(2,1)S(1)}, bf16[256,768]{1,0:T(8,128)(2,1)S(1)}, u32[]{:S(2)}, u32[]{:S(2)}) collective-permute-start(bf16[256,768]{1,0:T(8,128)(2,1)S(1)} %collective-permute-done.20.refs_4_), channel_id=1, source_target_pairs={{0,16},{16,0},{1,17},{17,1},{2,18},{18,2},{3,19},{19,3},{4,20},{20... | collective-permute-start | bytes 1179656 | tf_op jit(solution)/shard_map/ppermute | solution.py:282
  147.0 24.4 %collective-permute-start.27 = (bf16[256,768]{1,0:T(8,128)(2,1)S(1)}, bf16[256,768]{1,0:T(8,128)(2,1)S(1)}, u32[]{:S(2)}, u32[]{:S(2)}) collective-permute-start(bf16[256,768]{1,0:T(8,128)(2,1)S(1)} %collective-permute-done.26.refs_10_), channel_id=1, source_target_pairs={{4,0},{8,4},{12,8},{0,12},{5,1},{9,5},{13,9},{1,13},{6,2},{10,6},{... | collective-permute-start | bytes 1179656 | tf_op jit(solution)/shard_map/ppermute | solution.py:280
  147.2 26.4 %collective-permute-start.29 = (bf16[256,768]{1,0:T(8,128)(2,1)S(1)}, bf16[256,768]{1,0:T(8,128)(2,1)S(1)}, u32[]{:S(2)}, u32[]{:S(2)}) collective-permute-start(bf16[256,768]{1,0:T(8,128)(2,1)S(1)} %collective-permute-done.26.refs_10_), channel_id=1, source_target_pairs={{0,16},{16,0},{1,17},{17,1},{2,18},{18,2},{3,19},{19,3},{4,20},{20... | collective-permute-start | bytes 1179656 | tf_op jit(solution)/shard_map/ppermute | solution.py:282
  162.6 26.5 %collective-permute-start.18 = (bf16[2,512,256]{2,1,0:T(8,128)(2,1)S(1)}, bf16[2,512,256]{2,1,0:T(8,128)(2,1)S(1)}, u32[]{:S(2)}, u32[]{:S(2)}) collective-permute-start(bf16[2,512,256]{2,1,0:T(8,128)(2,1)S(1)} %fusion.5.b0), channel_id=1, source_target_pairs={{0,2},{1,3},{2,0},{3,1},{4,6},{5,7},{6,4},{7,5},{8,10},{9,11},{10,... | collective-permute-start | bytes 1572872 | tf_op jit(solution)/shard_map/ppermute | solution.py:289
  178.6 25.0 %collective-permute-start.17 = (bf16[2,512,256]{2,1,0:T(8,128)(2,1)S(1)}, bf16[2,512,256]{2,1,0:T(8,128)(2,1)S(1)}, u32[]{:S(2)}, u32[]{:S(2)}) collective-permute-start(bf16[2,512,256]{2,1,0:T(8,128)(2,1)S(1)} %fusion.5.b0), channel_id=1, source_target_pairs={{0,1},{1,0},{2,3},{3,2},{4,5},{5,4},{6,7},{7,6},{8,9},{9,8},{10,11... | collective-permute-start | bytes 1572872 | tf_op jit(solution)/shard_map/ppermute | solution.py:286
  197.3 33.0 %collective-permute-start.25 = (bf16[256,768]{1,0:T(8,128)(2,1)S(1)}, bf16[256,768]{1,0:T(8,128)(2,1)S(1)}, u32[]{:S(2)}, u32[]{:S(2)}) collective-permute-start(bf16[256,768]{1,0:T(8,128)(2,1)S(1)} %collective-permute-done.22.refs_6_), channel_id=1, source_target_pairs={{0,16},{16,0},{1,17},{17,1},{2,18},{18,2},{3,19},{19,3},{4,20},{20... | collective-permute-start | bytes 1179656 | tf_op jit(solution)/shard_map/ppermute | solution.py:282
  201.9 19.6 %collective-permute-start.37 = (bf16[256,640]{1,0:T(8,128)(2,1)S(1)}, bf16[256,640]{1,0:T(8,128)(2,1)S(1)}, u32[]{:S(2)}, u32[]{:S(2)}) collective-permute-start(bf16[256,640]{1,0:T(8,128)(2,1)S(1)} %collective-permute-done.34.refs_6_), channel_id=1, source_target_pairs={{0,16},{16,0},{1,17},{17,1},{2,18},{18,2},{3,19},{19,3},{4,20},{20... | collective-permute-start | bytes 983048 | tf_op jit(solution)/shard_map/ppermute | solution.py:282
  203.7 24.9 %collective-permute-start.43 = (bf16[256,640]{1,0:T(8,128)(2,1)S(1)}, bf16[256,640]{1,0:T(8,128)(2,1)S(1)}, u32[]{:S(2)}, u32[]{:S(2)}) collective-permute-start(bf16[256,640]{1,0:T(8,128)(2,1)S(1)} %collective-permute-done.40.refs_12_), channel_id=1, source_target_pairs={{0,16},{16,0},{1,17},{17,1},{2,18},{18,2},{3,19},{19,3},{4,20},{20... | collective-permute-start | bytes 983048 | tf_op jit(solution)/shard_map/ppermute | solution.py:282
  204.0 33.0 %collective-permute-start.31 = (bf16[256,768]{1,0:T(8,128)(2,1)S(1)}, bf16[256,768]{1,0:T(8,128)(2,1)S(1)}, u32[]{:S(2)}, u32[]{:S(2)}) collective-permute-start(bf16[256,768]{1,0:T(8,128)(2,1)S(1)} %collective-permute-done.28.refs_12_), channel_id=1, source_target_pairs={{0,16},{16,0},{1,17},{17,1},{2,18},{18,2},{3,19},{19,3},{4,20},{20... | collective-permute-start | bytes 1179656 | tf_op jit(solution)/shard_map/ppermute | solution.py:282
  207.2 37.5 %collective-permute-start.46 = (bf16[1408,128]{1,0:T(8,128)(2,1)S(1)}, bf16[1408,128]{1,0:T(8,128)(2,1)S(1)}, u32[]{:S(2)}, u32[]{:S(2)}) collective-permute-start(bf16[1408,128]{1,0:T(8,128)(2,1)S(1)} %collective-permute-done.44.refs_4_), channel_id=1, source_target_pairs={{0,16},{16,0},{1,17},{17,1},{2,18},{18,2},{3,19},{19,3},{4,20},{20... | collective-permute-start | bytes 1081352 | tf_op jit(solution)/shard_map/ppermute | solution.py:282
  221.6 30.9 %collective-permute-start.50 = (bf16[1408,128]{1,0:T(8,128)(2,1)S(1)}, bf16[1408,128]{1,0:T(8,128)(2,1)S(1)}, u32[]{:S(2)}, u32[]{:S(2)}) collective-permute-start(bf16[1408,128]{1,0:T(8,128)(2,1)S(1)} %collective-permute-done.48.refs_8_), channel_id=1, source_target_pairs={{0,16},{16,0},{1,17},{17,1},{2,18},{18,2},{3,19},{19,3},{4,20},{20... | collective-permute-start | bytes 1081352 | tf_op jit(solution)/shard_map/ppermute | solution.py:282
  228.6 31.6 %collective-permute-start.47 = (bf16[1408,128]{1,0:T(8,128)(2,1)S(1)}, bf16[1408,128]{1,0:T(8,128)(2,1)S(1)}, u32[]{:S(2)}, u32[]{:S(2)}) collective-permute-start(bf16[1408,128]{1,0:T(8,128)(2,1)S(1)} %collective-permute-done.45.refs_5_), channel_id=1, source_target_pairs={{0,16},{16,0},{1,17},{17,1},{2,18},{18,2},{3,19},{19,3},{4,20},{20... | collective-permute-start | bytes 1081352 | tf_op jit(solution)/shard_map/ppermute | solution.py:282
  230.3 36.4 %collective-permute-start.51 = (bf16[1408,128]{1,0:T(8,128)(2,1)S(1)}, bf16[1408,128]{1,0:T(8,128)(2,1)S(1)}, u32[]{:S(2)}, u32[]{:S(2)}) collective-permute-start(bf16[1408,128]{1,0:T(8,128)(2,1)S(1)} %collective-permute-done.49.refs_9_), channel_id=1, source_target_pairs={{0,16},{16,0},{1,17},{17,1},{2,18},{18,2},{3,19},{19,3},{4,20},{20... | collective-permute-start | bytes 1081352 | tf_op jit(solution)/shard_map/ppermute | solution.py:282
  271.7 36.7 %collective-permute-start.52 = (bf16[2,4,512,128]{3,2,1,0:T(8,128)(2,1)}, bf16[2,4,512,128]{3,2,1,0:T(8,128)(2,1)}, u32[]{:S(2)}, u32[]{:S(2)}) collective-permute-start(bf16[2,4,512,128]{3,2,1,0:T(8,128)(2,1)} %get-tuple-element.14), channel_id=1, source_target_pairs={{0,1},{1,0},{2,3},{3,2},{4,5},{5,4},{6,7},{7,6},{8,9},{9,8},{10,11... | collective-permute-start | bytes 3145736 | tf_op jit(solution)/shard_map/ppermute | solution.py:286
  272.3 18.4 %collective-permute-start.56 = (bf16[1408,128]{1,0:T(8,128)(2,1)S(1)}, bf16[1408,128]{1,0:T(8,128)(2,1)}, u32[]{:S(2)}, u32[]{:S(2)}) collective-permute-start(bf16[1408,128]{1,0:T(8,128)(2,1)S(1)} %collective-permute-done.49.refs_9_), channel_id=1, source_target_pairs={{4,0},{8,4},{12,8},{0,12},{5,1},{9,5},{13,9},{1,13},{6,2},{10,6},{... | collective-permute-start | bytes 1081352 | tf_op jit(solution)/shard_map/ppermute | solution.py:280
  (50 other events, 976.7 us)

commit v4 on v3

--- a/solution.py
+++ b/solution.py
@@ -209,46 +209,62 @@
     return call(kernel, info, operands, [(rows, size)], 4 * rows * 8 * half * size)[0]
 
 
-def down_early_kernel(*refs, count, split):
-    info, left, right, own = refs[:4]
-    steps = count - 2
-    groups = [refs[4 + i * steps : 4 + (i + 1) * steps] for i in range(4)]
+def split_refs(refs, steps):
+    return [refs[i * steps : (i + 1) * steps] for i in range(4)]
+
+
+def down_product(left, right, weight, split):
+    return dot(left[...], weight[:split]) + dot(right[...], weight[split:])
+
+
+def down_first_kernel(info, left, right, own, cw, cw_y, ccw, ccw_y, keep, give, *, count, split):
+    g = info[1]
+    rows, piece = keep.shape[-2:]
+
+    def store(step, direction, part, value):
+        sort_out(keep, give, place(info, step, direction, count), part, value)
+
+    value = down_product(left, right, own, split)
+    for i in range(4):
+        store(0, 1, i, value[:, i * piece : (i + 1) * piece])
+    weight = jnp.concatenate([p[...] for p in (cw, cw_y, ccw, ccw_y)], axis=1)
+    value = down_product(left, right, weight, split)
+    for last, direction in enumerate((1, -1)):
+        at = 2 * last * piece
+        store(1, direction, 2 * g + last, value[:, at : at + piece])
+        store(1, direction, 2 * (1 - g) + last, value[:, at + piece : at + 2 * piece])
+        for i in range(2):
+            store(count - 1, direction, 2 * i + last, jnp.zeros((rows, piece), F32))
+
+
+def down_next_kernel(*refs, count, split):
+    info, left, right, keep_in, give_in = refs[:5]
+    steps = count - 3
+    groups = split_refs(refs[5 : 5 + 4 * steps], steps)
     keep, give = refs[-2:]
     g = info[1]
-    rows, piece = keep.shape[-2:]
-
-    def product(weight):
-        return dot(left[...], weight[:split]) + dot(right[...], weight[split:])
-
-    def store(step, direction, part, value):
-        sort_out(keep, give, place(info, step, direction, count), part, value)
-
-    value = product(own[...])
-    for i in range(4):
-        store(0, 1, i, value[:, i * piece : (i + 1) * piece])
-    for direction, last, mine, other in ((1, 0, groups[0], groups[1]), (-1, 1, groups[2], groups[3])):
-        value = product(jnp.concatenate([p[...] for k in range(steps) for p in (mine[k], other[k])], axis=1))
-        for k in range(steps):
-            at = 2 * k * piece
-            store(k + 1, direction, 2 * g + last, value[:, at : at + piece])
-            store(k + 1, direction, 2 * (1 - g) + last, value[:, at + piece : at + 2 * piece])
-        for i in range(2):
-            store(count - 1, direction, 2 * i + last, jnp.zeros((rows, piece), F32))
-
-
-def down_late_kernel(info, left, right, cw, cw_y, ccw, ccw_y, near, far, *, count, split):
+    piece = keep.shape[-1]
+    keep[...] = keep_in[...]
+    give[...] = give_in[...]
+    for k in range(steps):
+        weight = jnp.concatenate([group[k][...] for group in groups], axis=1)
+        value = down_product(left, right, weight, split)
+        for last, direction in enumerate((1, -1)):
+            at = 2 * last * piece
+            spot = place(info, k + 2, direction, count)
+            sort_out(keep, give, spot, 2 * g + last, value[:, at : at + piece])
+            sort_out(keep, give, spot, 2 * (1 - g) + last, value[:, at + piece : at + 2 * piece])
+
+
+def down_late_kernel(info, left, right, cw, cw_y, ccw, ccw_y, out, *, count, split):
     g = info[1]
-    piece = near.shape[-1]
+    piece = out.shape[-1]
     weight = jnp.concatenate([p[...] for p in (cw, cw_y, ccw, ccw_y)], axis=1)
-    value = (dot(left[...], weight[:split]) + dot(right[...], weight[split:])).astype(BF16)
+    value = down_product(left, right, weight, split).astype(BF16)
     for i, direction in enumerate((1, -1)):
         spot = place(info, count - 1, direction, count) // 2
-        for at, target in enumerate((near, far)):
-
-            @pl.when(spot == at)
-            def _():
-                target[g] = value[:, 2 * i * piece : (2 * i + 1) * piece]
-                target[1 - g] = value[:, (2 * i + 1) * piece : (2 * i + 2) * piece]
+        out[spot, g] = value[:, 2 * i * piece : (2 * i + 1) * piece]
+        out[spot, 1 - g] = value[:, (2 * i + 1) * piece : (2 * i + 2) * piece]
 
 
 def close_kernel(squares, second, gain, out, *, width):
@@ -313,46 +329,53 @@
     d_ccw = ring(down_half[:, half // 2 :], behind)
 
     def scatter(partial):
-        met = partial[0].astype(F32) + mate(partial[1]).astype(F32)
-        return met[0] + across(met[1].astype(BF16)).astype(F32)
+        keep, got = partial[0], mate(partial[1])
+        far = (keep[1].astype(F32) + got[1].astype(F32)).astype(BF16)
+        far = lax.optimization_barrier(far)
+        near = keep[0].astype(F32) + got[0].astype(F32)
+        return near, across(far).astype(F32)
 
     x = norm_call(info, mix_gain, blocks)
+    own_gain = lax.dynamic_slice_in_dim(out_gain, q * columns, columns, 0).reshape(4, 1, half // 2)
+    x, own_gain = lax.optimization_barrier((x, own_gain))
     owns = (gate_outer, gate_inner, value_weight, mix_out)
     partial = mixer_call(info, conv_taps, x, owns, *m_cw, *m_ccw, count, length)
-    first = (own_tokens.astype(F32) + scatter(partial)).astype(BF16)
+    near, other = scatter(partial)
+    first = (own_tokens.astype(F32) + (near + other)).astype(BF16)
     blocks = gather(first)
     x = norm_call(info, ffn_gain, blocks)
     left = hidden_call(info, x, ffn_gate, ffn_up, *g1, *u1, count, 0, split)
     right = hidden_call(info, x, ffn_gate, ffn_up, *g2, *u2, count, split, units - split)
     flops = 2 * rows * units * width
-    early = [left, right, ffn_down, *[p for ring_part in (*d_cw, *d_ccw) for p in ring_part[:-1]]]
-    late = [left, right, *[ring_part[-1] for ring_part in (*d_cw, *d_ccw)]]
+    rings = (*d_cw, *d_ccw)
     split_by = {"count": count, "split": split}
     piece = (rows, half // 2)
-    kernel = functools.partial(down_early_kernel, **split_by)
-    partial = call(kernel, info, early, [(2, 4, *piece)] * 2, flops * 3 // 4)
+    kernel = functools.partial(down_first_kernel, **split_by)
+    operands = [left, right, ffn_down, *[ring_part[0] for ring_part in rings]]
+    partial = call(kernel, info, operands, [(2, 4, *piece)] * 2, flops // 2)
+    kernel = functools.partial(down_next_kernel, **split_by)
+    operands = [left, right, *partial, *[p for ring_part in rings for p in ring_part[1:-1]]]
+    partial = call(kernel, info, operands, [(2, 4, *piece)] * 2, flops // 4)
     second = first.reshape(2, rows, 2, half // 2).transpose(0, 2, 1, 3).reshape(4, rows, half // 2)
-    second = second.astype(F32) + scatter(partial)
+    near, other = scatter(partial)
+    second = lax.optimization_barrier(second.astype(F32) + near)
     kernel = functools.partial(down_late_kernel, **split_by)
-    near, far = call(kernel, info, late, [(2, *piece)] * 2, flops // 4)
-
-    both = [(s, i) for s in range(count) for i in range(4)]
-    takers = [(s, i) for s, i in both if (s + 1) % 2 == i % 2]
-    others = [(s, i) for s, i in both if (s + 1) % 2 != i % 2]
-
-    def late_send(value, senders, flip):
-        pairs = [(4 * s + i, 4 * s + (i ^ flip)) for s, i in senders]
-        return lax.ppermute(value, ("fs", "tp"), pairs).astype(F32)
-
-    met = late_send(far, takers, 2) + late_send(far, others, 3)
-    met = met + late_send(near, others, 1) + near.astype(F32)
+    late = [left, right, *[ring_part[-1] for ring_part in rings]]
+    rest = call(kernel, info, late, [(2, 2, *piece)], flops // 4)[0]
+
+    pairs = [(s, i) for s in range(count) for i in range(4)]
+    to_mate = [(4 * s + i, 4 * s + (i ^ 1)) for s, i in pairs if (s + 1) % 2 != i % 2]
+    to_other = [(4 * s + i, 4 * s + (i ^ 2)) for s, i in pairs if (s + 1) % 2 == i % 2]
+    got = lax.ppermute(rest, ("fs", "tp"), to_mate)
+    far = lax.optimization_barrier((rest[1].astype(F32) + got[1].astype(F32)).astype(BF16))
+    met = rest[0].astype(F32) + got[0].astype(F32)
+    met = met + lax.ppermute(far, ("fs", "tp"), to_other).astype(F32)
     takes = lax.rem(z + 1 + q, 2) == 0
     parity = jnp.where(q == lax.rem(z + 1, count), 0, 1)
     mask = takes & (jnp.arange(2) == parity)
     late_part = jnp.where(mask[None, :, None, None], met[:, None], 0.0).reshape(second.shape)
-    second = second + late_part
+    second = second + other + late_part
     squares = lax.psum(jnp.sum(second * second, axis=(0, 2)), "tp")
-    own_gain = lax.dynamic_slice_in_dim(out_gain, q * columns, columns, 0).reshape(4, 1, half // 2)
     in_vmem = pl.BlockSpec(memory_space=pltpu.VMEM)
     result = pl.pallas_call(
         functools.partial(close_kernel, width=width),

time: 333 us -> 309 us (0.928)
  waiting for transfers between devices: 208 us -> 186 us
  starting transfers between devices: 75.4 us -> 67.7 us
  other arithmetic: 3.81 us -> 7.37 us
    ppermute x24, waiting for transfers between devices: 119 us -> 105 us  [ring(): value = lax.ppermute(value, 'fs', pairs)]
    ppermute x24, waiting for transfers between devices: 75.6 us -> 68.5 us  [ring(): swapped.append(lax.ppermute(value, 'grp', [(0, 1), (1, 0)]))]
    ppermute x24, starting transfers between devices: 35.4 us -> 30.1 us  [ring(): swapped.append(lax.ppermute(value, 'grp', [(0, 1), (1, 0)]))]
    convert_element_type x1 -> x4, other arithmetic: 0.21 us -> 4.64 us  [the longest x2 2.35 us: scatter(): far = (keep[1].astype(F32) + got[1].astype(F32)).astype(BF16)]
    pallas_call x7 -> x8, Pallas kernels: 25.8 us -> 24.5 us  [call(): pl.pallas_call(kernel, in_specs=[pl.BlockSpec(memory_space=pltpu.SMEM)] +...]
  transfers between devices with their start and end apart: 61 -> 60, of which waited for: 39 -> 37; matrix products, arithmetic and copies ran while one was open for 4% -> 4% of each run, Pallas kernels for 4% -> 6%
where the time goes in v4:
time: 309 us; the launch traced here: 308 us
  waiting for transfers between devices  186 us (60%)
  starting transfers between devices  67.7 us (22%)
  Pallas kernels  25.5 us (8%)
  local copies, waits for them, and re-layouts  13.3 us (4%)
  blocking collectives  7.99 us (3%)
  other arithmetic  7.37 us (2%)
    ppermute x24, waiting for transfers between devices, ring(): value = lax.ppermute(value, 'fs', pairs)  105 us
    ppermute x24, waiting for transfers between devices, ring(): swapped.append(lax.ppermute(value, 'grp', [(0, 1), (1, 0)]))  68.5 us
    ppermute x24, starting transfers between devices, ring(): swapped.append(lax.ppermute(value, 'grp', [(0, 1), (1, 0)]))  30.1 us
    ppermute x24, starting transfers between devices, ring(): value = lax.ppermute(value, 'fs', pairs)  29 us
    pallas_call x8, Pallas kernels, call(): pl.pallas_call(kernel, in_specs=[pl.BlockSpec(memory_space=pltpu.SMEM)] +...  24.5 us
    ppermute x4, waiting for transfers between devices, across(): return lax.ppermute(value, 'tp', [(i, i ^ 2) for i in range(4)])  11.8 us
    psum x1, blocking collectives, ring_local(): squares = lax.psum(jnp.sum(second * second, axis=(0, 2)), 'tp')  7.99 us
  transfers between devices with their start and end apart: 60, of which 37 were waited for; matrix products, arithmetic and copies ran while one was open for 4% of the time, Pallas kernels for 6%

profile of v4, /device:TPU:0, one launch (start us, length us, event | category | flops | bytes accessed | tf_op | source)
XLA Modules:
  0.0 308.2 jit_solution(18185507127967776545)
XLA Ops:
  2.1 3.0 collective-permute-start.1
  9.1 7.1 %collective-permute-done.3.refs_7_ = bf16[512,256]{1,0:T(8,128)(2,1)S(1)} collective-permute-done((bf16[512,256]{1,0:T(8,128)(2,1)S(1)}, bf16[512,256]{1,0:T(8,128)(2,1)S(1)}, u32[]{:S(2)}, u32[]{:S(2)}) %collective-permute-start.3) | collective-permute-done | bytes 262176 | tf_op jit(solution)/shard_map/ppermute | solution.py:296
  16.2 4.6 %collective-permute-done.9.refs_13_ = bf16[512,256]{1,0:T(8,128)(2,1)S(1)} collective-permute-done((bf16[512,256]{1,0:T(8,128)(2,1)S(1)}, bf16[512,256]{1,0:T(8,128)(2,1)S(1)}, u32[]{:S(2)}, u32[]{:S(2)}) %collective-permute-start.9) | collective-permute-done | bytes 262176 | tf_op jit(solution)/shard_map/ppermute | solution.py:296
  24.9 3.4 %collective-permute-done.4.refs_8_ = bf16[512,256]{1,0:T(8,128)(2,1)S(1)} collective-permute-done((bf16[512,256]{1,0:T(8,128)(2,1)S(1)}, bf16[512,256]{1,0:T(8,128)(2,1)S(1)}, u32[]{:S(2)}, u32[]{:S(2)}) %collective-permute-start.4) | collective-permute-done | bytes 262176 | tf_op jit(solution)/shard_map/ppermute | solution.py:296
  28.3 5.6 %collective-permute-done.10.refs_14_ = bf16[512,256]{1,0:T(8,128)(2,1)} collective-permute-done((bf16[512,256]{1,0:T(8,128)(2,1)S(1)}, bf16[512,256]{1,0:T(8,128)(2,1)}, u32[]{:S(2)}, u32[]{:S(2)}) %collective-permute-start.10) | collective-permute-done | bytes 262176 | tf_op jit(solution)/shard_map/ppermute | solution.py:296
  49.7 5.6 %collective-permute-done.13.refs_17_ = bf16[512,256]{1,0:T(8,128)(2,1)} collective-permute-done((bf16[512,256]{1,0:T(8,128)(2,1)}, bf16[512,256]{1,0:T(8,128)(2,1)}, u32[]{:S(2)}, u32[]{:S(2)}) %collective-permute-start.13) | collective-permute-done | bytes 262176 | tf_op jit(solution)/shard_map/ppermute | solution.py:298
  55.3 5.6 %collective-permute-done.8.refs_12_ = bf16[512,256]{1,0:T(8,128)(2,1)} collective-permute-done((bf16[512,256]{1,0:T(8,128)(2,1)}, bf16[512,256]{1,0:T(8,128)(2,1)}, u32[]{:S(2)}, u32[]{:S(2)}) %collective-permute-start.8) | collective-permute-done | bytes 262176 | tf_op jit(solution)/shard_map/ppermute | solution.py:298
  60.9 3.4 %collective-permute-done.14.refs_18_ = bf16[512,256]{1,0:T(8,128)(2,1)} collective-permute-done((bf16[512,256]{1,0:T(8,128)(2,1)}, bf16[512,256]{1,0:T(8,128)(2,1)}, u32[]{:S(2)}, u32[]{:S(2)}) %collective-permute-start.14) | collective-permute-done | bytes 262176 | tf_op jit(solution)/shard_map/ppermute | solution.py:298
  67.2 7.0 %shard_map.119 = (bf16[2,2,512,256]{3,2,1,0:T(8,128)(2,1)S(1)}, bf16[2,2,512,256]{3,2,1,0:T(8,128)(2,1)}) custom-call(s32[3]{0:T(128)S(1)} %pad_add_fusion.info.refs_0_, f32[3,1024]{1,0:T(4,128)S(1)} %copy-done.21, bf16[8,512,256]{2,1,0:T(8,128)(2,1)S(1)} %shard_map.118.refs_2_, bf16[512,256]{1,0:T(8,128)(2,1)S(1)} %copy-done.3, ...), custom_call_target="tpu_custom_call" | custom-call | flops 2147483648 | bytes 6297600 | tf_op jit(solution)/shard_map/pallas_call | solution.py:92
  81.8 3.4 %collective-permute-start.38 = (bf16[256,640]{1,0:T(8,128)(2,1)}, bf16[256,640]{1,0:T(8,128)(2,1)}, u32[]{:S(2)}, u32[]{:S(2)}) collective-permute-start(bf16[256,640]{1,0:T(8,128)(2,1)} %dynamic-slice.3), channel_id=1, source_target_pairs={{4,0},{8,4},{12,8},{0,12},{5,1},{9,5},{13,9},{1,13},{6,2},{10,6},{... | collective-permute-start | bytes 983048 | tf_op jit(solution)/shard_map/ppermute | solution.py:296
  86.5 10.7 %collective-permute-done.32.refs_4_ = bf16[256,640]{1,0:T(8,128)(2,1)S(1)} collective-permute-done((bf16[256,640]{1,0:T(8,128)(2,1)}, bf16[256,640]{1,0:T(8,128)(2,1)S(1)}, u32[]{:S(2)}, u32[]{:S(2)}) %collective-permute-start.32) | collective-permute-done | bytes 327712 | tf_op jit(solution)/shard_map/ppermute | solution.py:296
  97.2 7.2 %collective-permute-done.38.refs_10_ = bf16[256,640]{1,0:T(8,128)(2,1)} collective-permute-done((bf16[256,640]{1,0:T(8,128)(2,1)}, bf16[256,640]{1,0:T(8,128)(2,1)}, u32[]{:S(2)}, u32[]{:S(2)}) %collective-permute-start.38) | collective-permute-done | bytes 327712 | tf_op jit(solution)/shard_map/ppermute | solution.py:296
  106.0 5.9 %collective-permute-done.44.cw = bf16[1408,128]{1,0:T(8,128)(2,1)S(1)} collective-permute-done((bf16[1408,128]{1,0:T(8,128)(2,1)S(1)}, bf16[1408,128]{1,0:T(8,128)(2,1)S(1)}, u32[]{:S(2)}, u32[]{:S(2)}) %collective-permute-start.44) | collective-permute-done | bytes 360480 | tf_op jit(solution)/shard_map/ppermute | solution.py:296
  112.0 16.0 %collective-permute-done.46.ccw = bf16[1408,128]{1,0:T(8,128)(2,1)S(1)} collective-permute-done((bf16[1408,128]{1,0:T(8,128)(2,1)S(1)}, bf16[1408,128]{1,0:T(8,128)(2,1)S(1)}, u32[]{:S(2)}, u32[]{:S(2)}) %collective-permute-start.46) | collective-permute-done | bytes 360480 | tf_op jit(solution)/shard_map/ppermute | solution.py:296
  146.1 3.9 %collective-permute-done.48.refs_5_ = bf16[1408,128]{1,0:T(8,128)(2,1)S(1)} collective-permute-done((bf16[1408,128]{1,0:T(8,128)(2,1)S(1)}, bf16[1408,128]{1,0:T(8,128)(2,1)S(1)}, u32[]{:S(2)}, u32[]{:S(2)}) %collective-permute-start.48) | collective-permute-done | bytes 360480 | tf_op jit(solution)/shard_map/ppermute | solution.py:296
  151.6 5.9 %collective-permute-done.50.refs_7_ = bf16[1408,128]{1,0:T(8,128)(2,1)S(1)} collective-permute-done((bf16[1408,128]{1,0:T(8,128)(2,1)S(1)}, bf16[1408,128]{1,0:T(8,128)(2,1)S(1)}, u32[]{:S(2)}, u32[]{:S(2)}) %collective-permute-start.50) | collective-permute-done | bytes 360480 | tf_op jit(solution)/shard_map/ppermute | solution.py:296
  167.8 3.8 %collective-permute-start.40 = (bf16[256,640]{1,0:T(8,128)(2,1)S(1)}, bf16[256,640]{1,0:T(8,128)(2,1)S(1)}, u32[]{:S(2)}, u32[]{:S(2)}) collective-permute-start(bf16[256,640]{1,0:T(8,128)(2,1)S(1)} %collective-permute-done.39.refs_11_), channel_id=1, source_target_pairs={{4,0},{8,4},{12,8},{0,12},{5,1},{9,5},{13,9},{1,13},{6,2},{10,6},{... | collective-permute-start | bytes 983048 | tf_op jit(solution)/shard_map/ppermute | solution.py:296
  176.8 4.9 %collective-permute-done.34.refs_6_ = bf16[256,640]{1,0:T(8,128)(2,1)S(1)} collective-permute-done((bf16[256,640]{1,0:T(8,128)(2,1)S(1)}, bf16[256,640]{1,0:T(8,128)(2,1)S(1)}, u32[]{:S(2)}, u32[]{:S(2)}) %collective-permute-start.34) | collective-permute-done | bytes 327712 | tf_op jit(solution)/shard_map/ppermute | solution.py:296
  183.3 5.2 %collective-permute-done.40.refs_12_ = bf16[256,640]{1,0:T(8,128)(2,1)S(1)} collective-permute-done((bf16[256,640]{1,0:T(8,128)(2,1)S(1)}, bf16[256,640]{1,0:T(8,128)(2,1)S(1)}, u32[]{:S(2)}, u32[]{:S(2)}) %collective-permute-start.40) | collective-permute-done | bytes 327712 | tf_op jit(solution)/shard_map/ppermute | solution.py:296
  191.1 6.1 %collective-permute-done.22.refs_6_ = bf16[256,768]{1,0:T(8,128)(2,1)S(1)} collective-permute-done((bf16[256,768]{1,0:T(8,128)(2,1)S(1)}, bf16[256,768]{1,0:T(8,128)(2,1)S(1)}, u32[]{:S(2)}, u32[]{:S(2)}) %collective-permute-start.22) | collective-permute-done | bytes 393248 | tf_op jit(solution)/shard_map/ppermute | solution.py:296
  199.2 5.8 %collective-permute-done.28.refs_12_ = bf16[256,768]{1,0:T(8,128)(2,1)S(1)} collective-permute-done((bf16[256,768]{1,0:T(8,128)(2,1)S(1)}, bf16[256,768]{1,0:T(8,128)(2,1)S(1)}, u32[]{:S(2)}, u32[]{:S(2)}) %collective-permute-start.28) | collective-permute-done | bytes 393248 | tf_op jit(solution)/shard_map/ppermute | solution.py:296
  210.7 6.8 %collective-permute-done.25.refs_9_ = bf16[256,768]{1,0:T(8,128)(2,1)S(1)} collective-permute-done((bf16[256,768]{1,0:T(8,128)(2,1)S(1)}, bf16[256,768]{1,0:T(8,128)(2,1)S(1)}, u32[]{:S(2)}, u32[]{:S(2)}) %collective-permute-start.25) | collective-permute-done | bytes 393248 | tf_op jit(solution)/shard_map/ppermute | solution.py:298
  217.6 8.4 %collective-permute-done.31.refs_15_ = bf16[256,768]{1,0:T(8,128)(2,1)S(1)} collective-permute-done((bf16[256,768]{1,0:T(8,128)(2,1)S(1)}, bf16[256,768]{1,0:T(8,128)(2,1)S(1)}, u32[]{:S(2)}, u32[]{:S(2)}) %collective-permute-start.31) | collective-permute-done | bytes 393248 | tf_op jit(solution)/shard_map/ppermute | solution.py:298
  227.8 4.0 %shard_map.121.left.refs_1_ = bf16[512,768]{1,0:T(8,128)(2,1)S(1)} custom-call(s32[3]{0:T(128)S(1)} %pad_add_fusion.info.refs_0_, bf16[8,512,256]{2,1,0:T(8,128)(2,1)S(1)} %shard_map.120.refs_1_, bf16[512,1408]{1,0:T(8,128)(2,1)S(1)} %copy-done.1, bf16[512,1408]{1,0:T(8,128)(2,1)S(1)} %copy-done.2, bf16[256,768]{1,0:T(8,128)(2,1)S(1)} %collective-permute-done.20.refs_4_, ...), custom_call_target="tpu_custom_call" | custom-call | flops 3221225472 | bytes 9699328 | tf_op jit(solution)/shard_map/pallas_call | solution.py:92
  234.6 5.4 %collective-permute-done.43.refs_15_ = bf16[256,640]{1,0:T(8,128)(2,1)S(1)} collective-permute-done((bf16[256,640]{1,0:T(8,128)(2,1)S(1)}, bf16[256,640]{1,0:T(8,128)(2,1)S(1)}, u32[]{:S(2)}, u32[]{:S(2)}) %collective-permute-start.43) | collective-permute-done | bytes 327712 | tf_op jit(solution)/shard_map/ppermute | solution.py:298
  241.6 4.4 %shard_map.122.right.refs_2_ = bf16[512,640]{1,0:T(8,128)(2,1)S(1)} custom-call(s32[3]{0:T(128)S(1)} %pad_add_fusion.info.refs_0_, bf16[8,512,256]{2,1,0:T(8,128)(2,1)S(1)} %shard_map.120.refs_1_, bf16[512,1408]{1,0:T(8,128)(2,1)S(1)} %copy-done.1, bf16[512,1408]{1,0:T(8,128)(2,1)S(1)} %copy-done.2, bf16[256,640]{1,0:T(8,128)(2,1)S(1)} %copy-done.12, ...), custom_call_target="tpu_custom_call" | custom-call | flops 2684354560 | bytes 8912896 | tf_op jit(solution)/shard_map/pallas_call | solution.py:92
  251.0 4.4 %collective-permute-done.49.refs_6_ = bf16[1408,128]{1,0:T(8,128)(2,1)S(1)} collective-permute-done((bf16[1408,128]{1,0:T(8,128)(2,1)S(1)}, bf16[1408,128]{1,0:T(8,128)(2,1)S(1)}, u32[]{:S(2)}, u32[]{:S(2)}) %collective-permute-start.49) | collective-permute-done | bytes 360480 | tf_op jit(solution)/shard_map/ppermute | solution.py:298
  255.5 7.7 %collective-permute-done.51.refs_8_ = bf16[1408,128]{1,0:T(8,128)(2,1)S(1)} collective-permute-done((bf16[1408,128]{1,0:T(8,128)(2,1)S(1)}, bf16[1408,128]{1,0:T(8,128)(2,1)S(1)}, u32[]{:S(2)}, u32[]{:S(2)}) %collective-permute-start.51) | collective-permute-done | bytes 360480 | tf_op jit(solution)/shard_map/ppermute | solution.py:298
  265.1 5.9 %collective-permute-done.55.cw_y = bf16[1408,128]{1,0:T(8,128)(2,1)S(1)} collective-permute-done((bf16[1408,128]{1,0:T(8,128)(2,1)S(1)}, bf16[1408,128]{1,0:T(8,128)(2,1)S(1)}, u32[]{:S(2)}, u32[]{:S(2)}) %collective-permute-start.55) | collective-permute-done | bytes 360480 | tf_op jit(solution)/shard_map/ppermute | solution.py:298
  270.9 5.7 %collective-permute-done.57.ccw_y = bf16[1408,128]{1,0:T(8,128)(2,1)S(1)} collective-permute-done((bf16[1408,128]{1,0:T(8,128)(2,1)S(1)}, bf16[1408,128]{1,0:T(8,128)(2,1)S(1)}, u32[]{:S(2)}, u32[]{:S(2)}) %collective-permute-start.57) | collective-permute-done | bytes 360480 | tf_op jit(solution)/shard_map/ppermute | solution.py:298
  287.1 11.8 %collective-permute-done.53 = bf16[4,512,128]{2,1,0:T(8,128)(2,1)S(1)} collective-permute-done((bf16[4,512,128]{2,1,0:T(8,128)(2,1)S(1)}, bf16[4,512,128]{2,1,0:T(8,128)(2,1)S(1)}, u32[]{:S(2)}, u32[]{:S(2)}) %collective-permute-start.53) | collective-permute-done | bytes 524320 | tf_op jit(solution)/shard_map/ppermute | solution.py:305
  299.2 8.0 %psum.7.squares = f32[1,512]{1,0:T(1,128)S(1)} all-reduce(f32[1,512]{1,0:T(1,128)S(1)} %bitcast.43), channel_id=1, replica_groups=mesh['grp'=2,'fs'=4,'tp'=4] {'tp'}, use_global_device_ids=true, to_apply=%region_1.2 | all-reduce | flops 512 | bytes 4096 | tf_op jit(solution)/shard_map/psum | solution.py:378
  (171 shorter events, 111.3 us)
Async XLA Ops:
  2.1 21.3 %collective-permute-start.1 = (bf16[2,512,256]{2,1,0:T(8,128)(2,1)S(1)}, bf16[2,512,256]{2,1,0:T(8,128)(2,1)S(1)}, u32[]{:S(2)}, u32[]{:S(2)}) collective-permute-start(bf16[2,512,256]{2,1,0:T(8,128)(2,1)S(1)} %bitcast.36), channel_id=1, source_target_pairs={{0,2},{1,3},{2,0},{3,1},{4,6},{5,7},{6,4},{7,5},{8,10},{9,11},{10,... | collective-permute-start | bytes 1572872 | tf_op jit(solution)/shard_map/ppermute | solution.py:305
  9.1 25.7 %collective-permute-start = (bf16[2,512,256]{2,1,0:T(8,128)(2,1)S(1)}, bf16[2,512,256]{2,1,0:T(8,128)(2,1)S(1)}, u32[]{:S(2)}, u32[]{:S(2)}) collective-permute-start(bf16[2,512,256]{2,1,0:T(8,128)(2,1)S(1)} %bitcast.37), channel_id=1, source_target_pairs={{0,1},{1,0},{2,3},{3,2},{4,5},{5,4},{6,7},{7,6},{8,9},{9,8},{10,11... | collective-permute-start | bytes 1572872 | tf_op jit(solution)/shard_map/ppermute | solution.py:302
  23.4 22.4 %collective-permute-start.2 = (bf16[2,512,256]{2,1,0:T(8,128)(2,1)S(1)}, bf16[2,512,256]{2,1,0:T(8,128)(2,1)S(1)}, u32[]{:S(2)}, u32[]{:S(2)}) collective-permute-start(bf16[2,512,256]{2,1,0:T(8,128)(2,1)S(1)} %collective-permute-done.1.b2), channel_id=1, source_target_pairs={{0,1},{1,0},{2,3},{3,2},{4,5},{5,4},{6,7},{7,6},{8,9},{9,8},{10,11... | collective-permute-start | bytes 1572872 | tf_op jit(solution)/shard_map/ppermute | solution.py:302
  45.8 18.5 %collective-permute-start.14 = (bf16[512,256]{1,0:T(8,128)(2,1)}, bf16[512,256]{1,0:T(8,128)(2,1)}, u32[]{:S(2)}, u32[]{:S(2)}) collective-permute-start(bf16[512,256]{1,0:T(8,128)(2,1)} %collective-permute-done.11.refs_15_), channel_id=1, source_target_pairs={{0,16},{16,0},{1,17},{17,1},{2,18},{18,2},{3,19},{19,3},{4,20},{20... | collective-permute-start | bytes 786440 | tf_op jit(solution)/shard_map/ppermute | solution.py:298
  74.2 57.7 %collective-permute-start.15 = (bf16[2,2,512,256]{3,2,1,0:T(8,128)(2,1)}, bf16[2,2,512,256]{3,2,1,0:T(8,128)(2,1)}, u32[]{:S(2)}, u32[]{:S(2)}) collective-permute-start(bf16[2,2,512,256]{3,2,1,0:T(8,128)(2,1)} %get-tuple-element.15), channel_id=1, source_target_pairs={{0,1},{1,0},{2,3},{3,2},{4,5},{5,4},{6,7},{7,6},{8,9},{9,8},{10,11... | collective-permute-start | bytes 3145736 | tf_op jit(solution)/shard_map/ppermute | solution.py:302
  76.1 53.4 %collective-permute-start.20 = (bf16[256,768]{1,0:T(8,128)(2,1)}, bf16[256,768]{1,0:T(8,128)(2,1)S(1)}, u32[]{:S(2)}, u32[]{:S(2)}) collective-permute-start(bf16[256,768]{1,0:T(8,128)(2,1)} %constant_dynamic-slice_fusion.1), channel_id=1, source_target_pairs={{0,4},{4,8},{8,12},{12,0},{1,5},{5,9},{9,13},{13,1},{2,6},{6,10},{... | collective-permute-start | bytes 1179656 | tf_op jit(solution)/shard_map/ppermute | solution.py:296
  79.6 17.6 %collective-permute-start.32 = (bf16[256,640]{1,0:T(8,128)(2,1)}, bf16[256,640]{1,0:T(8,128)(2,1)S(1)}, u32[]{:S(2)}, u32[]{:S(2)}) collective-permute-start(bf16[256,640]{1,0:T(8,128)(2,1)} %dynamic-slice.2), channel_id=1, source_target_pairs={{0,4},{4,8},{8,12},{12,0},{1,5},{5,9},{9,13},{13,1},{2,6},{6,10},{... | collective-permute-start | bytes 983048 | tf_op jit(solution)/shard_map/ppermute | solution.py:296
  81.8 22.6 %collective-permute-start.38 = (bf16[256,640]{1,0:T(8,128)(2,1)}, bf16[256,640]{1,0:T(8,128)(2,1)}, u32[]{:S(2)}, u32[]{:S(2)}) collective-permute-start(bf16[256,640]{1,0:T(8,128)(2,1)} %dynamic-slice.3), channel_id=1, source_target_pairs={{4,0},{8,4},{12,8},{0,12},{5,1},{9,5},{13,9},{1,13},{6,2},{10,6},{... | collective-permute-start | bytes 983048 | tf_op jit(solution)/shard_map/ppermute | solution.py:296
  85.2 26.7 %collective-permute-start.44 = (bf16[1408,128]{1,0:T(8,128)(2,1)S(1)}, bf16[1408,128]{1,0:T(8,128)(2,1)S(1)}, u32[]{:S(2)}, u32[]{:S(2)}) collective-permute-start(bf16[1408,128]{1,0:T(8,128)(2,1)S(1)} %get-tuple-element.24), channel_id=1, source_target_pairs={{0,4},{4,8},{8,12},{12,0},{1,5},{5,9},{9,13},{13,1},{2,6},{6,10},{... | collective-permute-start | bytes 1081352 | tf_op jit(solution)/shard_map/ppermute | solution.py:296
  97.2 34.3 %collective-permute-start.26 = (bf16[256,768]{1,0:T(8,128)(2,1)S(1)}, bf16[256,768]{1,0:T(8,128)(2,1)S(1)}, u32[]{:S(2)}, u32[]{:S(2)}) collective-permute-start(bf16[256,768]{1,0:T(8,128)(2,1)S(1)} %constant_dynamic-slice_fusion), channel_id=1, source_target_pairs={{4,0},{8,4},{12,8},{0,12},{5,1},{9,5},{13,9},{1,13},{6,2},{10,6},{... | collective-permute-start | bytes 1179656 | tf_op jit(solution)/shard_map/ppermute | solution.py:296
  104.4 23.6 %collective-permute-start.46 = (bf16[1408,128]{1,0:T(8,128)(2,1)S(1)}, bf16[1408,128]{1,0:T(8,128)(2,1)S(1)}, u32[]{:S(2)}, u32[]{:S(2)}) collective-permute-start(bf16[1408,128]{1,0:T(8,128)(2,1)S(1)} %get-tuple-element.23), channel_id=1, source_target_pairs={{4,0},{8,4},{12,8},{0,12},{5,1},{9,5},{13,9},{1,13},{6,2},{10,6},{... | collective-permute-start | bytes 1081352 | tf_op jit(solution)/shard_map/ppermute | solution.py:296
  112.0 23.2 %collective-permute-start.33 = (bf16[256,640]{1,0:T(8,128)(2,1)S(1)}, bf16[256,640]{1,0:T(8,128)(2,1)S(1)}, u32[]{:S(2)}, u32[]{:S(2)}) collective-permute-start(bf16[256,640]{1,0:T(8,128)(2,1)S(1)} %collective-permute-done.32.refs_4_), channel_id=1, source_target_pairs={{0,4},{4,8},{8,12},{12,0},{1,5},{5,9},{9,13},{13,1},{2,6},{6,10},{... | collective-permute-start | bytes 983048 | tf_op jit(solution)/shard_map/ppermute | solution.py:296
  131.9 18.1 %collective-permute-start.48 = (bf16[1408,128]{1,0:T(8,128)(2,1)S(1)}, bf16[1408,128]{1,0:T(8,128)(2,1)S(1)}, u32[]{:S(2)}, u32[]{:S(2)}) collective-permute-start(bf16[1408,128]{1,0:T(8,128)(2,1)S(1)} %collective-permute-done.44.cw), channel_id=1, source_target_pairs={{0,4},{4,8},{8,12},{12,0},{1,5},{5,9},{9,13},{13,1},{2,6},{6,10},{... | collective-permute-start | bytes 1081352 | tf_op jit(solution)/shard_map/ppermute | solution.py:296
  135.2 32.6 %collective-permute-start.16 = (bf16[2,512,256]{2,1,0:T(8,128)(2,1)S(1)}, bf16[2,512,256]{2,1,0:T(8,128)(2,1)S(1)}, u32[]{:S(2)}, u32[]{:S(2)}) collective-permute-start(bf16[2,512,256]{2,1,0:T(8,128)(2,1)S(1)} %fusion.3), channel_id=1, source_target_pairs={{0,2},{1,3},{2,0},{3,1},{4,6},{5,7},{6,4},{7,5},{8,10},{9,11},{10,... | collective-permute-start | bytes 1572872 | tf_op jit(solution)/shard_map/ppermute | solution.py:305
  138.5 19.0 %collective-permute-start.50 = (bf16[1408,128]{1,0:T(8,128)(2,1)S(1)}, bf16[1408,128]{1,0:T(8,128)(2,1)S(1)}, u32[]{:S(2)}, u32[]{:S(2)}) collective-permute-start(bf16[1408,128]{1,0:T(8,128)(2,1)S(1)} %collective-permute-done.46.ccw), channel_id=1, source_target_pairs={{4,0},{8,4},{12,8},{0,12},{5,1},{9,5},{13,9},{1,13},{6,2},{10,6},{... | collective-permute-start | bytes 1081352 | tf_op jit(solution)/shard_map/ppermute | solution.py:296
  142.3 23.9 %collective-permute-start.21 = (bf16[256,768]{1,0:T(8,128)(2,1)S(1)}, bf16[256,768]{1,0:T(8,128)(2,1)S(1)}, u32[]{:S(2)}, u32[]{:S(2)}) collective-permute-start(bf16[256,768]{1,0:T(8,128)(2,1)S(1)} %collective-permute-done.20.refs_4_), channel_id=1, source_target_pairs={{0,4},{4,8},{8,12},{12,0},{1,5},{5,9},{9,13},{13,1},{2,6},{6,10},{... | collective-permute-start | bytes 1179656 | tf_op jit(solution)/shard_map/ppermute | solution.py:296
  144.5 21.7 %collective-permute-start.23 = (bf16[256,768]{1,0:T(8,128)(2,1)S(1)}, bf16[256,768]{1,0:T(8,128)(2,1)S(1)}, u32[]{:S(2)}, u32[]{:S(2)}) collective-permute-start(bf16[256,768]{1,0:T(8,128)(2,1)S(1)} %collective-permute-done.20.refs_4_), channel_id=1, source_target_pairs={{0,16},{16,0},{1,17},{17,1},{2,18},{18,2},{3,19},{19,3},{4,20},{20... | collective-permute-start | bytes 1179656 | tf_op jit(solution)/shard_map/ppermute | solution.py:298
  157.5 17.1 %collective-permute-start.27 = (bf16[256,768]{1,0:T(8,128)(2,1)S(1)}, bf16[256,768]{1,0:T(8,128)(2,1)S(1)}, u32[]{:S(2)}, u32[]{:S(2)}) collective-permute-start(bf16[256,768]{1,0:T(8,128)(2,1)S(1)} %collective-permute-done.26.refs_10_), channel_id=1, source_target_pairs={{4,0},{8,4},{12,8},{0,12},{5,1},{9,5},{13,9},{1,13},{6,2},{10,6},{... | collective-permute-start | bytes 1179656 | tf_op jit(solution)/shard_map/ppermute | solution.py:296
  167.8 20.7 %collective-permute-start.40 = (bf16[256,640]{1,0:T(8,128)(2,1)S(1)}, bf16[256,640]{1,0:T(8,128)(2,1)S(1)}, u32[]{:S(2)}, u32[]{:S(2)}) collective-permute-start(bf16[256,640]{1,0:T(8,128)(2,1)S(1)} %collective-permute-done.39.refs_11_), channel_id=1, source_target_pairs={{4,0},{8,4},{12,8},{0,12},{5,1},{9,5},{13,9},{1,13},{6,2},{10,6},{... | collective-permute-start | bytes 983048 | tf_op jit(solution)/shard_map/ppermute | solution.py:296
  181.7 17.0 %collective-permute-start.24 = (bf16[256,768]{1,0:T(8,128)(2,1)S(1)}, bf16[256,768]{1,0:T(8,128)(2,1)S(1)}, u32[]{:S(2)}, u32[]{:S(2)}) collective-permute-start(bf16[256,768]{1,0:T(8,128)(2,1)S(1)} %collective-permute-done.21.refs_5_), channel_id=1, source_target_pairs={{0,16},{16,0},{1,17},{17,1},{2,18},{18,2},{3,19},{19,3},{4,20},{20... | collective-permute-start | bytes 1179656 | tf_op jit(solution)/shard_map/ppermute | solution.py:298
  198.8 18.8 %collective-permute-start.25 = (bf16[256,768]{1,0:T(8,128)(2,1)S(1)}, bf16[256,768]{1,0:T(8,128)(2,1)S(1)}, u32[]{:S(2)}, u32[]{:S(2)}) collective-permute-start(bf16[256,768]{1,0:T(8,128)(2,1)S(1)} %collective-permute-done.22.refs_6_), channel_id=1, source_target_pairs={{0,16},{16,0},{1,17},{17,1},{2,18},{18,2},{3,19},{19,3},{4,20},{20... | collective-permute-start | bytes 1179656 | tf_op jit(solution)/shard_map/ppermute | solution.py:298
  205.0 21.0 %collective-permute-start.31 = (bf16[256,768]{1,0:T(8,128)(2,1)S(1)}, bf16[256,768]{1,0:T(8,128)(2,1)S(1)}, u32[]{:S(2)}, u32[]{:S(2)}) collective-permute-start(bf16[256,768]{1,0:T(8,128)(2,1)S(1)} %collective-permute-done.28.refs_12_), channel_id=1, source_target_pairs={{0,16},{16,0},{1,17},{17,1},{2,18},{18,2},{3,19},{19,3},{4,20},{20... | collective-permute-start | bytes 1179656 | tf_op jit(solution)/shard_map/ppermute | solution.py:298
  206.6 26.5 %collective-permute-start.37 = (bf16[256,640]{1,0:T(8,128)(2,1)S(1)}, bf16[256,640]{1,0:T(8,128)(2,1)S(1)}, u32[]{:S(2)}, u32[]{:S(2)}) collective-permute-start(bf16[256,640]{1,0:T(8,128)(2,1)S(1)} %collective-permute-done.34.refs_6_), channel_id=1, source_target_pairs={{0,16},{16,0},{1,17},{17,1},{2,18},{18,2},{3,19},{19,3},{4,20},{20... | collective-permute-start | bytes 983048 | tf_op jit(solution)/shard_map/ppermute | solution.py:298
  207.0 33.0 %collective-permute-start.43 = (bf16[256,640]{1,0:T(8,128)(2,1)S(1)}, bf16[256,640]{1,0:T(8,128)(2,1)S(1)}, u32[]{:S(2)}, u32[]{:S(2)}) collective-permute-start(bf16[256,640]{1,0:T(8,128)(2,1)S(1)} %collective-permute-done.40.refs_12_), channel_id=1, source_target_pairs={{0,16},{16,0},{1,17},{17,1},{2,18},{18,2},{3,19},{19,3},{4,20},{20... | collective-permute-start | bytes 983048 | tf_op jit(solution)/shard_map/ppermute | solution.py:298
  210.1 38.1 %collective-permute-start.47 = (bf16[1408,128]{1,0:T(8,128)(2,1)S(1)}, bf16[1408,128]{1,0:T(8,128)(2,1)S(1)}, u32[]{:S(2)}, u32[]{:S(2)}) collective-permute-start(bf16[1408,128]{1,0:T(8,128)(2,1)S(1)} %collective-permute-done.46.ccw), channel_id=1, source_target_pairs={{0,16},{16,0},{1,17},{17,1},{2,18},{18,2},{3,19},{19,3},{4,20},{20... | collective-permute-start | bytes 1081352 | tf_op jit(solution)/shard_map/ppermute | solution.py:298
  217.6 28.5 %collective-permute-start.54 = (bf16[1408,128]{1,0:T(8,128)(2,1)S(1)}, bf16[1408,128]{1,0:T(8,128)(2,1)S(1)}, u32[]{:S(2)}, u32[]{:S(2)}) collective-permute-start(bf16[1408,128]{1,0:T(8,128)(2,1)S(1)} %collective-permute-done.48.refs_5_), channel_id=1, source_target_pairs={{0,4},{4,8},{8,12},{12,0},{1,5},{5,9},{9,13},{13,1},{2,6},{6,10},{... | collective-permute-start | bytes 1081352 | tf_op jit(solution)/shard_map/ppermute | solution.py:296
  226.0 20.5 %collective-permute-start.56 = (bf16[1408,128]{1,0:T(8,128)(2,1)S(1)}, bf16[1408,128]{1,0:T(8,128)(2,1)S(1)}, u32[]{:S(2)}, u32[]{:S(2)}) collective-permute-start(bf16[1408,128]{1,0:T(8,128)(2,1)S(1)} %collective-permute-done.50.refs_7_), channel_id=1, source_target_pairs={{4,0},{8,4},{12,8},{0,12},{5,1},{9,5},{13,9},{1,13},{6,2},{10,6},{... | collective-permute-start | bytes 1081352 | tf_op jit(solution)/shard_map/ppermute | solution.py:296
  233.0 22.5 %collective-permute-start.49 = (bf16[1408,128]{1,0:T(8,128)(2,1)S(1)}, bf16[1408,128]{1,0:T(8,128)(2,1)S(1)}, u32[]{:S(2)}, u32[]{:S(2)}) collective-permute-start(bf16[1408,128]{1,0:T(8,128)(2,1)S(1)} %collective-permute-done.48.refs_5_), channel_id=1, source_target_pairs={{0,16},{16,0},{1,17},{17,1},{2,18},{18,2},{3,19},{19,3},{4,20},{20... | collective-permute-start | bytes 1081352 | tf_op jit(solution)/shard_map/ppermute | solution.py:298
  240.0 23.2 %collective-permute-start.51 = (bf16[1408,128]{1,0:T(8,128)(2,1)S(1)}, bf16[1408,128]{1,0:T(8,128)(2,1)S(1)}, u32[]{:S(2)}, u32[]{:S(2)}) collective-permute-start(bf16[1408,128]{1,0:T(8,128)(2,1)S(1)} %collective-permute-done.50.refs_7_), channel_id=1, source_target_pairs={{0,16},{16,0},{1,17},{17,1},{2,18},{18,2},{3,19},{19,3},{4,20},{20... | collective-permute-start | bytes 1081352 | tf_op jit(solution)/shard_map/ppermute | solution.py:298
  246.0 24.9 %collective-permute-start.55 = (bf16[1408,128]{1,0:T(8,128)(2,1)S(1)}, bf16[1408,128]{1,0:T(8,128)(2,1)S(1)}, u32[]{:S(2)}, u32[]{:S(2)}) collective-permute-start(bf16[1408,128]{1,0:T(8,128)(2,1)S(1)} %collective-permute-done.54.cw), channel_id=1, source_target_pairs={{0,16},{16,0},{1,17},{17,1},{2,18},{18,2},{3,19},{19,3},{4,20},{20... | collective-permute-start | bytes 1081352 | tf_op jit(solution)/shard_map/ppermute | solution.py:298
  246.5 30.1 %collective-permute-start.57 = (bf16[1408,128]{1,0:T(8,128)(2,1)S(1)}, bf16[1408,128]{1,0:T(8,128)(2,1)S(1)}, u32[]{:S(2)}, u32[]{:S(2)}) collective-permute-start(bf16[1408,128]{1,0:T(8,128)(2,1)S(1)} %collective-permute-done.56.ccw), channel_id=1, source_target_pairs={{0,16},{16,0},{1,17},{17,1},{2,18},{18,2},{3,19},{19,3},{4,20},{20... | collective-permute-start | bytes 1081352 | tf_op jit(solution)/shard_map/ppermute | solution.py:298
  265.0 17.9 %collective-permute-start.52 = (bf16[2,4,512,128]{3,2,1,0:T(8,128)(2,1)S(1)}, bf16[2,4,512,128]{3,2,1,0:T(8,128)(2,1)}, u32[]{:S(2)}, u32[]{:S(2)}) collective-permute-start(bf16[2,4,512,128]{3,2,1,0:T(8,128)(2,1)S(1)} %get-tuple-element.19), channel_id=1, source_target_pairs={{0,1},{1,0},{2,3},{3,2},{4,5},{5,4},{6,7},{7,6},{8,9},{9,8},{10,11... | collective-permute-start | bytes 3145736 | tf_op jit(solution)/shard_map/ppermute | solution.py:302
  (52 other events, 883.6 us)

commit v5 on v4

--- a/solution.py
+++ b/solution.py
@@ -368,13 +368,17 @@
     to_other = [(4 * s + i, 4 * s + (i ^ 2)) for s, i in pairs if (s + 1) % 2 == i % 2]
     got = lax.ppermute(rest, ("fs", "tp"), to_mate)
     far = lax.optimization_barrier((rest[1].astype(F32) + got[1].astype(F32)).astype(BF16))
-    met = rest[0].astype(F32) + got[0].astype(F32)
-    met = met + lax.ppermute(far, ("fs", "tp"), to_other).astype(F32)
     takes = lax.rem(z + 1 + q, 2) == 0
     parity = jnp.where(q == lax.rem(z + 1, count), 0, 1)
     mask = takes & (jnp.arange(2) == parity)
-    late_part = jnp.where(mask[None, :, None, None], met[:, None], 0.0).reshape(second.shape)
-    second = second + other + late_part
+
+    def late_part(value):
+        return jnp.where(mask[None, :, None, None], value[:, None], 0.0).reshape(second.shape)
+
+    crossed = lax.ppermute(far, ("fs", "tp"), to_other)
+    second = second + other + late_part(rest[0].astype(F32) + got[0].astype(F32))
+    second = lax.optimization_barrier(second)
+    second = second + late_part(crossed.astype(F32))
     squares = lax.psum(jnp.sum(second * second, axis=(0, 2)), "tp")
     in_vmem = pl.BlockSpec(memory_space=pltpu.VMEM)
     result = pl.pallas_call(

time: 309 us -> 309 us (level)
  waiting for transfers between devices: 186 us -> 190 us
  starting transfers between devices: 67.7 us -> 64.2 us
    ppermute x24, waiting for transfers between devices: 68.5 us -> 76.5 us  [ring(): swapped.append(lax.ppermute(value, 'grp', [(0, 1), (1, 0)]))]
    ppermute x24, waiting for transfers between devices: 105 us -> 100 us  [ring(): value = lax.ppermute(value, 'fs', pairs)]
    ppermute x24, starting transfers between devices: 29 us -> 24.9 us  [ring(): value = lax.ppermute(value, 'fs', pairs)]
  transfers between devices with their start and end apart: 60 -> 60, of which waited for: 37 -> 38; matrix products, arithmetic and copies ran while one was open for 4% -> 4% of each run, Pallas kernels for 6% -> 6%
where the time goes in v5:
time: 309 us; the launch traced here: 308 us
  waiting for transfers between devices  190 us (61%)
  starting transfers between devices  64.2 us (21%)
  Pallas kernels  25.5 us (8%)
  local copies, waits for them, and re-layouts  13.2 us (4%)
  blocking collectives  7.99 us (3%)
  other arithmetic  6.72 us (2%)
    ppermute x24, waiting for transfers between devices, ring(): value = lax.ppermute(value, 'fs', pairs)  100 us
    ppermute x24, waiting for transfers between devices, ring(): swapped.append(lax.ppermute(value, 'grp', [(0, 1), (1, 0)]))  76.5 us
    ppermute x24, starting transfers between devices, ring(): swapped.append(lax.ppermute(value, 'grp', [(0, 1), (1, 0)]))  30.7 us
    ppermute x24, starting transfers between devices, ring(): value = lax.ppermute(value, 'fs', pairs)  24.9 us
    pallas_call x8, Pallas kernels, call(): pl.pallas_call(kernel, in_specs=[pl.BlockSpec(memory_space=pltpu.SMEM)] +...  24.5 us
    ppermute x4, waiting for transfers between devices, across(): return lax.ppermute(value, 'tp', [(i, i ^ 2) for i in range(4)])  12.6 us
    psum x1, blocking collectives, ring_local(): squares = lax.psum(jnp.sum(second * second, axis=(0, 2)), 'tp')  7.99 us
  transfers between devices with their start and end apart: 60, of which 38 were waited for; matrix products, arithmetic and copies ran while one was open for 4% of the time, Pallas kernels for 6%

profile of v5, /device:TPU:0, one launch (start us, length us, event | category | flops | bytes accessed | tf_op | source)
XLA Modules:
  0.0 308.3 jit_solution(9150471461897327782)
XLA Ops:
  9.1 7.1 %collective-permute-done.3.refs_7_ = bf16[512,256]{1,0:T(8,128)(2,1)S(1)} collective-permute-done((bf16[512,256]{1,0:T(8,128)(2,1)S(1)}, bf16[512,256]{1,0:T(8,128)(2,1)S(1)}, u32[]{:S(2)}, u32[]{:S(2)}) %collective-permute-start.3) | collective-permute-done | bytes 262176 | tf_op jit(solution)/shard_map/ppermute | solution.py:296
  16.2 4.6 %collective-permute-done.9.refs_13_ = bf16[512,256]{1,0:T(8,128)(2,1)S(1)} collective-permute-done((bf16[512,256]{1,0:T(8,128)(2,1)S(1)}, bf16[512,256]{1,0:T(8,128)(2,1)S(1)}, u32[]{:S(2)}, u32[]{:S(2)}) %collective-permute-start.9) | collective-permute-done | bytes 262176 | tf_op jit(solution)/shard_map/ppermute | solution.py:296
  24.9 3.4 %collective-permute-done.4.refs_8_ = bf16[512,256]{1,0:T(8,128)(2,1)S(1)} collective-permute-done((bf16[512,256]{1,0:T(8,128)(2,1)S(1)}, bf16[512,256]{1,0:T(8,128)(2,1)S(1)}, u32[]{:S(2)}, u32[]{:S(2)}) %collective-permute-start.4) | collective-permute-done | bytes 262176 | tf_op jit(solution)/shard_map/ppermute | solution.py:296
  28.3 5.6 %collective-permute-done.10.refs_14_ = bf16[512,256]{1,0:T(8,128)(2,1)} collective-permute-done((bf16[512,256]{1,0:T(8,128)(2,1)S(1)}, bf16[512,256]{1,0:T(8,128)(2,1)}, u32[]{:S(2)}, u32[]{:S(2)}) %collective-permute-start.10) | collective-permute-done | bytes 262176 | tf_op jit(solution)/shard_map/ppermute | solution.py:296
  49.7 5.6 %collective-permute-done.13.refs_17_ = bf16[512,256]{1,0:T(8,128)(2,1)} collective-permute-done((bf16[512,256]{1,0:T(8,128)(2,1)}, bf16[512,256]{1,0:T(8,128)(2,1)}, u32[]{:S(2)}, u32[]{:S(2)}) %collective-permute-start.13) | collective-permute-done | bytes 262176 | tf_op jit(solution)/shard_map/ppermute | solution.py:298
  55.3 5.6 %collective-permute-done.8.refs_12_ = bf16[512,256]{1,0:T(8,128)(2,1)} collective-permute-done((bf16[512,256]{1,0:T(8,128)(2,1)}, bf16[512,256]{1,0:T(8,128)(2,1)}, u32[]{:S(2)}, u32[]{:S(2)}) %collective-permute-start.8) | collective-permute-done | bytes 262176 | tf_op jit(solution)/shard_map/ppermute | solution.py:298
  60.9 3.4 %collective-permute-done.14.refs_18_ = bf16[512,256]{1,0:T(8,128)(2,1)} collective-permute-done((bf16[512,256]{1,0:T(8,128)(2,1)}, bf16[512,256]{1,0:T(8,128)(2,1)}, u32[]{:S(2)}, u32[]{:S(2)}) %collective-permute-start.14) | collective-permute-done | bytes 262176 | tf_op jit(solution)/shard_map/ppermute | solution.py:298
  67.2 7.0 %shard_map.119 = (bf16[2,2,512,256]{3,2,1,0:T(8,128)(2,1)S(1)}, bf16[2,2,512,256]{3,2,1,0:T(8,128)(2,1)}) custom-call(s32[3]{0:T(128)S(1)} %pad_add_fusion.info.refs_0_, f32[3,1024]{1,0:T(4,128)S(1)} %copy-done.21, bf16[8,512,256]{2,1,0:T(8,128)(2,1)S(1)} %shard_map.118.refs_2_, bf16[512,256]{1,0:T(8,128)(2,1)S(1)} %copy-done.3, ...), custom_call_target="tpu_custom_call" | custom-call | flops 2147483648 | bytes 6297600 | tf_op jit(solution)/shard_map/pallas_call | solution.py:92
  81.7 3.4 %collective-permute-start.38 = (bf16[256,640]{1,0:T(8,128)(2,1)}, bf16[256,640]{1,0:T(8,128)(2,1)}, u32[]{:S(2)}, u32[]{:S(2)}) collective-permute-start(bf16[256,640]{1,0:T(8,128)(2,1)} %dynamic-slice.3), channel_id=1, source_target_pairs={{4,0},{8,4},{12,8},{0,12},{5,1},{9,5},{13,9},{1,13},{6,2},{10,6},{... | collective-permute-start | bytes 983048 | tf_op jit(solution)/shard_map/ppermute | solution.py:296
  86.5 10.7 %collective-permute-done.32.refs_4_ = bf16[256,640]{1,0:T(8,128)(2,1)S(1)} collective-permute-done((bf16[256,640]{1,0:T(8,128)(2,1)}, bf16[256,640]{1,0:T(8,128)(2,1)S(1)}, u32[]{:S(2)}, u32[]{:S(2)}) %collective-permute-start.32) | collective-permute-done | bytes 327712 | tf_op jit(solution)/shard_map/ppermute | solution.py:296
  97.2 7.2 %collective-permute-done.38.refs_10_ = bf16[256,640]{1,0:T(8,128)(2,1)} collective-permute-done((bf16[256,640]{1,0:T(8,128)(2,1)}, bf16[256,640]{1,0:T(8,128)(2,1)}, u32[]{:S(2)}, u32[]{:S(2)}) %collective-permute-start.38) | collective-permute-done | bytes 327712 | tf_op jit(solution)/shard_map/ppermute | solution.py:296
  106.0 5.9 %collective-permute-done.44.cw = bf16[1408,128]{1,0:T(8,128)(2,1)S(1)} collective-permute-done((bf16[1408,128]{1,0:T(8,128)(2,1)S(1)}, bf16[1408,128]{1,0:T(8,128)(2,1)S(1)}, u32[]{:S(2)}, u32[]{:S(2)}) %collective-permute-start.44) | collective-permute-done | bytes 360480 | tf_op jit(solution)/shard_map/ppermute | solution.py:296
  112.0 16.0 %collective-permute-done.46.ccw = bf16[1408,128]{1,0:T(8,128)(2,1)S(1)} collective-permute-done((bf16[1408,128]{1,0:T(8,128)(2,1)S(1)}, bf16[1408,128]{1,0:T(8,128)(2,1)S(1)}, u32[]{:S(2)}, u32[]{:S(2)}) %collective-permute-start.46) | collective-permute-done | bytes 360480 | tf_op jit(solution)/shard_map/ppermute | solution.py:296
  139.1 3.0 collective-permute-done.39.refs_11_
  147.1 6.1 %collective-permute-done.45.cw_y = bf16[1408,128]{1,0:T(8,128)(2,1)S(1)} collective-permute-done((bf16[1408,128]{1,0:T(8,128)(2,1)S(1)}, bf16[1408,128]{1,0:T(8,128)(2,1)S(1)}, u32[]{:S(2)}, u32[]{:S(2)}) %collective-permute-start.45) | collective-permute-done | bytes 360480 | tf_op jit(solution)/shard_map/ppermute | solution.py:298
  155.5 10.7 %collective-permute-done.50.refs_7_ = bf16[1408,128]{1,0:T(8,128)(2,1)S(1)} collective-permute-done((bf16[1408,128]{1,0:T(8,128)(2,1)S(1)}, bf16[1408,128]{1,0:T(8,128)(2,1)S(1)}, u32[]{:S(2)}, u32[]{:S(2)}) %collective-permute-start.50) | collective-permute-done | bytes 360480 | tf_op jit(solution)/shard_map/ppermute | solution.py:296
  168.7 3.3 %collective-permute-start.40 = (bf16[256,640]{1,0:T(8,128)(2,1)S(1)}, bf16[256,640]{1,0:T(8,128)(2,1)S(1)}, u32[]{:S(2)}, u32[]{:S(2)}) collective-permute-start(bf16[256,640]{1,0:T(8,128)(2,1)S(1)} %collective-permute-done.39.refs_11_), channel_id=1, source_target_pairs={{4,0},{8,4},{12,8},{0,12},{5,1},{9,5},{13,9},{1,13},{6,2},{10,6},{... | collective-permute-start | bytes 983048 | tf_op jit(solution)/shard_map/ppermute | solution.py:296
  173.3 6.7 %collective-permute-done.27.refs_11_ = bf16[256,768]{1,0:T(8,128)(2,1)S(1)} collective-permute-done((bf16[256,768]{1,0:T(8,128)(2,1)S(1)}, bf16[256,768]{1,0:T(8,128)(2,1)S(1)}, u32[]{:S(2)}, u32[]{:S(2)}) %collective-permute-start.27) | collective-permute-done | bytes 393248 | tf_op jit(solution)/shard_map/ppermute | solution.py:296
  186.8 3.4 %collective-permute-done.40.refs_12_ = bf16[256,640]{1,0:T(8,128)(2,1)S(1)} collective-permute-done((bf16[256,640]{1,0:T(8,128)(2,1)S(1)}, bf16[256,640]{1,0:T(8,128)(2,1)S(1)}, u32[]{:S(2)}, u32[]{:S(2)}) %collective-permute-start.40) | collective-permute-done | bytes 327712 | tf_op jit(solution)/shard_map/ppermute | solution.py:296
  192.7 6.0 %collective-permute-done.22.refs_6_ = bf16[256,768]{1,0:T(8,128)(2,1)S(1)} collective-permute-done((bf16[256,768]{1,0:T(8,128)(2,1)S(1)}, bf16[256,768]{1,0:T(8,128)(2,1)S(1)}, u32[]{:S(2)}, u32[]{:S(2)}) %collective-permute-start.22) | collective-permute-done | bytes 393248 | tf_op jit(solution)/shard_map/ppermute | solution.py:296
  201.5 3.3 %collective-permute-done.28.refs_12_ = bf16[256,768]{1,0:T(8,128)(2,1)S(1)} collective-permute-done((bf16[256,768]{1,0:T(8,128)(2,1)S(1)}, bf16[256,768]{1,0:T(8,128)(2,1)S(1)}, u32[]{:S(2)}, u32[]{:S(2)}) %collective-permute-start.28) | collective-permute-done | bytes 393248 | tf_op jit(solution)/shard_map/ppermute | solution.py:296
  212.3 6.8 %collective-permute-done.25.refs_9_ = bf16[256,768]{1,0:T(8,128)(2,1)S(1)} collective-permute-done((bf16[256,768]{1,0:T(8,128)(2,1)S(1)}, bf16[256,768]{1,0:T(8,128)(2,1)S(1)}, u32[]{:S(2)}, u32[]{:S(2)}) %collective-permute-start.25) | collective-permute-done | bytes 393248 | tf_op jit(solution)/shard_map/ppermute | solution.py:298
  219.2 8.4 %collective-permute-done.31.refs_15_ = bf16[256,768]{1,0:T(8,128)(2,1)S(1)} collective-permute-done((bf16[256,768]{1,0:T(8,128)(2,1)S(1)}, bf16[256,768]{1,0:T(8,128)(2,1)S(1)}, u32[]{:S(2)}, u32[]{:S(2)}) %collective-permute-start.31) | collective-permute-done | bytes 393248 | tf_op jit(solution)/shard_map/ppermute | solution.py:298
  228.0 4.0 %shard_map.121.left.refs_1_ = bf16[512,768]{1,0:T(8,128)(2,1)S(1)} custom-call(s32[3]{0:T(128)S(1)} %pad_add_fusion.info.refs_0_, bf16[8,512,256]{2,1,0:T(8,128)(2,1)S(1)} %shard_map.120.refs_1_, bf16[512,1408]{1,0:T(8,128)(2,1)S(1)} %copy-done.1, bf16[512,1408]{1,0:T(8,128)(2,1)S(1)} %copy-done.2, bf16[256,768]{1,0:T(8,128)(2,1)S(1)} %collective-permute-done.20.refs_4_, ...), custom_call_target="tpu_custom_call" | custom-call | flops 3221225472 | bytes 9699328 | tf_op jit(solution)/shard_map/pallas_call | solution.py:92
  236.2 5.4 %collective-permute-done.43.refs_15_ = bf16[256,640]{1,0:T(8,128)(2,1)S(1)} collective-permute-done((bf16[256,640]{1,0:T(8,128)(2,1)S(1)}, bf16[256,640]{1,0:T(8,128)(2,1)S(1)}, u32[]{:S(2)}, u32[]{:S(2)}) %collective-permute-start.43) | collective-permute-done | bytes 327712 | tf_op jit(solution)/shard_map/ppermute | solution.py:298
  243.2 4.4 %shard_map.122.right.refs_2_ = bf16[512,640]{1,0:T(8,128)(2,1)S(1)} custom-call(s32[3]{0:T(128)S(1)} %pad_add_fusion.info.refs_0_, bf16[8,512,256]{2,1,0:T(8,128)(2,1)S(1)} %shard_map.120.refs_1_, bf16[512,1408]{1,0:T(8,128)(2,1)S(1)} %copy-done.1, bf16[512,1408]{1,0:T(8,128)(2,1)S(1)} %copy-done.2, bf16[256,640]{1,0:T(8,128)(2,1)S(1)} %copy-done.12, ...), custom_call_target="tpu_custom_call" | custom-call | flops 2684354560 | bytes 8912896 | tf_op jit(solution)/shard_map/pallas_call | solution.py:92
  252.6 4.4 %collective-permute-done.49.refs_6_ = bf16[1408,128]{1,0:T(8,128)(2,1)S(1)} collective-permute-done((bf16[1408,128]{1,0:T(8,128)(2,1)S(1)}, bf16[1408,128]{1,0:T(8,128)(2,1)S(1)}, u32[]{:S(2)}, u32[]{:S(2)}) %collective-permute-start.49) | collective-permute-done | bytes 360480 | tf_op jit(solution)/shard_map/ppermute | solution.py:298
  257.1 7.7 %collective-permute-done.51.refs_8_ = bf16[1408,128]{1,0:T(8,128)(2,1)S(1)} collective-permute-done((bf16[1408,128]{1,0:T(8,128)(2,1)S(1)}, bf16[1408,128]{1,0:T(8,128)(2,1)S(1)}, u32[]{:S(2)}, u32[]{:S(2)}) %collective-permute-start.51) | collective-permute-done | bytes 360480 | tf_op jit(solution)/shard_map/ppermute | solution.py:298
  266.6 5.9 %collective-permute-done.55.cw_y = bf16[1408,128]{1,0:T(8,128)(2,1)S(1)} collective-permute-done((bf16[1408,128]{1,0:T(8,128)(2,1)S(1)}, bf16[1408,128]{1,0:T(8,128)(2,1)S(1)}, u32[]{:S(2)}, u32[]{:S(2)}) %collective-permute-start.55) | collective-permute-done | bytes 360480 | tf_op jit(solution)/shard_map/ppermute | solution.py:298
  272.5 3.9 %collective-permute-done.57.ccw_y = bf16[1408,128]{1,0:T(8,128)(2,1)S(1)} collective-permute-done((bf16[1408,128]{1,0:T(8,128)(2,1)S(1)}, bf16[1408,128]{1,0:T(8,128)(2,1)S(1)}, u32[]{:S(2)}, u32[]{:S(2)}) %collective-permute-start.57) | collective-permute-done | bytes 360480 | tf_op jit(solution)/shard_map/ppermute | solution.py:298
  286.1 12.6 %collective-permute-done.53 = bf16[4,512,128]{2,1,0:T(8,128)(2,1)S(1)} collective-permute-done((bf16[4,512,128]{2,1,0:T(8,128)(2,1)S(1)}, bf16[4,512,128]{2,1,0:T(8,128)(2,1)S(1)}, u32[]{:S(2)}, u32[]{:S(2)}) %collective-permute-start.53) | collective-permute-done | bytes 524320 | tf_op jit(solution)/shard_map/ppermute | solution.py:305
  299.3 8.0 %psum.7.squares = f32[1,512]{1,0:T(1,128)S(1)} all-reduce(f32[1,512]{1,0:T(1,128)S(1)} %bitcast.47), channel_id=1, replica_groups=mesh['grp'=2,'fs'=4,'tp'=4] {'tp'}, use_global_device_ids=true, to_apply=%region_1.2 | all-reduce | flops 512 | bytes 4096 | tf_op jit(solution)/shard_map/psum | solution.py:382
  (172 shorter events, 108.3 us)
Async XLA Ops:
  2.1 21.3 %collective-permute-start.1 = (bf16[2,512,256]{2,1,0:T(8,128)(2,1)S(1)}, bf16[2,512,256]{2,1,0:T(8,128)(2,1)S(1)}, u32[]{:S(2)}, u32[]{:S(2)}) collective-permute-start(bf16[2,512,256]{2,1,0:T(8,128)(2,1)S(1)} %bitcast.40), channel_id=1, source_target_pairs={{0,2},{1,3},{2,0},{3,1},{4,6},{5,7},{6,4},{7,5},{8,10},{9,11},{10,... | collective-permute-start | bytes 1572872 | tf_op jit(solution)/shard_map/ppermute | solution.py:305
  9.1 25.7 %collective-permute-start = (bf16[2,512,256]{2,1,0:T(8,128)(2,1)S(1)}, bf16[2,512,256]{2,1,0:T(8,128)(2,1)S(1)}, u32[]{:S(2)}, u32[]{:S(2)}) collective-permute-start(bf16[2,512,256]{2,1,0:T(8,128)(2,1)S(1)} %bitcast.41), channel_id=1, source_target_pairs={{0,1},{1,0},{2,3},{3,2},{4,5},{5,4},{6,7},{7,6},{8,9},{9,8},{10,11... | collective-permute-start | bytes 1572872 | tf_op jit(solution)/shard_map/ppermute | solution.py:302
  23.4 22.4 %collective-permute-start.2 = (bf16[2,512,256]{2,1,0:T(8,128)(2,1)S(1)}, bf16[2,512,256]{2,1,0:T(8,128)(2,1)S(1)}, u32[]{:S(2)}, u32[]{:S(2)}) collective-permute-start(bf16[2,512,256]{2,1,0:T(8,128)(2,1)S(1)} %collective-permute-done.1.b2), channel_id=1, source_target_pairs={{0,1},{1,0},{2,3},{3,2},{4,5},{5,4},{6,7},{7,6},{8,9},{9,8},{10,11... | collective-permute-start | bytes 1572872 | tf_op jit(solution)/shard_map/ppermute | solution.py:302
  44.1 16.8 %collective-permute-start.8 = (bf16[512,256]{1,0:T(8,128)(2,1)}, bf16[512,256]{1,0:T(8,128)(2,1)}, u32[]{:S(2)}, u32[]{:S(2)}) collective-permute-start(bf16[512,256]{1,0:T(8,128)(2,1)} %collective-permute-done.5.refs_9_), channel_id=1, source_target_pairs={{0,16},{16,0},{1,17},{17,1},{2,18},{18,2},{3,19},{19,3},{4,20},{20... | collective-permute-start | bytes 786440 | tf_op jit(solution)/shard_map/ppermute | solution.py:298
  45.8 18.5 %collective-permute-start.14 = (bf16[512,256]{1,0:T(8,128)(2,1)}, bf16[512,256]{1,0:T(8,128)(2,1)}, u32[]{:S(2)}, u32[]{:S(2)}) collective-permute-start(bf16[512,256]{1,0:T(8,128)(2,1)} %collective-permute-done.11.refs_15_), channel_id=1, source_target_pairs={{0,16},{16,0},{1,17},{17,1},{2,18},{18,2},{3,19},{19,3},{4,20},{20... | collective-permute-start | bytes 786440 | tf_op jit(solution)/shard_map/ppermute | solution.py:298
  74.2 57.7 %collective-permute-start.15 = (bf16[2,2,512,256]{3,2,1,0:T(8,128)(2,1)}, bf16[2,2,512,256]{3,2,1,0:T(8,128)(2,1)}, u32[]{:S(2)}, u32[]{:S(2)}) collective-permute-start(bf16[2,2,512,256]{3,2,1,0:T(8,128)(2,1)} %get-tuple-element.15), channel_id=1, source_target_pairs={{0,1},{1,0},{2,3},{3,2},{4,5},{5,4},{6,7},{7,6},{8,9},{9,8},{10,11... | collective-permute-start | bytes 3145736 | tf_op jit(solution)/shard_map/ppermute | solution.py:302
  76.1 53.4 %collective-permute-start.20 = (bf16[256,768]{1,0:T(8,128)(2,1)}, bf16[256,768]{1,0:T(8,128)(2,1)S(1)}, u32[]{:S(2)}, u32[]{:S(2)}) collective-permute-start(bf16[256,768]{1,0:T(8,128)(2,1)} %constant_dynamic-slice_fusion.1), channel_id=1, source_target_pairs={{0,4},{4,8},{8,12},{12,0},{1,5},{5,9},{9,13},{13,1},{2,6},{6,10},{... | collective-permute-start | bytes 1179656 | tf_op jit(solution)/shard_map/ppermute | solution.py:296
  79.5 17.6 %collective-permute-start.32 = (bf16[256,640]{1,0:T(8,128)(2,1)}, bf16[256,640]{1,0:T(8,128)(2,1)S(1)}, u32[]{:S(2)}, u32[]{:S(2)}) collective-permute-start(bf16[256,640]{1,0:T(8,128)(2,1)} %dynamic-slice.2), channel_id=1, source_target_pairs={{0,4},{4,8},{8,12},{12,0},{1,5},{5,9},{9,13},{13,1},{2,6},{6,10},{... | collective-permute-start | bytes 983048 | tf_op jit(solution)/shard_map/ppermute | solution.py:296
  81.7 22.6 %collective-permute-start.38 = (bf16[256,640]{1,0:T(8,128)(2,1)}, bf16[256,640]{1,0:T(8,128)(2,1)}, u32[]{:S(2)}, u32[]{:S(2)}) collective-permute-start(bf16[256,640]{1,0:T(8,128)(2,1)} %dynamic-slice.3), channel_id=1, source_target_pairs={{4,0},{8,4},{12,8},{0,12},{5,1},{9,5},{13,9},{1,13},{6,2},{10,6},{... | collective-permute-start | bytes 983048 | tf_op jit(solution)/shard_map/ppermute | solution.py:296
  85.2 26.7 %collective-permute-start.44 = (bf16[1408,128]{1,0:T(8,128)(2,1)S(1)}, bf16[1408,128]{1,0:T(8,128)(2,1)S(1)}, u32[]{:S(2)}, u32[]{:S(2)}) collective-permute-start(bf16[1408,128]{1,0:T(8,128)(2,1)S(1)} %get-tuple-element.24), channel_id=1, source_target_pairs={{0,4},{4,8},{8,12},{12,0},{1,5},{5,9},{9,13},{13,1},{2,6},{6,10},{... | collective-permute-start | bytes 1081352 | tf_op jit(solution)/shard_map/ppermute | solution.py:296
  97.2 34.3 %collective-permute-start.26 = (bf16[256,768]{1,0:T(8,128)(2,1)S(1)}, bf16[256,768]{1,0:T(8,128)(2,1)S(1)}, u32[]{:S(2)}, u32[]{:S(2)}) collective-permute-start(bf16[256,768]{1,0:T(8,128)(2,1)S(1)} %constant_dynamic-slice_fusion), channel_id=1, source_target_pairs={{4,0},{8,4},{12,8},{0,12},{5,1},{9,5},{13,9},{1,13},{6,2},{10,6},{... | collective-permute-start | bytes 1179656 | tf_op jit(solution)/shard_map/ppermute | solution.py:296
  104.3 23.6 %collective-permute-start.46 = (bf16[1408,128]{1,0:T(8,128)(2,1)S(1)}, bf16[1408,128]{1,0:T(8,128)(2,1)S(1)}, u32[]{:S(2)}, u32[]{:S(2)}) collective-permute-start(bf16[1408,128]{1,0:T(8,128)(2,1)S(1)} %get-tuple-element.23), channel_id=1, source_target_pairs={{4,0},{8,4},{12,8},{0,12},{5,1},{9,5},{13,9},{1,13},{6,2},{10,6},{... | collective-permute-start | bytes 1081352 | tf_op jit(solution)/shard_map/ppermute | solution.py:296
  111.9 23.2 %collective-permute-start.33 = (bf16[256,640]{1,0:T(8,128)(2,1)S(1)}, bf16[256,640]{1,0:T(8,128)(2,1)S(1)}, u32[]{:S(2)}, u32[]{:S(2)}) collective-permute-start(bf16[256,640]{1,0:T(8,128)(2,1)S(1)} %collective-permute-done.32.refs_4_), channel_id=1, source_target_pairs={{0,4},{4,8},{8,12},{12,0},{1,5},{5,9},{9,13},{13,1},{2,6},{6,10},{... | collective-permute-start | bytes 983048 | tf_op jit(solution)/shard_map/ppermute | solution.py:296
  131.9 21.4 %collective-permute-start.45 = (bf16[1408,128]{1,0:T(8,128)(2,1)S(1)}, bf16[1408,128]{1,0:T(8,128)(2,1)S(1)}, u32[]{:S(2)}, u32[]{:S(2)}) collective-permute-start(bf16[1408,128]{1,0:T(8,128)(2,1)S(1)} %collective-permute-done.44.cw), channel_id=1, source_target_pairs={{0,16},{16,0},{1,17},{17,1},{2,18},{18,2},{3,19},{19,3},{4,20},{20... | collective-permute-start | bytes 1081352 | tf_op jit(solution)/shard_map/ppermute | solution.py:298
  135.2 33.6 %collective-permute-start.16 = (bf16[2,512,256]{2,1,0:T(8,128)(2,1)S(1)}, bf16[2,512,256]{2,1,0:T(8,128)(2,1)S(1)}, u32[]{:S(2)}, u32[]{:S(2)}) collective-permute-start(bf16[2,512,256]{2,1,0:T(8,128)(2,1)S(1)} %fusion.4), channel_id=1, source_target_pairs={{0,2},{1,3},{2,0},{3,1},{4,6},{5,7},{6,4},{7,5},{8,10},{9,11},{10,... | collective-permute-start | bytes 1572872 | tf_op jit(solution)/shard_map/ppermute | solution.py:305
  138.5 16.7 %collective-permute-start.48 = (bf16[1408,128]{1,0:T(8,128)(2,1)S(1)}, bf16[1408,128]{1,0:T(8,128)(2,1)S(1)}, u32[]{:S(2)}, u32[]{:S(2)}) collective-permute-start(bf16[1408,128]{1,0:T(8,128)(2,1)S(1)} %collective-permute-done.44.cw), channel_id=1, source_target_pairs={{0,4},{4,8},{8,12},{12,0},{1,5},{5,9},{9,13},{13,1},{2,6},{6,10},{... | collective-permute-start | bytes 1081352 | tf_op jit(solution)/shard_map/ppermute | solution.py:296
  142.1 25.6 %collective-permute-start.21 = (bf16[256,768]{1,0:T(8,128)(2,1)S(1)}, bf16[256,768]{1,0:T(8,128)(2,1)S(1)}, u32[]{:S(2)}, u32[]{:S(2)}) collective-permute-start(bf16[256,768]{1,0:T(8,128)(2,1)S(1)} %collective-permute-done.20.refs_4_), channel_id=1, source_target_pairs={{0,4},{4,8},{8,12},{12,0},{1,5},{5,9},{9,13},{13,1},{2,6},{6,10},{... | collective-permute-start | bytes 1179656 | tf_op jit(solution)/shard_map/ppermute | solution.py:296
  145.5 22.8 %collective-permute-start.23 = (bf16[256,768]{1,0:T(8,128)(2,1)S(1)}, bf16[256,768]{1,0:T(8,128)(2,1)S(1)}, u32[]{:S(2)}, u32[]{:S(2)}) collective-permute-start(bf16[256,768]{1,0:T(8,128)(2,1)S(1)} %collective-permute-done.20.refs_4_), channel_id=1, source_target_pairs={{0,16},{16,0},{1,17},{17,1},{2,18},{18,2},{3,19},{19,3},{4,20},{20... | collective-permute-start | bytes 1179656 | tf_op jit(solution)/shard_map/ppermute | solution.py:298
  155.2 24.8 %collective-permute-start.27 = (bf16[256,768]{1,0:T(8,128)(2,1)S(1)}, bf16[256,768]{1,0:T(8,128)(2,1)S(1)}, u32[]{:S(2)}, u32[]{:S(2)}) collective-permute-start(bf16[256,768]{1,0:T(8,128)(2,1)S(1)} %collective-permute-done.26.refs_10_), channel_id=1, source_target_pairs={{4,0},{8,4},{12,8},{0,12},{5,1},{9,5},{13,9},{1,13},{6,2},{10,6},{... | collective-permute-start | bytes 1179656 | tf_op jit(solution)/shard_map/ppermute | solution.py:296
  168.3 16.8 %collective-permute-start.36 = (bf16[256,640]{1,0:T(8,128)(2,1)S(1)}, bf16[256,640]{1,0:T(8,128)(2,1)S(1)}, u32[]{:S(2)}, u32[]{:S(2)}) collective-permute-start(bf16[256,640]{1,0:T(8,128)(2,1)S(1)} %collective-permute-done.33.refs_5_), channel_id=1, source_target_pairs={{0,16},{16,0},{1,17},{17,1},{2,18},{18,2},{3,19},{19,3},{4,20},{20... | collective-permute-start | bytes 983048 | tf_op jit(solution)/shard_map/ppermute | solution.py:298
  168.7 21.4 %collective-permute-start.40 = (bf16[256,640]{1,0:T(8,128)(2,1)S(1)}, bf16[256,640]{1,0:T(8,128)(2,1)S(1)}, u32[]{:S(2)}, u32[]{:S(2)}) collective-permute-start(bf16[256,640]{1,0:T(8,128)(2,1)S(1)} %collective-permute-done.39.refs_11_), channel_id=1, source_target_pairs={{4,0},{8,4},{12,8},{0,12},{5,1},{9,5},{13,9},{1,13},{6,2},{10,6},{... | collective-permute-start | bytes 983048 | tf_op jit(solution)/shard_map/ppermute | solution.py:296
  200.3 18.8 %collective-permute-start.25 = (bf16[256,768]{1,0:T(8,128)(2,1)S(1)}, bf16[256,768]{1,0:T(8,128)(2,1)S(1)}, u32[]{:S(2)}, u32[]{:S(2)}) collective-permute-start(bf16[256,768]{1,0:T(8,128)(2,1)S(1)} %collective-permute-done.22.refs_6_), channel_id=1, source_target_pairs={{0,16},{16,0},{1,17},{17,1},{2,18},{18,2},{3,19},{19,3},{4,20},{20... | collective-permute-start | bytes 1179656 | tf_op jit(solution)/shard_map/ppermute | solution.py:298
  204.9 22.7 %collective-permute-start.31 = (bf16[256,768]{1,0:T(8,128)(2,1)S(1)}, bf16[256,768]{1,0:T(8,128)(2,1)S(1)}, u32[]{:S(2)}, u32[]{:S(2)}) collective-permute-start(bf16[256,768]{1,0:T(8,128)(2,1)S(1)} %collective-permute-done.28.refs_12_), channel_id=1, source_target_pairs={{0,16},{16,0},{1,17},{17,1},{2,18},{18,2},{3,19},{19,3},{4,20},{20... | collective-permute-start | bytes 1179656 | tf_op jit(solution)/shard_map/ppermute | solution.py:298
  206.5 28.1 %collective-permute-start.37 = (bf16[256,640]{1,0:T(8,128)(2,1)S(1)}, bf16[256,640]{1,0:T(8,128)(2,1)S(1)}, u32[]{:S(2)}, u32[]{:S(2)}) collective-permute-start(bf16[256,640]{1,0:T(8,128)(2,1)S(1)} %collective-permute-done.34.refs_6_), channel_id=1, source_target_pairs={{0,16},{16,0},{1,17},{17,1},{2,18},{18,2},{3,19},{19,3},{4,20},{20... | collective-permute-start | bytes 983048 | tf_op jit(solution)/shard_map/ppermute | solution.py:298
  206.9 34.7 %collective-permute-start.43 = (bf16[256,640]{1,0:T(8,128)(2,1)S(1)}, bf16[256,640]{1,0:T(8,128)(2,1)S(1)}, u32[]{:S(2)}, u32[]{:S(2)}) collective-permute-start(bf16[256,640]{1,0:T(8,128)(2,1)S(1)} %collective-permute-done.40.refs_12_), channel_id=1, source_target_pairs={{0,16},{16,0},{1,17},{17,1},{2,18},{18,2},{3,19},{19,3},{4,20},{20... | collective-permute-start | bytes 983048 | tf_op jit(solution)/shard_map/ppermute | solution.py:298
  210.7 39.0 %collective-permute-start.47 = (bf16[1408,128]{1,0:T(8,128)(2,1)S(1)}, bf16[1408,128]{1,0:T(8,128)(2,1)S(1)}, u32[]{:S(2)}, u32[]{:S(2)}) collective-permute-start(bf16[1408,128]{1,0:T(8,128)(2,1)S(1)} %collective-permute-done.46.ccw), channel_id=1, source_target_pairs={{0,16},{16,0},{1,17},{17,1},{2,18},{18,2},{3,19},{19,3},{4,20},{20... | collective-permute-start | bytes 1081352 | tf_op jit(solution)/shard_map/ppermute | solution.py:298
  219.1 28.5 %collective-permute-start.54 = (bf16[1408,128]{1,0:T(8,128)(2,1)S(1)}, bf16[1408,128]{1,0:T(8,128)(2,1)S(1)}, u32[]{:S(2)}, u32[]{:S(2)}) collective-permute-start(bf16[1408,128]{1,0:T(8,128)(2,1)S(1)} %collective-permute-done.48.refs_5_), channel_id=1, source_target_pairs={{0,4},{4,8},{8,12},{12,0},{1,5},{5,9},{9,13},{13,1},{2,6},{6,10},{... | collective-permute-start | bytes 1081352 | tf_op jit(solution)/shard_map/ppermute | solution.py:296
  227.6 20.5 %collective-permute-start.56 = (bf16[1408,128]{1,0:T(8,128)(2,1)S(1)}, bf16[1408,128]{1,0:T(8,128)(2,1)S(1)}, u32[]{:S(2)}, u32[]{:S(2)}) collective-permute-start(bf16[1408,128]{1,0:T(8,128)(2,1)S(1)} %collective-permute-done.50.refs_7_), channel_id=1, source_target_pairs={{4,0},{8,4},{12,8},{0,12},{5,1},{9,5},{13,9},{1,13},{6,2},{10,6},{... | collective-permute-start | bytes 1081352 | tf_op jit(solution)/shard_map/ppermute | solution.py:296
  234.6 22.5 %collective-permute-start.49 = (bf16[1408,128]{1,0:T(8,128)(2,1)S(1)}, bf16[1408,128]{1,0:T(8,128)(2,1)S(1)}, u32[]{:S(2)}, u32[]{:S(2)}) collective-permute-start(bf16[1408,128]{1,0:T(8,128)(2,1)S(1)} %collective-permute-done.48.refs_5_), channel_id=1, source_target_pairs={{0,16},{16,0},{1,17},{17,1},{2,18},{18,2},{3,19},{19,3},{4,20},{20... | collective-permute-start | bytes 1081352 | tf_op jit(solution)/shard_map/ppermute | solution.py:298
  241.6 23.2 %collective-permute-start.51 = (bf16[1408,128]{1,0:T(8,128)(2,1)S(1)}, bf16[1408,128]{1,0:T(8,128)(2,1)S(1)}, u32[]{:S(2)}, u32[]{:S(2)}) collective-permute-start(bf16[1408,128]{1,0:T(8,128)(2,1)S(1)} %collective-permute-done.50.refs_7_), channel_id=1, source_target_pairs={{0,16},{16,0},{1,17},{17,1},{2,18},{18,2},{3,19},{19,3},{4,20},{20... | collective-permute-start | bytes 1081352 | tf_op jit(solution)/shard_map/ppermute | solution.py:298
  247.6 24.9 %collective-permute-start.55 = (bf16[1408,128]{1,0:T(8,128)(2,1)S(1)}, bf16[1408,128]{1,0:T(8,128)(2,1)S(1)}, u32[]{:S(2)}, u32[]{:S(2)}) collective-permute-start(bf16[1408,128]{1,0:T(8,128)(2,1)S(1)} %collective-permute-done.54.cw), channel_id=1, source_target_pairs={{0,16},{16,0},{1,17},{17,1},{2,18},{18,2},{3,19},{19,3},{4,20},{20... | collective-permute-start | bytes 1081352 | tf_op jit(solution)/shard_map/ppermute | solution.py:298
  248.1 28.2 %collective-permute-start.57 = (bf16[1408,128]{1,0:T(8,128)(2,1)S(1)}, bf16[1408,128]{1,0:T(8,128)(2,1)S(1)}, u32[]{:S(2)}, u32[]{:S(2)}) collective-permute-start(bf16[1408,128]{1,0:T(8,128)(2,1)S(1)} %collective-permute-done.56.ccw), channel_id=1, source_target_pairs={{0,16},{16,0},{1,17},{17,1},{2,18},{18,2},{3,19},{19,3},{4,20},{20... | collective-permute-start | bytes 1081352 | tf_op jit(solution)/shard_map/ppermute | solution.py:298
  (52 other events, 874.2 us)
